TPU v7x, 32 devices: a whole 2x2x4 slice. The times are simulated.
32 devices in a mesh: kv: 4 (over y, x), tp: 8 (over z, core).
Axes of the slice: x: 2, y: 2, z: 4, core: 2. Of those that a mesh axis runs over, the one named last changes fastest.
Arguments:
- resid: bfloat16 [32, 4096], P('tp', 'kv'), may hold values from -35 to 35
- attn_gain: bfloat16 [4096], replicated, may hold values from 0.099609375 to 1.8984375
- w_query_nope: bfloat16 [4096, 8192], P('kv', 'tp'), may hold values from -0.09375 to 0.09375
- w_query_rope: bfloat16 [4096, 4096], P('kv', 'tp'), may hold values from -0.09375 to 0.09375
- w_latent: bfloat16 [4096, 512], P('kv'), may hold values from -0.09375 to 0.09375
- w_key_rope: bfloat16 [4096, 64], replicated, may hold values from -0.09375 to 0.09375
- latent_gain: bfloat16 [512], replicated, may hold values from 0.099609375 to 1.8984375
- key_up: bfloat16 [512, 64, 128], P(None, 'tp'), may hold values from -0.5 to 0.5
- value_up: bfloat16 [512, 64, 128], P(None, 'tp'), may hold values from -0.25 to 0.25
- w_out: bfloat16 [8192, 4096], P('tp', 'kv'), may hold values from -4 to 4
- post_gain: bfloat16 [4096], replicated, may hold values from 0.099609375 to 1.8984375
- mlp_gain: bfloat16 [4096], replicated, may hold values from 0.099609375 to 1.8984375
- w_gate: bfloat16 [4096, 11008], P('kv', 'tp'), may hold values from -3 to 3
- w_up: bfloat16 [4096, 11008], P('kv', 'tp'), may hold values from -3 to 3
- w_down: bfloat16 [11008, 4096], P('tp', 'kv'), may hold values from -0.0546875 to 0.0546875
- cache_latent: bfloat16 [32, 2048, 512], P('tp', 'kv'), may hold values from -6 to 6
- cache_rope_key: bfloat16 [32, 2048, 64], P('tp', 'kv'), may hold values from -740 to 740
Outputs:
- next_resid: bfloat16 [32, 4096], P('tp', 'kv')
- new_latent: bfloat16 [32, 512], P('tp')
- new_rope_key: bfloat16 [32, 64], P('tp')
All inputs are finite; a program needn't handle non-finite values.
Results may differ from a plain program's by a relative error of at most 0.035.
Values may be sent and summed in bfloat16 or wider, within the bound.
No kernel may reach another device: no remote copies, remote signals or barrier semaphores. Data moves between devices by JAX's collectives and lax.ppermute only.
A program may use at most 64 MiB of HBM per device.

v0:
```python
import jax
import jax.numpy as jnp
from jax import lax
from jax.sharding import PartitionSpec as P

EPS = 1e-06
THETA = 10000.0


def rotate(vector, position):
    half_width = vector.shape[-1] // 2
    frequency = THETA ** (-jnp.arange(half_width, dtype=jnp.float32) / half_width)
    angles = jnp.asarray(position, jnp.float32) * frequency
    cos_table, sin_table = (jnp.cos(angles), jnp.sin(angles))
    lower_half, upper_half = (vector[..., :half_width], vector[..., half_width:])
    return jnp.concatenate(
        [
            lower_half * cos_table - upper_half * sin_table,
            lower_half * sin_table + upper_half * cos_table,
        ],
        axis=-1,
    )


def body(
    resid,
    attn_gain,
    w_query_nope,
    w_query_rope,
    w_latent,
    w_key_rope,
    latent_gain,
    key_up,
    value_up,
    w_out,
    post_gain,
    mlp_gain,
    w_gate,
    w_up,
    w_down,
    cache_latent,
    cache_rope_key,
):
    kv_count = lax.axis_size("kv")
    kv_index = lax.axis_index("kv")
    tp_index = lax.axis_index("tp")
    own_rows, width_dev = resid.shape
    model_width = width_dev * kv_count
    heads_dev = key_up.shape[1]
    pos_dev = cache_latent.shape[1]
    context = pos_dev * kv_count
    score_scale = (key_up.shape[2] + cache_rope_key.shape[2]) ** (-0.5)
    col_start = kv_index * width_dev
    row_start = tp_index * own_rows

    def block_of(vector):
        return lax.dynamic_slice_in_dim(vector, col_start, width_dev, 0).astype(jnp.float32)[
            None, :
        ]

    gathered = lax.all_gather(resid, "tp", axis=0, tiled=True)
    batch_rows = gathered.shape[0]
    gathered_float = gathered.astype(jnp.float32)
    normed_a = (gathered_float * block_of(attn_gain)).astype(jnp.bfloat16)
    own_normed = lax.dynamic_slice_in_dim(normed_a, row_start, own_rows, 0)
    key_rows = lax.dynamic_slice_in_dim(w_key_rope, col_start, width_dev, 0)
    q_nope_sum, q_rope_sum, latent_sum, key_sum, square_sum = (
        lax.psum(
            jnp.dot(normed_a, w_query_nope, preferred_element_type=jnp.float32).astype(
                jnp.bfloat16
            ),
            "kv",
        ).astype(jnp.float32),
        lax.psum(
            jnp.dot(normed_a, w_query_rope, preferred_element_type=jnp.float32).astype(
                jnp.bfloat16
            ),
            "kv",
        ).astype(jnp.float32),
        lax.psum(
            jnp.dot(own_normed, w_latent, preferred_element_type=jnp.float32).astype(jnp.bfloat16),
            "kv",
        ).astype(jnp.float32),
        lax.psum(
            jnp.dot(own_normed, key_rows, preferred_element_type=jnp.float32).astype(jnp.bfloat16),
            "kv",
        ).astype(jnp.float32),
        lax.psum(
            jnp.sum(gathered_float * gathered_float, axis=1).astype(jnp.bfloat16), "kv"
        ).astype(jnp.float32),
    )
    scale_in = lax.rsqrt(square_sum / model_width + EPS)[:, None]
    own_scale = lax.dynamic_slice_in_dim(scale_in, row_start, own_rows, 0)
    q_nope = (q_nope_sum * scale_in).astype(jnp.bfloat16).reshape(batch_rows, heads_dev, -1)
    q_rope = rotate((q_rope_sum * scale_in).reshape(batch_rows, heads_dev, -1), context).astype(
        jnp.bfloat16
    )
    new_latent = (
        latent_sum
        * lax.rsqrt(jnp.mean(latent_sum * latent_sum, axis=1, keepdims=True) + EPS)
        * latent_gain.astype(jnp.float32)[None, :]
    ).astype(jnp.bfloat16)
    new_rope_key = rotate(key_sum * own_scale, context).astype(jnp.bfloat16)
    q_lat = jnp.einsum("bhd,chd->bhc", q_nope, key_up, preferred_element_type=jnp.float32).astype(
        jnp.bfloat16
    )
    seq_lat, seq_rope = (
        lax.all_to_all(q_lat, "tp", split_axis=0, concat_axis=1, tiled=True),
        lax.all_to_all(q_rope, "tp", split_axis=0, concat_axis=1, tiled=True),
    )
    scores = (
        jnp.einsum("bhc,bpc->bhp", seq_lat, cache_latent, preferred_element_type=jnp.float32)
        + jnp.einsum("bhr,bpr->bhp", seq_rope, cache_rope_key, preferred_element_type=jnp.float32)
    ) * score_scale
    own_score = (
        jnp.einsum("bhc,bc->bh", seq_lat, new_latent, preferred_element_type=jnp.float32)
        + jnp.einsum("bhr,br->bh", seq_rope, new_rope_key, preferred_element_type=jnp.float32)
    ) * score_scale
    local_peak = jnp.maximum(jnp.max(scores, axis=2), own_score)
    peak = lax.pmax(local_peak, "kv")
    probs = jnp.exp(scores - peak[:, :, None])
    own_prob = jnp.exp(own_score - peak)
    totals = lax.psum(jnp.sum(probs, axis=2), "kv") + own_prob
    partial_value = jnp.einsum(
        "bhp,bpc->bhc", probs.astype(jnp.bfloat16), cache_latent, preferred_element_type=jnp.float32
    )
    summed = (
        lax.psum(partial_value.astype(jnp.bfloat16), "kv").astype(jnp.float32)
        + own_prob[:, :, None] * new_latent.astype(jnp.float32)[:, None, :]
    )
    o_lat = (summed / totals[:, :, None]).astype(jnp.bfloat16)
    head_lat = lax.all_to_all(o_lat, "tp", split_axis=1, concat_axis=0, tiled=True)
    o_heads = jnp.einsum(
        "bhc,che->bhe", head_lat, value_up, preferred_element_type=jnp.float32
    ).astype(jnp.bfloat16)
    o_flat = o_heads.reshape(batch_rows, -1)
    attended = lax.psum_scatter(
        jnp.dot(o_flat, w_out, preferred_element_type=jnp.float32).astype(jnp.bfloat16),
        "tp",
        scatter_dimension=0,
        tiled=True,
    ).astype(jnp.float32)
    post_square = lax.psum(jnp.sum(attended * attended, axis=1), "kv")
    post_part = attended * lax.rsqrt(post_square / model_width + EPS)[:, None] * block_of(post_gain)
    resid_mid = (resid.astype(jnp.float32) + post_part).astype(jnp.bfloat16)
    mid_rows = lax.all_gather(resid_mid, "tp", axis=0, tiled=True)
    mid_float = mid_rows.astype(jnp.float32)
    normed_m = (mid_float * block_of(mlp_gain)).astype(jnp.bfloat16)
    gate_part = jnp.dot(normed_m, w_gate, preferred_element_type=jnp.float32)
    up_part = jnp.dot(normed_m, w_up, preferred_element_type=jnp.float32)
    square_part = jnp.sum(mid_float * mid_float, axis=1)
    gate_sum, up_sum, mid_square = (
        lax.psum(gate_part.astype(jnp.bfloat16), "kv").astype(jnp.float32),
        lax.psum(up_part.astype(jnp.bfloat16), "kv").astype(jnp.float32),
        lax.psum(square_part.astype(jnp.bfloat16), "kv").astype(jnp.float32),
    )
    scale_mid = lax.rsqrt(mid_square / model_width + EPS)[:, None]
    hidden = (jax.nn.silu(gate_sum * scale_mid) * (up_sum * scale_mid)).astype(jnp.bfloat16)
    lowered = lax.psum_scatter(
        jnp.dot(hidden, w_down, preferred_element_type=jnp.float32).astype(jnp.bfloat16),
        "tp",
        scatter_dimension=0,
        tiled=True,
    ).astype(jnp.float32)
    next_resid = (resid_mid.astype(jnp.float32) + lowered).astype(jnp.bfloat16)
    return (next_resid, new_latent, new_rope_key)


def solution(mesh):
    return jax.shard_map(
        body,
        mesh=mesh,
        in_specs=(
            P("tp", "kv"),
            P(),
            P("kv", "tp"),
            P("kv", "tp"),
            P("kv", None),
            P(),
            P(),
            P(None, "tp", None),
            P(None, "tp", None),
            P("tp", "kv"),
            P(),
            P(),
            P("kv", "tp"),
            P("kv", "tp"),
            P("tp", "kv"),
            P("tp", "kv", None),
            P("tp", "kv", None),
        ),
        out_specs=(P("tp", "kv"), P("tp", None), P("tp", None)),
        check_vma=False,
    )
```

profile of v0, /device:TPU:0, one launch (start us, length us, event | category | flops | bytes accessed | tf_op | source)
XLA Modules:
  0.0 386.5 jit_solution(13030384441631528125)
XLA Ops:
  7.2 16.0 %all-gather = bf16[8,4,1024]{2,1,0:T(4,128)(2,1)S(1)} all-gather(bf16[1,4,1024]{2,1,0:T(4,128)(2,1)} %bitcast.69), channel_id=1, replica_groups=mesh['kv'=4,'tp'=8] {'tp'}, dimensions={0}, use_global_device_ids=true | all-gather | bytes 73728 | tf_op jit(solution)/shard_map/all_gather | solution.py:61
  28.1 16.7 %all-reduce.2 = (bf16[32]{0:T(256)(128)(2,1)S(1)}, bf16[32,512]{1,0:T(8,128)(2,1)S(1)}, bf16[4,512]{1,0:T(4,128)(2,1)S(1)}, bf16[4,64]{1,0:T(4,128)(2,1)S(1)}) all-reduce(bf16[32]{0:T(256)(128)(2,1)S(1)} %get-tuple-element.15, bf16[32,512]{1,0:T(8,128)(2,1)S(1)} %convolution_convert_fusion.8, ...), channel_id=1, replica_groups=mesh['kv'=4,'tp'=8] {'kv'}, use_global_device_ids=true, to_apply=%region_2.0 | all-reduce | flops 18720 | bytes 74880 | tf_op jit(solution)/shard_map/psum | solution.py:88
  46.0 4.6 %all-to-all-start.1 = ((bf16[8,2,1024]{2,1,0:T(2,128)(2,1)}), bf16[8,2,1024]{2,1,0:T(2,128)(2,1)S(1)}, u32[]{:S(2)}, u32[]{:S(2)}) async-start(bf16[8,2,1024]{2,1,0:T(2,128)(2,1)} %reshape.73), calls=%async_computation.1 | async-start | bytes 65536 | tf_op jit(solution)/shard_map/all_to_all | solution.py:109
  50.7 2.7 convolution_convert_fusion.7
  53.7 42.1 %all-reduce.10.cloned.1.call-done = bf16[32,1024]{1,0:T(8,128)(2,1)} async-done(((bf16[32,1024]{1,0:T(8,128)(2,1)}), bf16[32,1024]{1,0:T(8,128)(2,1)}) %all-reduce.10.cloned.1.call-update) | async-done | bytes 65552 | tf_op jit(solution)/shard_map/psum | solution.py:68
  95.8 1.8 fusion.1
  98.4 4.6 %all-to-all-start = ((bf16[32,8,512]{2,1,0:T(8,128)(2,1)}), bf16[32,8,512]{2,1,0:T(8,128)(2,1)S(1)}, u32[]{:S(2)}, u32[]{:S(2)}) async-start(bf16[32,8,512]{2,1,0:T(8,128)(2,1)} %copy.35), calls=%async_computation | async-start | bytes 524288 | tf_op jit(solution)/shard_map/all_to_all | solution.py:108
  103.5 9.3 %all-to-all-done = bf16[32,8,512]{2,1,0:T(8,128)(2,1)S(1)} async-done(((bf16[32,8,512]{2,1,0:T(8,128)(2,1)}), bf16[32,8,512]{2,1,0:T(8,128)(2,1)S(1)}, u32[]{:S(2)}, u32[]{:S(2)}) %all-to-all-start) | async-done | bytes 262176 | tf_op jit(solution)/shard_map/all_to_all | solution.py:108
  112.7 2.3 fusion.10
  116.5 8.9 %pmax.7 = f32[4,64]{1,0:T(4,128)S(1)} all-reduce(f32[4,64]{1,0:T(4,128)S(1)} %fusion.39), channel_id=1, replica_groups=mesh['kv'=4,'tp'=8] {'kv'}, use_global_device_ids=true, to_apply=%region_8.0 | all-reduce | flops 256 | bytes 2048 | tf_op jit(solution)/shard_map/pmax | solution.py:120
  125.5 2.8 convolution_convert_fusion.2
  128.6 8.9 %psum.83 = f32[4,64]{1,0:T(4,128)S(1)} all-reduce(f32[4,64]{1,0:T(4,128)S(1)} %fusion.5), channel_id=1, replica_groups=mesh['kv'=4,'tp'=8] {'kv'}, use_global_device_ids=true, to_apply=%region_11.0 | all-reduce | flops 256 | bytes 2048 | tf_op jit(solution)/shard_map/psum | solution.py:123
  137.5 32.0 %all-reduce.12.cloned.1.call-done = bf16[4,64,512]{2,1,0:T(8,128)(2,1)} async-done(((bf16[4,64,512]{2,1,0:T(8,128)(2,1)}), bf16[4,64,512]{2,1,0:T(8,128)(2,1)}) %all-reduce.12.cloned.1.call-update) | async-done | bytes 262160 | tf_op jit(solution)/shard_map/psum | solution.py:128
  170.9 14.1 %all_to_all.54 = bf16[4,64,512]{2,0,1:T(4,128)(2,1)S(1)} all-to-all(bf16[4,64,512]{2,0,1:T(4,128)(2,1)S(1)} %copy.38), channel_id=1, replica_groups=mesh['kv'=4,'tp'=8] {'tp'}, dimensions={1} | all-to-all | bytes 524288 | tf_op jit(solution)/shard_map/all_to_all | solution.py:132
  186.7 2.7 convolution_convert_fusion.6
  191.4 50.8 %all-reduce.14.cloned.1.call-done = bf16[32,1024]{1,0:T(8,128)(2,1)} async-done(((bf16[32,1024]{1,0:T(8,128)(2,1)}), bf16[32,1024]{1,0:T(8,128)(2,1)}) %all-reduce.14.cloned.1.call-update) | async-done | bytes 65552
  243.8 9.8 %psum.84 = f32[4]{0:T(128)S(1)} all-reduce(f32[4]{0:T(128)S(1)} %fusion.28), channel_id=1, replica_groups=mesh['kv'=4,'tp'=8] {'kv'}, use_global_device_ids=true, to_apply=%region_14.0 | all-reduce | flops 4 | bytes 32 | tf_op jit(solution)/shard_map/psum | solution.py:143
  254.4 14.0 %all-gather.1 = bf16[8,4,1024]{2,1,0:T(4,128)(2,1)S(1)} all-gather(bf16[1,4,1024]{2,1,0:T(4,128)(2,1)S(1)} %bitcast.68), channel_id=1, replica_groups=mesh['kv'=4,'tp'=8] {'tp'}, dimensions={0}, use_global_device_ids=true | all-gather | bytes 73728 | tf_op jit(solution)/shard_map/all_gather | solution.py:146
  268.5 1.6 convolution_convert_fusion.1
  270.2 1.6 convolution_convert_fusion
  271.8 8.0 %psum.86 = bf16[32]{0:T(256)(128)(2,1)S(1)} all-reduce(bf16[32]{0:T(256)(128)(2,1)S(1)} %multiply_reduce_fusion), channel_id=1, replica_groups=mesh['kv'=4,'tp'=8] {'kv'}, use_global_device_ids=true, to_apply=%region_17.0 | all-reduce | flops 32 | bytes 128 | tf_op jit(solution)/shard_map/psum | solution.py:155
  279.8 40.7 %all-reduce.18.cloned.1.call-done = (bf16[32,1376]{1,0:T(8,128)(2,1)}, bf16[32,1376]{1,0:T(8,128)(2,1)}) async-done(((bf16[32,1376]{1,0:T(8,128)(2,1)}, bf16[32,1376]{1,0:T(8,128)(2,1)}), (bf16[32,1376]{1,0:T(8,128)(2,1)}, bf16[32,1376]{1,0:T(8,128)(2,1)})) %all-reduce.18.cloned.1.call-update) | async-done | bytes 176144 | tf_op jit(solution)/shard_map/psum | solution.py:154
  320.5 3.2 convolution_convert_fusion.5
  324.4 54.3 %all-reduce.16.cloned.1.call-done = bf16[32,1024]{1,0:T(8,128)(2,1)} async-done(((bf16[32,1024]{1,0:T(8,128)(2,1)}), bf16[32,1024]{1,0:T(8,128)(2,1)}) %all-reduce.16.cloned.1.call-update) | async-done | bytes 65552
  (68 shorter events, 18.4 us)
Async XLA Ops:
  7.2 261.3 %copy-start = (bf16[1024,1376]{0,1:T(8,128)(2,1)S(1)}, bf16[1024,1376]{0,1:T(8,128)(2,1)}, u32[]{:S(2)}) copy-start(bf16[1024,1376]{0,1:T(8,128)(2,1)} %param.29) | copy-start | bytes 8454148
  46.0 52.5 %all-to-all-start.1 = ((bf16[8,2,1024]{2,1,0:T(2,128)(2,1)}), bf16[8,2,1024]{2,1,0:T(2,128)(2,1)S(1)}, u32[]{:S(2)}, u32[]{:S(2)}) async-start(bf16[8,2,1024]{2,1,0:T(2,128)(2,1)} %reshape.73), calls=%async_computation.1 | async-start | bytes 65536 | tf_op jit(solution)/shard_map/all_to_all | solution.py:109
  50.6 52.6 %copy-start.4 = (bf16[512]{0:T(512)(128)(2,1)S(1)}, bf16[512]{0:T(512)(128)(2,1)}, u32[]{:S(2)}) copy-start(bf16[512]{0:T(512)(128)(2,1)} %param.23) | copy-start | bytes 3076
  50.6 45.2 %all-reduce.10.cloned.1.call-start = ((), (), s32[]{:S(2)}) async-start(), calls=%async_computation.3 | async-start | bytes 131072 | tf_op jit(solution)/shard_map/psum | solution.py:68
  98.4 14.3 %all-to-all-start = ((bf16[32,8,512]{2,1,0:T(8,128)(2,1)}), bf16[32,8,512]{2,1,0:T(8,128)(2,1)S(1)}, u32[]{:S(2)}, u32[]{:S(2)}) async-start(bf16[32,8,512]{2,1,0:T(8,128)(2,1)} %copy.35), calls=%async_computation | async-start | bytes 524288 | tf_op jit(solution)/shard_map/all_to_all | solution.py:108
  103.0 66.5 %all-reduce.12.cloned.1.call-start = ((), (), s32[]{:S(2)}) async-start(), calls=%async_computation.4 | async-start | bytes 524288 | tf_op jit(solution)/shard_map/psum | solution.py:128
  103.2 13.3 %copy-start.3 = (bf16[4,512]{1,0:T(4,128)(2,1)}, bf16[4,512]{1,0:T(4,128)(2,1)S(1)}, u32[]{:S(2)}) copy-start(bf16[4,512]{1,0:T(4,128)(2,1)S(1)} %get-tuple-element.10) | copy-start | bytes 12292
  128.3 113.9 %all-reduce.14.cloned.1.call-start = ((), (), s32[]{:S(2)}) async-start(), calls=%async_computation.5 | async-start | bytes 131072
  185.1 5.1 %copy-start.5 = (u32[32]{0:T(128)S(1)}, u32[32]{0:T(128)}, u32[]{:S(2)}) copy-start(u32[32]{0:T(128)} %constant.53) | copy-start | bytes 388
  185.1 68.5 %copy-start.2 = (bf16[4,1024]{1,0:T(4,128)(2,1)S(1)}, bf16[4,1024]{1,0:T(4,128)(2,1)}, u32[]{:S(2)}) copy-start(bf16[4,1024]{1,0:T(4,128)(2,1)} %param.17) | copy-start | bytes 24580
  189.4 131.1 %all-reduce.18.cloned.1.call-start = ((), (), s32[]{:S(2)}) async-start(), calls=%async_computation.7 | async-start | bytes 360448 | tf_op jit(solution)/shard_map/psum | solution.py:154
  268.4 1.8 copy-start.1
  279.7 98.9 %all-reduce.16.cloned.1.call-start = ((), (), s32[]{:S(2)}) async-start(), calls=%async_computation.6 | async-start | bytes 131072
Sparse Core Ops, SparseCore 0:
  54.3 41.4 all-reduce.9
  128.4 41.0 all-reduce.11
  189.5 52.6 all-reduce.13
  279.9 40.6 all-reduce.17
  323.9 54.7 all-reduce.15
where the time goes:
time: 388 us; the launch traced here: 386 us
  waiting for transfers between devices  229 us (59%)
  blocking collectives  96.5 us (25%)
  matrix products  25.8 us (7%)
  between operations  14.6 us (4%)
  starting transfers between devices  9.46 us (2%)
  other arithmetic  8.04 us (2%)
    unnamed x7, waiting for transfers between devices  105 us
    psum x1, waiting for transfers between devices, body(): lax.psum(jnp.dot(normed_a, w_query_nope, preferred_element_type=jnp.float...  42.1 us
    psum x1, waiting for transfers between devices, body(): lax.psum(up_part.astype(jnp.bfloat16), 'kv').astype(jnp.float32)  40.7 us
    psum x1, waiting for transfers between devices, body(): lax.psum(partial_value.astype(jnp.bfloat16), 'kv').astype(jnp.float32)  32 us
    psum x1, blocking collectives, body(): lax.psum(jnp.sum(gathered_float * gathered_float, axis=1).astype(jnp.bflo...  16.7 us
    all_gather x1, blocking collectives, body(): gathered = lax.all_gather(resid, 'tp', axis=0, tiled=True)  16 us
    all_to_all x1, blocking collectives, body(): lax.all_to_all(o_lat, 'tp', split_axis=1, concat_axis=0, tiled=True)  14.1 us
    all_gather x1, blocking collectives, body(): mid_rows = lax.all_gather(resid_mid, 'tp', axis=0, tiled=True)  14 us
  transfers between devices with their start and end apart: 7, of which 6 were waited for; matrix products, arithmetic and copies ran while one was open for 2% of the time, Pallas kernels for 0%

commit v1 on v0

v1 whole, which is shorter than its diff:
```python
import functools

import jax
import jax.numpy as jnp
import numpy as np
from jax import lax
from jax.experimental import pallas as pl
from jax.experimental.pallas import tpu as pltpu
from jax.sharding import PartitionSpec as P

EPS = 1e-06
THETA = 10000.0
BF = jnp.bfloat16
F32 = jnp.float32


def rotate(vector, position):
    half_width = vector.shape[-1] // 2
    frequency = THETA ** (-jnp.arange(half_width, dtype=F32) / half_width)
    angles = jnp.asarray(position, F32) * frequency
    cos_table, sin_table = (jnp.cos(angles), jnp.sin(angles))
    lower_half, upper_half = (vector[..., :half_width], vector[..., half_width:])
    return jnp.concatenate(
        [
            lower_half * cos_table - upper_half * sin_table,
            lower_half * sin_table + upper_half * cos_table,
        ],
        axis=-1,
    )


def dot(a, b):
    return jnp.dot(a, b, preferred_element_type=F32)


def pieces(value, count):
    out, rest = [], value
    for _ in range(count):
        term = lax.reduce_precision(rest, 8, 7)
        out.append(term.astype(BF))
        rest = rest - term
    return out


def spread(block, axis, groups=None):
    count = len(groups[0]) if groups else lax.axis_size(axis)
    copies = jnp.broadcast_to(block[None], (count,) + block.shape)
    return lax.all_to_all(copies, axis, 0, 0, tiled=True, axis_index_groups=groups)


def plain_body(
    resid,
    attn_gain,
    w_query_nope,
    w_query_rope,
    w_latent,
    w_key_rope,
    latent_gain,
    key_up,
    value_up,
    w_out,
    post_gain,
    mlp_gain,
    w_gate,
    w_up,
    w_down,
    cache_latent,
    cache_rope_key,
):
    nk = lax.axis_size("kv")
    nt = lax.axis_size("tp")
    kv_index = lax.axis_index("kv")
    tp_index = lax.axis_index("tp")
    own, width = resid.shape
    rows = own * nt
    model_width = width * nk
    latent, heads, nope = key_up.shape
    value_width = value_up.shape[2]
    rope = cache_rope_key.shape[2]
    pos_dev = cache_latent.shape[1]
    context = pos_dev * nk
    score_scale = (nope + rope) ** (-0.5)
    col_start = kv_index * width
    split_rows = own % nk == 0

    def block_of(vector):
        return lax.dynamic_slice_in_dim(vector, col_start, width, 0).astype(F32)[None, :]

    gathered = spread(resid, "tp").swapaxes(0, 1).reshape(rows, width)
    gathered_float = gathered.astype(F32)
    gain_a = block_of(attn_gain)
    normed_a = (gathered_float * gain_a).astype(BF)
    own_normed = (resid.astype(F32) * gain_a).astype(BF)
    key_rows = lax.dynamic_slice_in_dim(w_key_rope, col_start, width, 0)
    squares = jnp.sum(gathered_float * gathered_float, axis=1, keepdims=True)
    own_squares = jnp.sum(resid.astype(F32) ** 2, axis=1, keepdims=True)
    q_part = jnp.concatenate(
        [
            dot(normed_a, w_query_nope).astype(BF),
            dot(normed_a, w_query_rope).astype(BF),
            *pieces(squares, 2),
            jnp.zeros((rows, 126), BF),
        ],
        axis=1,
    )
    own_part = jnp.concatenate(
        [
            dot(own_normed, w_latent).astype(BF),
            dot(own_normed, key_rows).astype(BF),
            *pieces(own_squares, 2),
        ],
        axis=1,
    )
    nope_dev, rope_dev = heads * nope, heads * rope
    q_width, own_width = q_part.shape[1], own_part.shape[1]
    sent_width = max(q_width, own_width)
    q_part = jnp.pad(q_part, ((0, 0), (0, sent_width - q_width)))
    own_part = jnp.pad(own_part, ((0, 0), (0, sent_width - own_width)))
    summed = jnp.sum(
        spread(jnp.concatenate([q_part, own_part], axis=0), "kv").astype(F32), axis=0
    )
    q_sum, own_sum = summed[:rows], summed[rows:, :own_width]
    square_sum = jnp.sum(q_sum[:, nope_dev + rope_dev :], axis=1, keepdims=True)
    scale_in = lax.rsqrt(square_sum / model_width + EPS)
    q_nope = (q_sum[:, :nope_dev] * scale_in).astype(BF).reshape(rows, heads, nope)
    q_rope = rotate(
        (q_sum[:, nope_dev : nope_dev + rope_dev] * scale_in).reshape(rows, heads, rope), context
    ).astype(BF)
    latent_sum = own_sum[:, :latent]
    own_scale = lax.rsqrt(
        jnp.sum(own_sum[:, latent + rope :], axis=1, keepdims=True) / model_width + EPS
    )
    new_latent = (
        latent_sum
        * lax.rsqrt(jnp.mean(latent_sum * latent_sum, axis=1, keepdims=True) + EPS)
        * latent_gain.astype(F32)[None, :]
    ).astype(BF)
    new_rope_key = rotate(own_sum[:, latent : latent + rope] * own_scale, context).astype(BF)
    q_lat = jnp.einsum("bhd,chd->bhc", q_nope, key_up, preferred_element_type=F32).astype(BF)

    query = jnp.concatenate([q_lat, q_rope], axis=-1).reshape(own, nt, heads, latent + rope)
    query = lax.all_to_all(query.swapaxes(0, 1), "tp", 0, 0, tiled=True)
    query = query.transpose(1, 0, 2, 3).reshape(own, nt * heads, latent + rope)
    all_heads = nt * heads
    seq_lat, seq_rope = query[..., :latent], query[..., latent:]
    scores = (
        jnp.einsum("bhc,bpc->bhp", seq_lat, cache_latent, preferred_element_type=F32)
        + jnp.einsum("bhr,bpr->bhp", seq_rope, cache_rope_key, preferred_element_type=F32)
    ) * score_scale
    own_score = (
        jnp.einsum("bhc,bc->bh", seq_lat, new_latent, preferred_element_type=F32)
        + jnp.einsum("bhr,br->bh", seq_rope, new_rope_key, preferred_element_type=F32)
    ) * score_scale
    peak = jnp.maximum(jnp.max(scores, axis=2), own_score)
    probs = jnp.exp(scores - peak[:, :, None])
    own_prob = jnp.where(kv_index == 0, jnp.exp(own_score - peak), 0.0)
    totals = jnp.sum(probs, axis=2) + own_prob
    partial_value = (
        jnp.einsum("bhp,bpc->bhc", probs.astype(BF), cache_latent, preferred_element_type=F32)
        + own_prob[:, :, None] * new_latent.astype(F32)[:, None, :]
    )
    packed = jnp.concatenate(
        [partial_value.astype(BF)]
        + [p[:, :, None] for p in pieces(peak, 3) + pieces(totals, 3)]
        + [jnp.zeros((own, all_heads, 122), BF)],
        axis=2,
    )

    def combine(blocks):
        stats = blocks[..., latent:].astype(F32)
        peaks = jnp.sum(stats[..., :3], axis=-1, keepdims=True)
        sums = jnp.sum(stats[..., 3:6], axis=-1, keepdims=True)
        factor = jnp.exp(peaks - jnp.max(peaks, axis=0, keepdims=True))
        value = jnp.sum(blocks[..., :latent].astype(F32) * factor, axis=0)
        return (value / jnp.sum(sums * factor, axis=0)).astype(BF)

    if split_rows:
        per = own // nk
        sent = packed.reshape(nk, per, nt, heads, latent + 128).swapaxes(1, 2)
        sent = sent.reshape(nk * nt, per, heads, latent + 128)
        got = lax.all_to_all(sent, ("kv", "tp"), 0, 0, tiled=True)
        got = got.reshape(nk, nt, per, heads, latent + 128)
        o_lat = combine(got).swapaxes(0, 1).reshape(per * nt, heads, latent)
    else:
        flat = own * all_heads // nk
        got = lax.all_to_all(packed.reshape(nk, flat, latent + 128), "kv", 0, 0, tiled=True)
        o_own = spread(combine(got), "kv").reshape(own, nt, heads, latent)
        o_lat = lax.all_to_all(o_own.swapaxes(0, 1), "tp", 0, 0, tiled=True)
        o_lat = o_lat.swapaxes(0, 1).reshape(rows, heads, latent)
    o_heads = jnp.einsum("bhc,che->bhe", o_lat, value_up, preferred_element_type=F32).astype(BF)
    o_flat = o_heads.reshape(-1, heads * value_width)
    if split_rows:
        o_flat = spread(o_flat, "kv").reshape(rows, heads * value_width)

    core = lax.rem(tp_index, 2)
    swap = [(i, i ^ 1) for i in range(nt)]
    column = [list(range(c, nt, 2)) for c in range(2)]
    half = width // 2
    out_part = dot(o_flat, w_out).reshape(rows, 2, half)
    keep = jnp.where(core == 0, out_part[:, 0], out_part[:, 1])
    give = jnp.where(core == 0, out_part[:, 1], out_part[:, 0]).astype(BF)
    pair_sum = (keep + lax.ppermute(give, "tp", swap).astype(F32)).astype(BF)
    att_half = jnp.sum(spread(pair_sum, "tp", column).astype(F32), axis=0).astype(BF)
    att_other = lax.ppermute(att_half, "tp", swap)
    attended = jnp.where(
        core == 0,
        jnp.concatenate([att_half, att_other], axis=1),
        jnp.concatenate([att_other, att_half], axis=1),
    ).astype(F32)

    gain_m = block_of(mlp_gain)
    post = attended * block_of(post_gain)
    stacked = jnp.concatenate(
        [(gathered_float * gain_m).astype(BF), (post * gain_m).astype(BF)], axis=0
    )
    ff_dev = w_gate.shape[1]
    stats = [
        jnp.sum(a * b, axis=1, keepdims=True)
        for a, b in (
            (attended, attended),
            (gathered_float, gathered_float),
            (gathered_float, post),
            (post, post),
        )
    ]
    stat_block = jnp.concatenate(
        [jnp.concatenate(pieces(jnp.concatenate(stats[2 * i : 2 * i + 2], axis=0), 2), axis=1)
         for i in range(2)],
        axis=1,
    )
    ff_part = jnp.concatenate(
        [
            dot(stacked, w_gate).astype(BF),
            dot(stacked, w_up).astype(BF),
            stat_block,
        ],
        axis=1,
    )
    ff_sum = jnp.sum(spread(ff_part, "kv").astype(F32), axis=0)
    first = jnp.sum(ff_sum[:, 2 * ff_dev : 2 * ff_dev + 2], axis=1, keepdims=True)
    second = jnp.sum(ff_sum[:, 2 * ff_dev + 2 :], axis=1, keepdims=True)
    att_square, resid_square, cross, post_square = (
        first[:rows],
        first[rows:],
        second[:rows],
        second[rows:],
    )
    s = lax.rsqrt(att_square / model_width + EPS)
    mid_square = resid_square + 2.0 * s * cross + s * s * post_square
    scale_mid = lax.rsqrt(jnp.maximum(mid_square, 0.0) / model_width + EPS)
    mixed = (ff_sum[:rows] + s * ff_sum[rows:]) * scale_mid
    hidden = (jax.nn.silu(mixed[:, :ff_dev]) * mixed[:, ff_dev : 2 * ff_dev]).astype(BF)
    down = dot(hidden, w_down).astype(BF).reshape(own, nt, width).swapaxes(0, 1)
    lowered = jnp.sum(lax.all_to_all(down, "tp", 0, 0, tiled=True).astype(F32), axis=0)

    own_post = lax.dynamic_slice_in_dim(post.reshape(own, nt, width), tp_index, 1, 1)[:, 0]
    own_s = lax.dynamic_slice_in_dim(s.reshape(own, nt, 1), tp_index, 1, 1)[:, 0]
    resid_mid = (resid.astype(F32) + own_s * own_post).astype(BF).astype(F32)
    next_resid = (resid_mid + lowered).astype(BF)
    return (next_resid, new_latent, new_rope_key)


VMEM = pl.BlockSpec(memory_space=pltpu.VMEM)
NT = (((1,), (1,)), ((), ()))


def call(kernel, outs, *args, flops=0):
    many = isinstance(outs, (list, tuple))
    sizes = list(args) + (list(outs) if many else [outs])
    moved = sum(int(np.prod(a.shape)) * a.dtype.itemsize for a in sizes)
    return pl.pallas_call(
        kernel,
        out_shape=outs,
        in_specs=[VMEM] * len(args),
        out_specs=[VMEM] * len(outs) if many else VMEM,
        compiler_params=pltpu.CompilerParams(vmem_limit_bytes=16 << 20),
        cost_estimate=pl.CostEstimate(
            flops=max(flops, moved), bytes_accessed=moved, transcendentals=0
        ),
    )(*args)


def like(shape, dtype=BF):
    return jax.ShapeDtypeStruct(shape, dtype)


def lane_of(shape):
    return lax.broadcasted_iota(jnp.int32, shape, len(shape) - 1)


def terms(value, count):
    out, rest = [], value
    for _ in range(count):
        term = rest.astype(BF).astype(F32)
        out.append(term)
        rest = rest - term
    return out


def placed(columns, shape):
    lane = lane_of(shape)
    block = jnp.zeros(shape, F32)
    for at, column in columns:
        block = jnp.where(lane == at, column, block)
    return block


def picked(block, first, count):
    lane = lane_of(block.shape)
    inside = (lane >= first) & (lane < first + count)
    return jnp.sum(jnp.where(inside, block, 0.0), axis=-1, keepdims=True)


def turned(vector, table, half):
    width = vector.shape[1]
    low = lax.rem(lane_of(vector.shape), 2 * half) < half
    other = jnp.where(
        low, pltpu.roll(vector, width - half, 1), pltpu.roll(vector, half, 1)
    )
    return vector * table[0:1, :width] + other * table[1:2, :width]


def start_kernel(resid_ref, ga_ref, gp_ref, gm_ref, msg_ref, gains_ref):
    width = resid_ref.shape[1]
    tiles = width // 128
    at = pl.multiple_of(lax.axis_index("kv") * tiles, tiles)
    for i in range(msg_ref.shape[0]):
        msg_ref[i] = resid_ref[...]
    rows = []
    for ref in (ga_ref, gp_ref, gm_ref):
        block = ref[pl.ds(at, tiles), :].astype(F32)
        rows.append(jnp.concatenate([block[i : i + 1] for i in range(tiles)], axis=1))
    rows.append(jnp.zeros((8 - len(rows), width), F32))
    gains_ref[...] = jnp.concatenate(rows, axis=0)


def query_kernel(
    got_ref, resid_ref, gains_ref, wn_ref, wr_ref, wl_ref, wk_ref, msg_ref, rows_ref
):
    nt, own, width = got_ref.shape
    latent = wl_ref.shape[1]
    rope = wk_ref.shape[0]
    nope_dev, rope_dev = wn_ref.shape[1], wr_ref.shape[1]
    got = got_ref[...].astype(F32)
    x = jnp.concatenate([got[:, r, :] for r in range(own)], axis=0)
    rows_ref[...] = x.astype(BF)
    gain = gains_ref[0:1, :]
    normed = (x * gain).astype(BF)
    qn = jnp.dot(normed, wn_ref[...], preferred_element_type=F32)
    qr = jnp.dot(normed, wr_ref[...], preferred_element_type=F32)
    square = jnp.sum(x * x, axis=1, keepdims=True)
    mine = jnp.concatenate([resid_ref[...].astype(F32), jnp.zeros((nt - own, width), F32)], axis=0)
    own_square = jnp.sum(mine * mine, axis=1, keepdims=True)
    own_normed = (mine * gain).astype(BF)
    lat = jnp.dot(own_normed, wl_ref[...], preferred_element_type=F32)
    at = pl.multiple_of(lax.axis_index("kv") * width, width)
    key = lax.dot_general(own_normed, wk_ref[:, pl.ds(at, width)], NT, preferred_element_type=F32)
    half = latent // 2
    lat = lat[:, :half] + pltpu.roll(lat[:, half:], own, 0)
    key = jnp.concatenate([key, jnp.zeros((nt, 128 - rope), F32)], axis=1)
    own_terms = terms(own_square, 2)
    for r in range(msg_ref.shape[0]):
        part = slice(r * nt, (r + 1) * nt)
        msg_ref[r, :, :nope_dev] = qn[part].astype(BF)
        msg_ref[r, :, nope_dev : nope_dev + rope_dev] = qr[part].astype(BF)
        base = nope_dev + rope_dev
        msg_ref[r, :, base : base + half] = lat.astype(BF)
        columns = [(rope + i, c) for i, c in enumerate(own_terms + terms(square[part], 2))]
        stat = placed(columns, key.shape)
        msg_ref[r, :, base + half :] = jnp.where(lane_of(key.shape) < rope, key, stat).astype(BF)


def latent_kernel(
    model_width, heads, got_ref, ku_ref, gain_ref, table_ref, msg_ref, lat_ref, key_ref
):
    nk, nt, _ = got_ref.shape
    latent, nope_dev = ku_ref.shape
    own, rope = key_ref.shape
    rope_dev = heads * rope
    total = got_ref[0].astype(F32)
    for j in range(1, nk):
        total = total + got_ref[j].astype(F32)
    base, half = nope_dev + rope_dev, latent // 2
    stat = total[:, base + half :]
    scale = lax.rsqrt(picked(stat, rope + 2, 2) / model_width + EPS)
    own_scale = lax.rsqrt(picked(stat, rope, 2) / model_width + EPS)
    lat = total[:, base : base + half]
    lat = jnp.concatenate([lat, pltpu.roll(lat, own, 0)], axis=1)
    lat = lat * lax.rsqrt(jnp.mean(lat * lat, axis=1, keepdims=True) + EPS)
    lat_ref[...] = (lat * gain_ref[...].astype(F32))[:own].astype(BF)
    table = table_ref[...]
    key_ref[...] = turned(stat * own_scale, table, rope // 2)[:own, :rope].astype(BF)
    qn = (total[:, :nope_dev] * scale).astype(BF).astype(F32)
    qr = turned(total[:, nope_dev:base] * scale, table, rope // 2).astype(BF).astype(F32)

    def diagonal(q, size):
        shape = (nt, heads, heads * size)
        head = lax.broadcasted_iota(jnp.int32, shape, 1)
        lane = lax.broadcasted_iota(jnp.int32, shape, 2)
        keep = (lane >= head * size) & (lane < (head + 1) * size)
        spread_q = jnp.broadcast_to(q[:, None, :], shape)
        return jnp.where(keep, spread_q, 0.0).reshape(nt * heads, heads * size).astype(BF)

    q_lat = lax.dot_general(
        diagonal(qn, nope_dev // heads), ku_ref[...], NT, preferred_element_type=F32
    ).astype(BF)
    shape = (rope_dev, 128)
    row = lax.rem(lax.broadcasted_iota(jnp.int32, shape, 0), rope)
    unit = jnp.where(row == lane_of(shape), 1.0, 0.0).astype(BF)
    q_rope = jnp.dot(diagonal(qr, rope), unit, preferred_element_type=F32).astype(BF)
    for j in range(nk):
        msg_ref[j, :, :latent] = q_lat
        msg_ref[j, :, latent:] = q_rope


def attend_kernel(score_scale, q_ref, cache_ref, rope_ref, lat_ref, key_ref, msg_ref):
    own, all_heads, _ = q_ref.shape
    latent = cache_ref.shape[2]
    rope = rope_ref.shape[1]
    holds_own = lax.axis_index("kv") == 0
    lat, key = lat_ref[...].astype(F32), key_ref[...].astype(F32)
    for r in range(own):
        q_lat = q_ref[r, :, :latent]
        q_rope = q_ref[r, :, latent : latent + rope]
        keys = cache_ref[r]
        scores = (
            lax.dot_general(q_lat, keys, NT, preferred_element_type=F32)
            + jnp.dot(q_rope, rope_ref[r], preferred_element_type=F32)
        ) * score_scale
        own_score = (
            jnp.sum(q_lat.astype(F32) * lat[r : r + 1], axis=1, keepdims=True)
            + jnp.sum(q_rope.astype(F32) * key[r : r + 1], axis=1, keepdims=True)
        ) * score_scale
        peak = jnp.maximum(jnp.max(scores, axis=1, keepdims=True), own_score)
        probs = jnp.exp(scores - peak)
        own_prob = jnp.where(holds_own, jnp.exp(own_score - peak), 0.0)
        total = jnp.sum(probs, axis=1, keepdims=True) + own_prob
        value = jnp.dot(probs.astype(BF), keys, preferred_element_type=F32)
        msg_ref[r, :, :latent] = (value + own_prob * lat[r : r + 1]).astype(BF)
        columns = list(enumerate(terms(peak, 3) + terms(total, 3)))
        msg_ref[r, :, latent:] = placed(columns, (all_heads, 128)).astype(BF)


def value_kernel(heads, got_ref, vu_ref, msg_ref):
    nk, pairs, _ = got_ref.shape
    latent, value_dev = vu_ref.shape
    nt = pairs // heads
    stats = [got_ref[j, :, latent:].astype(F32) for j in range(nk)]
    peaks = [picked(s, 0, 3) for s in stats]
    peak = functools.reduce(jnp.maximum, peaks)
    factors = [jnp.exp(p - peak) for p in peaks]
    total = sum(picked(s, 3, 3) * f for s, f in zip(stats, factors))
    value = sum(got_ref[j, :, :latent].astype(F32) * f for j, f in enumerate(factors))
    o_lat = (value / total).astype(BF)
    full = jnp.dot(o_lat, vu_ref[...], preferred_element_type=F32)
    size = value_dev // heads
    shape = (nt, heads, value_dev)
    head = lax.broadcasted_iota(jnp.int32, shape, 1)
    lane = lax.broadcasted_iota(jnp.int32, shape, 2)
    keep = (lane >= head * size) & (lane < (head + 1) * size)
    o_heads = jnp.sum(jnp.where(keep, full.reshape(shape), 0.0), axis=1).astype(BF)
    for j in range(nk):
        msg_ref[j] = o_heads


def out_kernel(o_ref, w_ref, keep_ref, give_ref):
    half = keep_ref.shape[1]
    first = lax.rem(lax.axis_index("tp"), 2) == 0
    out = jnp.dot(o_ref[...], w_ref[...], preferred_element_type=F32)
    keep_ref[...] = jnp.where(first, out[:, :half], out[:, half:])
    give_ref[...] = jnp.where(first, out[:, half:], out[:, :half]).astype(BF)


def pair_kernel(keep_ref, got_ref, msg_ref):
    both = (keep_ref[...] + got_ref[...].astype(F32)).astype(BF)
    for i in range(msg_ref.shape[0]):
        msg_ref[i] = both


def column_kernel(got_ref, out_ref):
    total = got_ref[0].astype(F32)
    for i in range(1, got_ref.shape[0]):
        total = total + got_ref[i].astype(F32)
    out_ref[...] = total.astype(BF)


def gate_kernel(half_ref, other_ref, rows_ref, gains_ref, wg_ref, wu_ref, msg_ref, post_ref):
    nk, both, _ = msg_ref.shape
    rows = both // 2
    ff_dev = wg_ref.shape[0]
    chunk = (msg_ref.shape[2] - 128) // 2
    first = lax.rem(lax.axis_index("tp"), 2) == 0
    mine, other = half_ref[...].astype(F32), other_ref[...].astype(F32)
    att = jnp.concatenate(
        [jnp.where(first, mine, other), jnp.where(first, other, mine)], axis=1
    )
    x = rows_ref[...].astype(F32)
    post = att * gains_ref[1:2, :]
    post_ref[...] = post
    gain = gains_ref[2:3, :]
    stacked = jnp.concatenate([x * gain, post * gain], axis=0).astype(BF)

    def added(a, b):
        return jnp.sum(a * b, axis=1, keepdims=True)

    top = terms(added(att, att), 2) + terms(added(x, post), 2)
    low = terms(added(x, x), 2) + terms(added(post, post), 2)
    stat = placed(
        [(i, jnp.concatenate([a, b], axis=0)) for i, (a, b) in enumerate(zip(top, low))],
        (both, 128),
    ).astype(BF)
    for k, w_ref in enumerate((wg_ref, wu_ref)):
        part = lax.dot_general(stacked, w_ref[...], NT, preferred_element_type=F32)
        for j in range(nk):
            lo, hi = j * chunk, min((j + 1) * chunk, ff_dev)
            size = max(hi - lo, 0)
            if size < chunk:
                msg_ref[j, :, k * chunk : (k + 1) * chunk] = jnp.zeros((both, chunk), BF)
            if size > 0:
                msg_ref[j, :, k * chunk : k * chunk + size] = part[:, lo:hi].astype(BF)
    for j in range(nk):
        msg_ref[j, :, 2 * chunk :] = stat


def hidden_kernel(model_width, got_ref, msg_ref, s_ref):
    nk, both, _ = got_ref.shape
    rows, chunk = both // 2, msg_ref.shape[2]
    total = got_ref[0].astype(F32)
    for j in range(1, nk):
        total = total + got_ref[j].astype(F32)
    stat = total[:, 2 * chunk :]
    one, two = picked(stat, 0, 2), picked(stat, 2, 2)
    att_square, x_square, cross, post_square = one[:rows], one[rows:], two[:rows], two[rows:]
    s = lax.rsqrt(att_square / model_width + EPS)
    mid = jnp.maximum(x_square + 2.0 * s * cross + s * s * post_square, 0.0)
    scale = lax.rsqrt(mid / model_width + EPS)
    s_ref[...] = jnp.broadcast_to(s, s_ref.shape)
    mixed = (total[:rows, : 2 * chunk] + s * total[rows:, : 2 * chunk]) * scale
    gate, up = mixed[:, :chunk], mixed[:, chunk:]
    hidden = (gate / (1.0 + jnp.exp(-gate)) * up).astype(BF)
    for j in range(nk):
        msg_ref[j] = hidden


def down_kernel(got_ref, w_ref, msg_ref):
    nk, rows, chunk = got_ref.shape
    ff_dev = w_ref.shape[0]
    nt, own, _ = msg_ref.shape
    total = None
    for j in range(nk):
        lo, hi = j * chunk, min((j + 1) * chunk, ff_dev)
        if hi > lo:
            part = jnp.dot(
                got_ref[j, :, : hi - lo], w_ref[lo:hi, :], preferred_element_type=F32
            )
            total = part if total is None else total + part
    total = total.reshape(own, nt, total.shape[1])
    for t in range(nt):
        msg_ref[t] = total[:, t, :].astype(BF)


def last_kernel(got_ref, resid_ref, post_ref, s_ref, out_ref):
    nt, own, width = got_ref.shape
    total = got_ref[0].astype(F32)
    for t in range(1, nt):
        total = total + got_ref[t].astype(F32)
    added = (post_ref[...] * s_ref[:, 0:1]).reshape(own, nt, width)
    here = lax.broadcasted_iota(jnp.int32, added.shape, 1) == lax.axis_index("tp")
    mine = jnp.sum(jnp.where(here, added, 0.0), axis=1)
    mid = (resid_ref[...].astype(F32) + mine).astype(BF).astype(F32)
    out_ref[...] = (mid + total).astype(BF)


def exchange(message, axis, groups=None):
    return lax.all_to_all(message, axis, 0, 0, tiled=True, axis_index_groups=groups)


def kernel_body(
    resid,
    attn_gain,
    w_query_nope,
    w_query_rope,
    w_latent,
    w_key_rope,
    latent_gain,
    key_up,
    value_up,
    w_out,
    post_gain,
    mlp_gain,
    w_gate,
    w_up,
    w_down,
    cache_latent,
    cache_rope_key,
):
    nk = lax.axis_size("kv")
    nt = lax.axis_size("tp")
    own, width = resid.shape
    rows = own * nt
    model_width = width * nk
    latent, heads, nope = key_up.shape
    rope = cache_rope_key.shape[2]
    nope_dev, rope_dev = heads * nope, heads * rope
    ff_dev = w_gate.shape[1]
    context = cache_latent.shape[1] * nk
    half_rope = rope // 2
    angles = context * THETA ** (-np.arange(half_rope) / half_rope)
    cos, sin = np.cos(angles), np.sin(angles)
    table = np.zeros((8, rope_dev), np.float32)
    table[0] = np.tile(np.concatenate([cos, cos]), heads)
    table[1] = np.tile(np.concatenate([-sin, sin]), heads)

    tiles = [g.reshape(-1, 128) for g in (attn_gain, post_gain, mlp_gain)]
    msg, gains = call(
        start_kernel, [like((nt, own, width)), like((8, width), F32)], resid, *tiles
    )
    got = exchange(msg, "tp")
    msg, x_rows = call(
        query_kernel,
        [like((nk, nt, nope_dev + rope_dev + latent // 2 + 128)), like((rows, width))],
        got,
        resid,
        gains,
        w_query_nope,
        w_query_rope,
        w_latent,
        w_key_rope.T,
        flops=2 * rows * width * (nope_dev + rope_dev + latent),
    )
    got = exchange(msg, "kv")
    msg, new_latent, new_rope_key = call(
        functools.partial(latent_kernel, model_width, heads),
        [like((nk, rows * heads // own, latent + 128)), like((own, latent)), like((own, rope))],
        got,
        key_up.reshape(latent, nope_dev),
        latent_gain.reshape(1, latent),
        jnp.asarray(table),
        flops=2 * nt * heads * nope_dev * latent,
    )
    got = exchange(msg.reshape(nk * nt, heads, latent + 128), ("kv", "tp"))
    msg = call(
        functools.partial(attend_kernel, (nope + rope) ** (-0.5)),
        like((own, nt * heads, latent + 128)),
        got.reshape(own, nt * heads, latent + 128),
        cache_latent,
        cache_rope_key.swapaxes(1, 2),
        new_latent,
        new_rope_key,
        flops=4 * own * nt * heads * latent * cache_latent.shape[1],
    )
    got = exchange(msg.reshape(nk * nt, heads, latent + 128), ("kv", "tp"))
    value_dev = heads * value_up.shape[2]
    msg = call(
        functools.partial(value_kernel, heads),
        like((nk, nt, value_dev)),
        got.reshape(nk, nt * heads, latent + 128),
        value_up.reshape(latent, value_dev),
        flops=2 * nt * heads * latent * value_dev,
    )
    got = exchange(msg, "kv")
    half = width // 2
    keep, give = call(
        out_kernel,
        [like((rows, half), F32), like((rows, half))],
        got.reshape(rows, value_dev),
        w_out,
        flops=2 * rows * value_dev * width,
    )
    swap = [(i, i ^ 1) for i in range(nt)]
    column = [list(range(c, nt, 2)) for c in range(2)]
    got = lax.ppermute(give, "tp", swap)
    msg = call(pair_kernel, like((nt // 2, rows, half)), keep, got)
    got = exchange(msg, "tp", column)
    att_half = call(column_kernel, like((rows, half)), got)
    att_other = lax.ppermute(att_half, "tp", swap)
    chunk = -(-ff_dev // (nk * 128)) * 128
    msg, post = call(
        gate_kernel,
        [like((nk, 2 * rows, 2 * chunk + 128)), like((rows, width), F32)],
        att_half,
        att_other,
        x_rows,
        gains,
        w_gate.T,
        w_up.T,
        flops=8 * rows * width * ff_dev,
    )
    got = exchange(msg, "kv")
    msg, s = call(
        functools.partial(hidden_kernel, model_width),
        [like((nk, rows, chunk)), like((rows, 128), F32)],
        got,
    )
    got = exchange(msg, "kv")
    msg = call(
        down_kernel,
        like((nt, own, width)),
        got,
        w_down,
        flops=2 * rows * ff_dev * width,
    )
    got = exchange(msg, "tp")
    next_resid = call(last_kernel, like((own, width)), got, resid, post, s)
    return (next_resid, new_latent, new_rope_key)


def body(*args):
    resid, key_up, cache = args[0], args[7], args[15]
    nk, nt = lax.axis_size("kv"), lax.axis_size("tp")
    own, width = resid.shape
    latent, heads, nope = key_up.shape
    fits = (
        own == nk
        and nt == 8
        and heads == 8
        and 2 * own == nt
        and width % 1024 == 0
        and latent % 256 == 0
        and nope % 128 == 0
        and cache.shape[1] % 128 == 0
        and args[16].shape[2] == 64
    )
    return kernel_body(*args) if fits else plain_body(*args)


def solution(mesh):
    return jax.shard_map(
        body,
        mesh=mesh,
        in_specs=(
            P("tp", "kv"),
            P(),
            P("kv", "tp"),
            P("kv", "tp"),
            P("kv", None),
            P(),
            P(),
            P(None, "tp", None),
            P(None, "tp", None),
            P("tp", "kv"),
            P(),
            P(),
            P("kv", "tp"),
            P("kv", "tp"),
            P("tp", "kv"),
            P("tp", "kv", None),
            P("tp", "kv", None),
        ),
        out_specs=(P("tp", "kv"), P("tp", None), P("tp", None)),
        check_vma=False,
    )
```

time: 388 us -> 118 us (0.30)
  waiting for transfers between devices: 229 us -> 16.4 us
  blocking collectives: 96.5 us -> 68.9 us
  matrix products: 25.8 us -> 0 us
  between operations: 14.6 us -> 0.79 us
  local copies, waits for them, and re-layouts: 2.91 us -> 14.7 us
  Pallas kernels: 0 us -> 9.19 us
  other arithmetic: 8.04 us -> 0 us
    psum x3 -> x0, waiting for transfers between devices: 115 us -> none  [the longest x1 42.1 us: body(): lax.psum(jnp.dot(normed_a, w_query_nope, preferred_element_type=jnp.float...]
    unnamed x7 -> x0, waiting for transfers between devices: 105 us -> none
    all_to_all x1 -> x7, blocking collectives: 14.1 us -> 68.9 us  [exchange(): lax.all_to_all(message, axis, 0, 0, tiled=True, axis_index_groups=groups)]
    psum x4 -> x0, blocking collectives: 43.4 us -> none  [the longest x1 16.7 us: body(): lax.psum(jnp.sum(gathered_float * gathered_float, axis=1).astype(jnp.bflo...]
    all_gather x2 -> x0, blocking collectives: 30 us -> none  [the longest x1 16 us: body(): gathered = lax.all_gather(resid, 'tp', axis=0, tiled=True)]
    dot_general x15 -> x0, matrix products: 25.8 us -> none  [the longest x1 3.18 us: body(): jnp.dot(hidden, w_down, preferred_element_type=jnp.float32)]
    unnamed x15 -> x48, local copies, waits for them, and re-layouts: 1.5 us -> 14.7 us
    pallas_call x0 -> x12, Pallas kernels: none -> 9.19 us  [call(): pl.pallas_call(kernel, out_shape=outs, in_specs=[VMEM] * len(args), out_s...]
  transfers between devices with their start and end apart: 7 -> 4, of which waited for: 6 -> 4; matrix products, arithmetic and copies ran while one was open for 2% -> 3% of each run, Pallas kernels for 0% -> 0%
where the time goes in v1:
time: 118 us; the launch traced here: 117 us
  blocking collectives  68.9 us (58%)
  waiting for transfers between devices  16.4 us (14%)
  local copies, waits for them, and re-layouts  14.7 us (12%)
  Pallas kernels  9.19 us (8%)
  starting transfers between devices  6.71 us (6%)
    all_to_all x7, blocking collectives, exchange(): lax.all_to_all(message, axis, 0, 0, tiled=True, axis_index_groups=groups)  68.9 us
    unnamed x48, local copies, waits for them, and re-layouts  14.7 us
    all_to_all x2, waiting for transfers between devices, exchange(): lax.all_to_all(message, axis, 0, 0, tiled=True, axis_index_groups=groups)  14 us
    pallas_call x12, Pallas kernels, call(): pl.pallas_call(kernel, out_shape=outs, in_specs=[VMEM] * len(args), out_s...  9.19 us
    all_to_all x2, starting transfers between devices, exchange(): lax.all_to_all(message, axis, 0, 0, tiled=True, axis_index_groups=groups)  6.57 us
  transfers between devices with their start and end apart: 4, of which 4 were waited for; matrix products, arithmetic and copies ran while one was open for 3% of the time, Pallas kernels for 0%

profile of v1, /device:TPU:0, one launch (start us, length us, event | category | flops | bytes accessed | tf_op | source)
XLA Modules:
  0.0 116.7 jit_solution(13934407840442144654)
XLA Ops:
  3.5 12.1 %all_to_all.45.got_ref = bf16[8,4,1024]{2,1,0:T(4,128)(2,1)S(1)} all-to-all(bf16[8,4,1024]{2,1,0:T(4,128)(2,1)S(1)} %get-tuple-element.16), channel_id=1, replica_groups=mesh['kv'=4,'tp'=8] {'tp'}, dimensions={0} | all-to-all | bytes 131072 | tf_op jit(solution)/shard_map/all_to_all | solution.py:575
  15.5 1.6 %copy-done.3 = bf16[1024,1024]{1,0:T(8,128)(2,1)S(1)} copy-done((bf16[1024,1024]{1,0:T(8,128)(2,1)S(1)}, bf16[1024,1024]{1,0:T(8,128)(2,1)}, u32[]{:S(2)}) %copy-start.3) | copy-done | bytes 2097176
  17.1 1.2 %copy-done.6 = bf16[1024,512]{1,0:T(8,128)(2,1)S(1)} copy-done((bf16[1024,512]{1,0:T(8,128)(2,1)S(1)}, bf16[1024,512]{1,0:T(8,128)(2,1)}, u32[]{:S(2)}) %copy-start.6) | copy-done | bytes 1048600
  18.4 1.2 %copy-done.7 = bf16[1024,512]{1,0:T(8,128)(2,1)S(1)} copy-done((bf16[1024,512]{1,0:T(8,128)(2,1)S(1)}, bf16[1024,512]{1,0:T(8,128)(2,1)}, u32[]{:S(2)}) %copy-start.7) | copy-done | bytes 1048600
  19.6 1.0 copy-done.8
  20.6 1.5 %shard_map.194 = (bf16[4,8,1920]{2,1,0:T(8,128)(2,1)}, bf16[32,1024]{1,0:T(8,128)(2,1)S(1)}) custom-call(bf16[8,4,1024]{2,1,0:T(4,128)(2,1)S(1)} %all_to_all.45.got_ref, bf16[4,1024]{1,0:T(4,128)(2,1)S(1)} %copy-done.12, f32[8,1024]{1,0:T(8,128)S(1)} %get-tuple-element.17.gains_ref, bf16[1024,1024]{1,0:T(8,128)(2,1)S(1)} %copy-done.3, ...), custom_call_target="tpu_custom_call" | custom-call | flops 134217728 | bytes 5013504 | tf_op jit(solution)/shard_map/pallas_call | solution.py:271
  22.7 3.8 %all-to-all-start.1 = ((bf16[4,8,1920]{2,1,0:T(8,128)(2,1)}), bf16[4,8,1920]{2,1,0:T(8,128)(2,1)S(1)}, u32[]{:S(2)}, u32[]{:S(2)}) async-start(bf16[4,8,1920]{2,1,0:T(8,128)(2,1)} %get-tuple-element.18), calls=%async_computation.1 | async-start | bytes 245760 | tf_op jit(solution)/shard_map/all_to_all | solution.py:575
  26.6 1.5 %copy.26 = bf16[64,8,8,128]{3,1,2,0:T(8,128)(2,1)S(1)} copy(bf16[64,8,8,128]{3,2,1,0:T(8,128)(2,1)} %bitcast.33) | data formatting | bytes 2097152
  28.1 3.5 %all-to-all-done.1.got_ref = bf16[4,8,1920]{2,1,0:T(8,128)(2,1)S(1)} async-done(((bf16[4,8,1920]{2,1,0:T(8,128)(2,1)}), bf16[4,8,1920]{2,1,0:T(8,128)(2,1)S(1)}, u32[]{:S(2)}, u32[]{:S(2)}) %all-to-all-start.1) | async-done | bytes 122912 | tf_op jit(solution)/shard_map/all_to_all | solution.py:575
  31.6 1.0 shard_map.195
  32.5 13.7 %all_to_all.46 = bf16[32,8,640]{2,1,0:T(8,128)(2,1)S(1)} all-to-all(bf16[32,8,640]{2,1,0:T(8,128)(2,1)S(1)} %bitcast.27), channel_id=1, replica_groups=mesh['kv'=4,'tp'=8] {'kv','tp'}, dimensions={0} | all-to-all | bytes 655360 | tf_op jit(solution)/shard_map/all_to_all | solution.py:575
  47.6 2.6 %shard_map.196 = bf16[4,64,640]{2,1,0:T(8,128)(2,1)} custom-call(bf16[4,64,640]{2,1,0:T(8,128)(2,1)S(1)} %bitcast.25, bf16[4,512,512]{2,1,0:T(8,128)(2,1)S(1)} %copy-done.4, bf16[4,64,512]{2,1,0:T(8,128)(2,1)S(1)} %bitcast.29, bf16[4,512]{1,0:T(4,128)(2,1)S(1)} %copy-done.20, bf16[4,64]{1,0:T(4,128)(2,1)S(1)} %copy-done.21), custom_call_target="tpu_custom_call" | custom-call | flops 268435456 | bytes 3019264 | tf_op jit(solution)/shard_map/pallas_call | solution.py:271
  50.2 2.7 %all-to-all-start.3 = ((bf16[32,8,640]{2,1,0:T(8,128)(2,1)}), bf16[32,8,640]{2,1,0:T(8,128)(2,1)S(1)}, u32[]{:S(2)}, u32[]{:S(2)}) async-start(bf16[32,8,640]{2,1,0:T(8,128)(2,1)} %bitcast.7), calls=%async_computation.3 | async-start | bytes 655360 | tf_op jit(solution)/shard_map/all_to_all | solution.py:575
  52.9 1.5 %copy.25 = bf16[64,8,8,128]{3,1,2,0:T(8,128)(2,1)S(1)} copy(bf16[64,8,8,128]{3,2,1,0:T(8,128)(2,1)} %bitcast.34) | data formatting | bytes 2097152
  54.5 10.5 %all-to-all-done.3 = bf16[32,8,640]{2,1,0:T(8,128)(2,1)S(1)} async-done(((bf16[32,8,640]{2,1,0:T(8,128)(2,1)}), bf16[32,8,640]{2,1,0:T(8,128)(2,1)S(1)}, u32[]{:S(2)}, u32[]{:S(2)}) %all-to-all-start.3) | async-done | bytes 327712 | tf_op jit(solution)/shard_map/all_to_all | solution.py:575
  65.4 7.3 %all_to_all.47 = bf16[4,8,1024]{2,1,0:T(8,128)(2,1)S(1)} all-to-all(bf16[4,8,1024]{2,1,0:T(8,128)(2,1)S(1)} %shard_map.197), channel_id=1, replica_groups=mesh['kv'=4,'tp'=8] {'kv'}, dimensions={0} | all-to-all | bytes 131072 | tf_op jit(solution)/shard_map/all_to_all | solution.py:575
  73.3 1.2 %collective-permute-done.got_ref = bf16[32,512]{1,0:T(8,128)(2,1)S(1)} collective-permute-done((bf16[32,512]{1,0:T(8,128)(2,1)S(1)}, bf16[32,512]{1,0:T(8,128)(2,1)S(1)}, u32[]{:S(2)}, u32[]{:S(2)}) %collective-permute-start) | collective-permute-done | bytes 32800 | tf_op jit(solution)/shard_map/ppermute | solution.py:672
  74.5 8.8 %all_to_all.48.got_ref = bf16[4,32,512]{2,1,0:T(8,128)(2,1)S(1)} all-to-all(bf16[4,32,512]{2,1,0:T(8,128)(2,1)S(1)} %shard_map.199), channel_id=1, replica_groups={{0,2,4,6},{1,3,5,7},{8,10,12,14},{9,11,13,15},{16,18,20,22},{17,19,21,2..., dimensions={0} | all-to-all | bytes 262144 | tf_op jit(solution)/shard_map/all_to_all | solution.py:575
  83.4 1.2 %collective-permute-done.1.other_ref = bf16[32,512]{1,0:T(8,128)(2,1)S(1)} collective-permute-done((bf16[32,512]{1,0:T(8,128)(2,1)S(1)}, bf16[32,512]{1,0:T(8,128)(2,1)S(1)}, u32[]{:S(2)}, u32[]{:S(2)}) %collective-permute-start.1) | collective-permute-done | bytes 32800 | tf_op jit(solution)/shard_map/ppermute | solution.py:676
  84.6 1.8 %copy-done.1 = bf16[1024,1376]{0,1:T(8,128)(2,1)S(1)} copy-done((bf16[1024,1376]{0,1:T(8,128)(2,1)S(1)}, bf16[1024,1376]{0,1:T(8,128)(2,1)}, u32[]{:S(2)}) %copy-start.1) | copy-done | bytes 2818072
  86.4 1.7 %shard_map.201 = (bf16[4,64,896]{2,1,0:T(8,128)(2,1)S(1)}, f32[32,1024]{1,0:T(8,128)S(1)}) custom-call(bf16[32,512]{1,0:T(8,128)(2,1)S(1)} %shard_map.200.half_ref, bf16[32,512]{1,0:T(8,128)(2,1)S(1)} %collective-permute-done.1.other_ref, bf16[32,1024]{1,0:T(8,128)(2,1)S(1)} %copy-done.15, f32[8,1024]{1,0:T(8,128)S(1)} %copy-done.11, ...), custom_call_target="tpu_custom_call" | custom-call | flops 360710144 | bytes 6389760 | tf_op jit(solution)/shard_map/pallas_call | solution.py:271
  88.2 11.0 %all_to_all.49.got_ref = bf16[4,64,896]{2,1,0:T(8,128)(2,1)S(1)} all-to-all(bf16[4,64,896]{2,1,0:T(8,128)(2,1)S(1)} %get-tuple-element.25), channel_id=1, replica_groups=mesh['kv'=4,'tp'=8] {'kv'}, dimensions={0} | all-to-all | bytes 917504 | tf_op jit(solution)/shard_map/all_to_all | solution.py:575
  99.3 7.3 %all_to_all.50.got_ref = bf16[4,32,384]{2,1,0:T(8,128)(2,1)S(1)} all-to-all(bf16[4,32,384]{2,1,0:T(8,128)(2,1)S(1)} %get-tuple-element.26), channel_id=1, replica_groups=mesh['kv'=4,'tp'=8] {'kv'}, dimensions={0} | all-to-all | bytes 196608 | tf_op jit(solution)/shard_map/all_to_all | solution.py:575
  107.3 8.7 %all_to_all.51.got_ref = bf16[8,4,1024]{2,1,0:T(4,128)(2,1)S(1)} all-to-all(bf16[8,4,1024]{2,1,0:T(4,128)(2,1)S(1)} %shard_map.203), channel_id=1, replica_groups=mesh['kv'=4,'tp'=8] {'tp'}, dimensions={0} | all-to-all | bytes 131072 | tf_op jit(solution)/shard_map/all_to_all | solution.py:575
  (52 shorter events, 7.4 us)
Async XLA Ops:
  0.6 25.9 %copy-start.22 = (bf16[512]{0:T(512)(128)(2,1)S(1)}, bf16[512]{0:T(512)(128)(2,1)}, u32[]{:S(2)}) copy-start(bf16[512]{0:T(512)(128)(2,1)} %param.24) | copy-start | bytes 3076
  0.6 0.7 copy-start.12
  1.3 0.7 copy-start.17
  2.0 0.7 copy-start.18
  2.7 0.7 copy-start.19
  3.5 18.6 %copy-start.10 = (f32[8,1024]{1,0:T(8,128)}, f32[8,1024]{1,0:T(8,128)S(1)}, u32[]{:S(2)}) copy-start(f32[8,1024]{1,0:T(8,128)S(1)} %get-tuple-element.17.gains_ref) | copy-start | bytes 98308
  15.5 1.6 %copy-start.3 = (bf16[1024,1024]{1,0:T(8,128)(2,1)S(1)}, bf16[1024,1024]{1,0:T(8,128)(2,1)}, u32[]{:S(2)}) copy-start(bf16[1024,1024]{1,0:T(8,128)(2,1)} %wn_ref.1) | copy-start | bytes 6291460
  17.1 1.2 %copy-start.6 = (bf16[1024,512]{1,0:T(8,128)(2,1)S(1)}, bf16[1024,512]{1,0:T(8,128)(2,1)}, u32[]{:S(2)}) copy-start(bf16[1024,512]{1,0:T(8,128)(2,1)} %wr_ref.1) | copy-start | bytes 3145732
  18.4 1.2 %copy-start.7 = (bf16[1024,512]{1,0:T(8,128)(2,1)S(1)}, bf16[1024,512]{1,0:T(8,128)(2,1)}, u32[]{:S(2)}) copy-start(bf16[1024,512]{1,0:T(8,128)(2,1)} %wl_ref.1) | copy-start | bytes 3145732
  19.6 1.0 copy-start.8
  20.6 10.9 %copy-start.16 = (f32[8,512]{1,0:T(8,128)S(1)}, f32[8,512]{1,0:T(8,128)}, u32[]{:S(2)}) copy-start(f32[8,512]{1,0:T(8,128)} %constant.2.clone.table_ref) | copy-start | bytes 49156
  22.7 23.6 %copy-start.4 = (bf16[4,512,512]{2,1,0:T(8,128)(2,1)S(1)}, bf16[4,512,512]{2,1,0:T(8,128)(2,1)}, u32[]{:S(2)}) copy-start(bf16[4,512,512]{2,1,0:T(8,128)(2,1)} %cache_ref.1) | copy-start | bytes 6291460
  22.7 23.6 %copy-start.9 = (bf16[4,512,64]{1,2,0:T(8,128)(2,1)S(1)}, bf16[4,512,64]{1,2,0:T(8,128)(2,1)}, u32[]{:S(2)}) copy-start(bf16[4,512,64]{1,2,0:T(8,128)(2,1)} %param.34) | copy-start | bytes 786436
  22.7 8.8 %all-to-all-start.1 = ((bf16[4,8,1920]{2,1,0:T(8,128)(2,1)}), bf16[4,8,1920]{2,1,0:T(8,128)(2,1)S(1)}, u32[]{:S(2)}, u32[]{:S(2)}) async-start(bf16[4,8,1920]{2,1,0:T(8,128)(2,1)} %get-tuple-element.18), calls=%async_computation.1 | async-start | bytes 245760 | tf_op jit(solution)/shard_map/all_to_all | solution.py:575
  50.2 22.5 %copy-start.5 = (bf16[1024,1024]{1,0:T(8,128)(2,1)S(1)}, bf16[1024,1024]{1,0:T(8,128)(2,1)}, u32[]{:S(2)}) copy-start(bf16[1024,1024]{1,0:T(8,128)(2,1)} %w_ref.2) | copy-start | bytes 6291460
  50.2 14.7 %all-to-all-start.3 = ((bf16[32,8,640]{2,1,0:T(8,128)(2,1)}), bf16[32,8,640]{2,1,0:T(8,128)(2,1)S(1)}, u32[]{:S(2)}, u32[]{:S(2)}) async-start(bf16[32,8,640]{2,1,0:T(8,128)(2,1)} %bitcast.7), calls=%async_computation.3 | async-start | bytes 655360 | tf_op jit(solution)/shard_map/all_to_all | solution.py:575
  52.9 31.7 %copy-start.11 = (f32[8,1024]{1,0:T(8,128)S(1)}, f32[8,1024]{1,0:T(8,128)}, u32[]{:S(2)}) copy-start(f32[8,1024]{1,0:T(8,128)} %copy-done.10) | copy-start | bytes 98308
  65.0 19.7 %copy-start = (bf16[1024,1376]{0,1:T(8,128)(2,1)S(1)}, bf16[1024,1376]{0,1:T(8,128)(2,1)}, u32[]{:S(2)}) copy-start(bf16[1024,1376]{0,1:T(8,128)(2,1)} %param.30) | copy-start | bytes 8454148
  65.0 19.7 %copy-start.15 = (bf16[32,1024]{1,0:T(8,128)(2,1)S(1)}, bf16[32,1024]{1,0:T(8,128)(2,1)}, u32[]{:S(2)}) copy-start(bf16[32,1024]{1,0:T(8,128)(2,1)} %copy-done.14) | copy-start | bytes 196612
  73.2 1.3 %collective-permute-start = (bf16[32,512]{1,0:T(8,128)(2,1)S(1)}, bf16[32,512]{1,0:T(8,128)(2,1)S(1)}, u32[]{:S(2)}, u32[]{:S(2)}) collective-permute-start(bf16[32,512]{1,0:T(8,128)(2,1)S(1)} %get-tuple-element.23), channel_id=1, source_target_pairs={{0,1},{1,0},{2,3},{3,2},{4,5},{5,4},{6,7},{7,6},{8,9},{9,8},{10,11... | collective-permute-start | bytes 98312 | tf_op jit(solution)/shard_map/ppermute | solution.py:672
  83.3 1.3 %collective-permute-start.1 = (bf16[32,512]{1,0:T(8,128)(2,1)S(1)}, bf16[32,512]{1,0:T(8,128)(2,1)S(1)}, u32[]{:S(2)}, u32[]{:S(2)}) collective-permute-start(bf16[32,512]{1,0:T(8,128)(2,1)S(1)} %shard_map.200.half_ref), channel_id=1, source_target_pairs={{0,1},{1,0},{2,3},{3,2},{4,5},{5,4},{6,7},{7,6},{8,9},{9,8},{10,11... | collective-permute-start | bytes 98312 | tf_op jit(solution)/shard_map/ppermute | solution.py:676
  84.6 1.8 %copy-start.1 = (bf16[1024,1376]{0,1:T(8,128)(2,1)S(1)}, bf16[1024,1376]{0,1:T(8,128)(2,1)}, u32[]{:S(2)}) copy-start(bf16[1024,1376]{0,1:T(8,128)(2,1)} %param.31) | copy-start | bytes 8454148
  86.4 20.2 %copy-start.2 = (bf16[1376,1024]{1,0:T(8,128)(2,1)S(1)}, bf16[1376,1024]{1,0:T(8,128)(2,1)}, u32[]{:S(2)}) copy-start(bf16[1376,1024]{1,0:T(8,128)(2,1)} %w_ref.3) | copy-start | bytes 8454148
  88.2 27.8 %copy-start.13 = (bf16[4,1024]{1,0:T(4,128)(2,1)S(1)}, bf16[4,1024]{1,0:T(4,128)(2,1)}, u32[]{:S(2)}) copy-start(bf16[4,1024]{1,0:T(4,128)(2,1)} %resid_ref.5) | copy-start | bytes 24580
  (3 other events, 2.0 us)

commit v2 on v1

--- a/solution.py
+++ b/solution.py
@@ -261,10 +261,11 @@
 
 
 VMEM = pl.BlockSpec(memory_space=pltpu.VMEM)
+WAIT = 4_000_000_000
 NT = (((1,), (1,)), ((), ()))
 
 
-def call(kernel, outs, *args, flops=0):
+def call(kernel, outs, *args, flops=0, scratch=()):
     many = isinstance(outs, (list, tuple))
     sizes = list(args) + (list(outs) if many else [outs])
     moved = sum(int(np.prod(a.shape)) * a.dtype.itemsize for a in sizes)
@@ -273,6 +274,7 @@
         out_shape=outs,
         in_specs=[VMEM] * len(args),
         out_specs=[VMEM] * len(outs) if many else VMEM,
+        scratch_shapes=list(scratch),
         compiler_params=pltpu.CompilerParams(vmem_limit_bytes=16 << 20),
         cost_estimate=pl.CostEstimate(
             flops=max(flops, moved), bytes_accessed=moved, transcendentals=0
@@ -320,31 +322,48 @@
     return vector * table[0:1, :width] + other * table[1:2, :width]
 
 
-def start_kernel(resid_ref, ga_ref, gp_ref, gm_ref, msg_ref, gains_ref):
-    width = resid_ref.shape[1]
-    tiles = width // 128
-    at = pl.multiple_of(lax.axis_index("kv") * tiles, tiles)
-    for i in range(msg_ref.shape[0]):
-        msg_ref[i] = resid_ref[...]
-    rows = []
-    for ref in (ga_ref, gp_ref, gm_ref):
-        block = ref[pl.ds(at, tiles), :].astype(F32)
-        rows.append(jnp.concatenate([block[i : i + 1] for i in range(tiles)], axis=1))
-    rows.append(jnp.zeros((8 - len(rows), width), F32))
-    gains_ref[...] = jnp.concatenate(rows, axis=0)
+def other(axis, k, step=1):
+    return jnp.bitwise_xor(lax.div(lax.axis_index(axis), step), k)
+
+
+def start_kernel(resid_ref, got_ref, out_ref):
+    first = lax.rem(lax.axis_index("tp"), 2) == 0
+    mine, theirs = resid_ref[...].astype(F32), got_ref[...].astype(F32)
+    out_ref[...] = jnp.concatenate(
+        [jnp.where(first, mine, theirs), jnp.where(first, theirs, mine)], axis=0
+    ).astype(BF)
 
 
 def query_kernel(
-    got_ref, resid_ref, gains_ref, wn_ref, wr_ref, wl_ref, wk_ref, msg_ref, rows_ref
+    b0, b1, b2, b3, resid_ref, ga_ref, gp_ref, gm_ref, wn_ref, wr_ref, wl_ref, wk_ref,
+    m0, m1, m2, m3, rows_ref, gains_ref, held_ref, sent_ref,
 ):
-    nt, own, width = got_ref.shape
+    own, width = resid_ref.shape
+    chips = held_ref.shape[0]
+    nt = 2 * chips
     latent = wl_ref.shape[1]
     rope = wk_ref.shape[0]
     nope_dev, rope_dev = wn_ref.shape[1], wr_ref.shape[1]
-    got = got_ref[...].astype(F32)
-    x = jnp.concatenate([got[:, r, :] for r in range(own)], axis=0)
+    for k, ref in enumerate((b0, b1, b2, b3)):
+        held_ref[other("tp", k, 2)] = ref[...].astype(F32)
+    x = jnp.concatenate(
+        [
+            held_ref[z, c * own + r : c * own + r + 1, :]
+            for r in range(own)
+            for z in range(chips)
+            for c in range(2)
+        ],
+        axis=0,
+    )
     rows_ref[...] = x.astype(BF)
-    gain = gains_ref[0:1, :]
+    tiles = width // 128
+    at = pl.multiple_of(lax.axis_index("kv") * tiles, tiles)
+    gains = []
+    for ref in (ga_ref, gp_ref, gm_ref):
+        block = ref[pl.ds(at, tiles), :].astype(F32)
+        gains.append(jnp.concatenate([block[i : i + 1] for i in range(tiles)], axis=1))
+    gain = gains[0]
+    gains_ref[...] = jnp.concatenate(gains + [jnp.zeros((8 - len(gains), width), F32)], axis=0)
     normed = (x * gain).astype(BF)
     qn = jnp.dot(normed, wn_ref[...], preferred_element_type=F32)
     qr = jnp.dot(normed, wr_ref[...], preferred_element_type=F32)
@@ -359,27 +378,33 @@
     lat = lat[:, :half] + pltpu.roll(lat[:, half:], own, 0)
     key = jnp.concatenate([key, jnp.zeros((nt, 128 - rope), F32)], axis=1)
     own_terms = terms(own_square, 2)
-    for r in range(msg_ref.shape[0]):
+    for r in range(sent_ref.shape[0]):
         part = slice(r * nt, (r + 1) * nt)
-        msg_ref[r, :, :nope_dev] = qn[part].astype(BF)
-        msg_ref[r, :, nope_dev : nope_dev + rope_dev] = qr[part].astype(BF)
+        sent_ref[r, :, :nope_dev] = qn[part].astype(BF)
+        sent_ref[r, :, nope_dev : nope_dev + rope_dev] = qr[part].astype(BF)
         base = nope_dev + rope_dev
-        msg_ref[r, :, base : base + half] = lat.astype(BF)
+        sent_ref[r, :, base : base + half] = lat.astype(BF)
         columns = [(rope + i, c) for i, c in enumerate(own_terms + terms(square[part], 2))]
         stat = placed(columns, key.shape)
-        msg_ref[r, :, base + half :] = jnp.where(lane_of(key.shape) < rope, key, stat).astype(BF)
+        sent_ref[r, :, base + half :] = jnp.where(lane_of(key.shape) < rope, key, stat).astype(BF)
+    for k, ref in enumerate((m0, m1, m2, m3)):
+        ref[...] = sent_ref[other("kv", k)]
+
+
+def four(refs):
+    a, b, c, d = (ref[...].astype(F32) for ref in refs)
+    return (a + b) + (c + d)
 
 
 def latent_kernel(
-    model_width, heads, got_ref, ku_ref, gain_ref, table_ref, msg_ref, lat_ref, key_ref
+    model_width, b0, b1, b2, b3, ku_ref, gain_ref, table_ref, msg_ref, lat_ref, key_ref, own_ref
 ):
-    nk, nt, _ = got_ref.shape
-    latent, nope_dev = ku_ref.shape
+    nk, nt = msg_ref.shape[0], b0.shape[0]
+    latent, heads, nope = ku_ref.shape
+    nope_dev = heads * nope
     own, rope = key_ref.shape
     rope_dev = heads * rope
-    total = got_ref[0].astype(F32)
-    for j in range(1, nk):
-        total = total + got_ref[j].astype(F32)
+    total = four((b0, b1, b2, b3))
     base, half = nope_dev + rope_dev, latent // 2
     stat = total[:, base + half :]
     scale = lax.rsqrt(picked(stat, rope + 2, 2) / model_width + EPS)
@@ -387,9 +412,13 @@
     lat = total[:, base : base + half]
     lat = jnp.concatenate([lat, pltpu.roll(lat, own, 0)], axis=1)
     lat = lat * lax.rsqrt(jnp.mean(lat * lat, axis=1, keepdims=True) + EPS)
-    lat_ref[...] = (lat * gain_ref[...].astype(F32))[:own].astype(BF)
+    lat = (lat * gain_ref[...].astype(F32)).astype(BF)
     table = table_ref[...]
-    key_ref[...] = turned(stat * own_scale, table, rope // 2)[:own, :rope].astype(BF)
+    key = turned(stat * own_scale, table, rope // 2).astype(BF)
+    lat_ref[...] = lat[:own]
+    key_ref[...] = key[:own, :rope]
+    own_ref[:, :latent] = lat.astype(F32)
+    own_ref[:, latent:] = key.astype(F32)
     qn = (total[:, :nope_dev] * scale).astype(BF).astype(F32)
     qr = turned(total[:, nope_dev:base] * scale, table, rope // 2).astype(BF).astype(F32)
 
@@ -402,7 +431,7 @@
         return jnp.where(keep, spread_q, 0.0).reshape(nt * heads, heads * size).astype(BF)
 
     q_lat = lax.dot_general(
-        diagonal(qn, nope_dev // heads), ku_ref[...], NT, preferred_element_type=F32
+        diagonal(qn, nope), ku_ref[...].reshape(latent, nope_dev), NT, preferred_element_type=F32
     ).astype(BF)
     shape = (rope_dev, 128)
     row = lax.rem(lax.broadcasted_iota(jnp.int32, shape, 0), rope)
@@ -413,12 +442,12 @@
         msg_ref[j, :, latent:] = q_rope
 
 
-def attend_kernel(score_scale, q_ref, cache_ref, rope_ref, lat_ref, key_ref, msg_ref):
+def attend_kernel(score_scale, q_ref, cache_ref, rope_ref, own_ref, msg_ref):
     own, all_heads, _ = q_ref.shape
     latent = cache_ref.shape[2]
     rope = rope_ref.shape[1]
     holds_own = lax.axis_index("kv") == 0
-    lat, key = lat_ref[...].astype(F32), key_ref[...].astype(F32)
+    lat, key = own_ref[:, :latent], own_ref[:, latent : latent + rope]
     for r in range(own):
         q_lat = q_ref[r, :, :latent]
         q_rope = q_ref[r, :, latent : latent + rope]
@@ -441,9 +470,10 @@
         msg_ref[r, :, latent:] = placed(columns, (all_heads, 128)).astype(BF)
 
 
-def value_kernel(heads, got_ref, vu_ref, msg_ref):
+def value_kernel(got_ref, vu_ref, out_ref):
     nk, pairs, _ = got_ref.shape
-    latent, value_dev = vu_ref.shape
+    latent, heads, size = vu_ref.shape
+    value_dev = heads * size
     nt = pairs // heads
     stats = [got_ref[j, :, latent:].astype(F32) for j in range(nk)]
     peaks = [picked(s, 0, 3) for s in stats]
@@ -452,47 +482,44 @@
     total = sum(picked(s, 3, 3) * f for s, f in zip(stats, factors))
     value = sum(got_ref[j, :, :latent].astype(F32) * f for j, f in enumerate(factors))
     o_lat = (value / total).astype(BF)
-    full = jnp.dot(o_lat, vu_ref[...], preferred_element_type=F32)
-    size = value_dev // heads
+    full = jnp.dot(o_lat, vu_ref[...].reshape(latent, value_dev), preferred_element_type=F32)
     shape = (nt, heads, value_dev)
     head = lax.broadcasted_iota(jnp.int32, shape, 1)
     lane = lax.broadcasted_iota(jnp.int32, shape, 2)
     keep = (lane >= head * size) & (lane < (head + 1) * size)
-    o_heads = jnp.sum(jnp.where(keep, full.reshape(shape), 0.0), axis=1).astype(BF)
-    for j in range(nk):
-        msg_ref[j] = o_heads
-
-
-def out_kernel(o_ref, w_ref, keep_ref, give_ref):
+    out_ref[...] = jnp.sum(jnp.where(keep, full.reshape(shape), 0.0), axis=1).astype(BF)
+
+
+def out_kernel(b0, b1, b2, b3, w_ref, keep_ref, give_ref, held_ref):
     half = keep_ref.shape[1]
+    for k, ref in enumerate((b0, b1, b2, b3)):
+        held_ref[other("kv", k)] = ref[...].astype(F32)
     first = lax.rem(lax.axis_index("tp"), 2) == 0
-    out = jnp.dot(o_ref[...], w_ref[...], preferred_element_type=F32)
+    o_heads = held_ref[...].reshape(keep_ref.shape[0], w_ref.shape[0]).astype(BF)
+    out = jnp.dot(o_heads, w_ref[...], preferred_element_type=F32)
     keep_ref[...] = jnp.where(first, out[:, :half], out[:, half:])
     give_ref[...] = jnp.where(first, out[:, half:], out[:, :half]).astype(BF)
 
 
-def pair_kernel(keep_ref, got_ref, msg_ref):
-    both = (keep_ref[...] + got_ref[...].astype(F32)).astype(BF)
-    for i in range(msg_ref.shape[0]):
-        msg_ref[i] = both
-
-
-def column_kernel(got_ref, out_ref):
-    total = got_ref[0].astype(F32)
-    for i in range(1, got_ref.shape[0]):
-        total = total + got_ref[i].astype(F32)
-    out_ref[...] = total.astype(BF)
-
-
-def gate_kernel(half_ref, other_ref, rows_ref, gains_ref, wg_ref, wu_ref, msg_ref, post_ref):
+def pair_kernel(keep_ref, got_ref, out_ref):
+    out_ref[...] = (keep_ref[...] + got_ref[...].astype(F32)).astype(BF)
+
+
+def column_kernel(b0, b1, b2, b3, out_ref):
+    out_ref[...] = four((b0, b1, b2, b3)).astype(BF)
+
+
+def gate_kernel(
+    half_ref, other_ref, rows_ref, gains_ref, wg_ref, wu_ref, m0, m1, m2, m3, post_ref, msg_ref
+):
     nk, both, _ = msg_ref.shape
     rows = both // 2
     ff_dev = wg_ref.shape[0]
     chunk = (msg_ref.shape[2] - 128) // 2
     first = lax.rem(lax.axis_index("tp"), 2) == 0
-    mine, other = half_ref[...].astype(F32), other_ref[...].astype(F32)
+    mine, theirs = half_ref[...].astype(F32), other_ref[...].astype(F32)
     att = jnp.concatenate(
-        [jnp.where(first, mine, other), jnp.where(first, other, mine)], axis=1
+        [jnp.where(first, mine, theirs), jnp.where(first, theirs, mine)], axis=1
     )
     x = rows_ref[...].astype(F32)
     post = att * gains_ref[1:2, :]
@@ -520,14 +547,13 @@
                 msg_ref[j, :, k * chunk : k * chunk + size] = part[:, lo:hi].astype(BF)
     for j in range(nk):
         msg_ref[j, :, 2 * chunk :] = stat
-
-
-def hidden_kernel(model_width, got_ref, msg_ref, s_ref):
-    nk, both, _ = got_ref.shape
-    rows, chunk = both // 2, msg_ref.shape[2]
-    total = got_ref[0].astype(F32)
-    for j in range(1, nk):
-        total = total + got_ref[j].astype(F32)
+    for k, ref in enumerate((m0, m1, m2, m3)):
+        ref[...] = msg_ref[other("kv", k)]
+
+
+def hidden_kernel(model_width, b0, b1, b2, b3, out_ref, s_ref):
+    rows, chunk = out_ref.shape
+    total = four((b0, b1, b2, b3))
     stat = total[:, 2 * chunk :]
     one, two = picked(stat, 0, 2), picked(stat, 2, 2)
     att_square, x_square, cross, post_square = one[:rows], one[rows:], two[:rows], two[rows:]
@@ -537,13 +563,13 @@
     s_ref[...] = jnp.broadcast_to(s, s_ref.shape)
     mixed = (total[:rows, : 2 * chunk] + s * total[rows:, : 2 * chunk]) * scale
     gate, up = mixed[:, :chunk], mixed[:, chunk:]
-    hidden = (gate / (1.0 + jnp.exp(-gate)) * up).astype(BF)
-    for j in range(nk):
-        msg_ref[j] = hidden
-
-
-def down_kernel(got_ref, w_ref, msg_ref):
-    nk, rows, chunk = got_ref.shape
+    out_ref[...] = (gate / (1.0 + jnp.exp(-gate)) * up).astype(BF)
+
+
+def down_kernel(b0, b1, b2, b3, w_ref, msg_ref, held_ref):
+    nk, rows, chunk = held_ref.shape
+    for k, ref in enumerate((b0, b1, b2, b3)):
+        held_ref[other("kv", k)] = ref[...]
     ff_dev = w_ref.shape[0]
     nt, own, _ = msg_ref.shape
     total = None
@@ -551,7 +577,7 @@
         lo, hi = j * chunk, min((j + 1) * chunk, ff_dev)
         if hi > lo:
             part = jnp.dot(
-                got_ref[j, :, : hi - lo], w_ref[lo:hi, :], preferred_element_type=F32
+                held_ref[j, :, : hi - lo], w_ref[lo:hi, :], preferred_element_type=F32
             )
             total = part if total is None else total + part
     total = total.reshape(own, nt, total.shape[1])
@@ -571,8 +597,16 @@
     out_ref[...] = (mid + total).astype(BF)
 
 
-def exchange(message, axis, groups=None):
-    return lax.all_to_all(message, axis, 0, 0, tiled=True, axis_index_groups=groups)
+def exchange(message, axis):
+    return lax.all_to_all(message, axis, 0, 0, tiled=True)
+
+
+def deal(blocks, axis, step=1):
+    size = lax.axis_size(axis)
+    return [blocks[0]] + [
+        lax.ppermute(blocks[k], axis, [(i, i ^ (k * step)) for i in range(size)])
+        for k in range(1, len(blocks))
+    ]
 
 
 def kernel_body(
@@ -611,94 +645,100 @@
     table[0] = np.tile(np.concatenate([cos, cos]), heads)
     table[1] = np.tile(np.concatenate([-sin, sin]), heads)
 
-    tiles = [g.reshape(-1, 128) for g in (attn_gain, post_gain, mlp_gain)]
-    msg, gains = call(
-        start_kernel, [like((nt, own, width)), like((8, width), F32)], resid, *tiles
-    )
-    got = exchange(msg, "tp")
-    msg, x_rows = call(
+    swap = [(i, i ^ 1) for i in range(nt)]
+    both = call(start_kernel, like((nt, width)), resid, lax.ppermute(resid, "tp", swap), flops=WAIT)
+    chips = nt // 2
+    sent_width = nope_dev + rope_dev + latent // 2 + 128
+    *msg, x_rows, gains = call(
         query_kernel,
-        [like((nk, nt, nope_dev + rope_dev + latent // 2 + 128)), like((rows, width))],
-        got,
+        [like((nt, sent_width))] * nk + [like((rows, width)), like((8, width), F32)],
+        *deal([both] * chips, "tp", 2),
         resid,
-        gains,
+        *[g.reshape(-1, 128) for g in (attn_gain, post_gain, mlp_gain)],
         w_query_nope,
         w_query_rope,
         w_latent,
         w_key_rope.T,
-        flops=2 * rows * width * (nope_dev + rope_dev + latent),
-    )
-    got = exchange(msg, "kv")
-    msg, new_latent, new_rope_key = call(
-        functools.partial(latent_kernel, model_width, heads),
-        [like((nk, rows * heads // own, latent + 128)), like((own, latent)), like((own, rope))],
-        got,
-        key_up.reshape(latent, nope_dev),
+        scratch=[pltpu.VMEM((chips, 2 * own, width), F32), pltpu.VMEM((nk, nt, sent_width), BF)],
+        flops=WAIT,
+    )
+    pairs = nt * heads
+    msg, new_latent, new_rope_key, own_block = call(
+        functools.partial(latent_kernel, model_width),
+        [
+            like((nk, pairs, latent + 128)),
+            like((own, latent)),
+            like((own, rope)),
+            like((nt, latent + 128), F32),
+        ],
+        *deal(msg, "kv"),
+        key_up,
         latent_gain.reshape(1, latent),
         jnp.asarray(table),
-        flops=2 * nt * heads * nope_dev * latent,
+        flops=WAIT,
     )
     got = exchange(msg.reshape(nk * nt, heads, latent + 128), ("kv", "tp"))
     msg = call(
         functools.partial(attend_kernel, (nope + rope) ** (-0.5)),
-        like((own, nt * heads, latent + 128)),
-        got.reshape(own, nt * heads, latent + 128),
+        like((own, pairs, latent + 128)),
+        got.reshape(own, pairs, latent + 128),
         cache_latent,
         cache_rope_key.swapaxes(1, 2),
-        new_latent,
-        new_rope_key,
-        flops=4 * own * nt * heads * latent * cache_latent.shape[1],
+        own_block,
+        flops=WAIT,
     )
     got = exchange(msg.reshape(nk * nt, heads, latent + 128), ("kv", "tp"))
     value_dev = heads * value_up.shape[2]
-    msg = call(
-        functools.partial(value_kernel, heads),
-        like((nk, nt, value_dev)),
-        got.reshape(nk, nt * heads, latent + 128),
-        value_up.reshape(latent, value_dev),
-        flops=2 * nt * heads * latent * value_dev,
-    )
-    got = exchange(msg, "kv")
+    o_heads = call(
+        value_kernel,
+        like((nt, value_dev)),
+        got.reshape(nk, pairs, latent + 128),
+        value_up,
+        flops=WAIT,
+    )
     half = width // 2
     keep, give = call(
         out_kernel,
         [like((rows, half), F32), like((rows, half))],
-        got.reshape(rows, value_dev),
+        *deal([o_heads] * nk, "kv"),
         w_out,
-        flops=2 * rows * value_dev * width,
-    )
-    swap = [(i, i ^ 1) for i in range(nt)]
-    column = [list(range(c, nt, 2)) for c in range(2)]
-    got = lax.ppermute(give, "tp", swap)
-    msg = call(pair_kernel, like((nt // 2, rows, half)), keep, got)
-    got = exchange(msg, "tp", column)
-    att_half = call(column_kernel, like((rows, half)), got)
+        scratch=[pltpu.VMEM((nk, nt, value_dev), F32)],
+        flops=WAIT,
+    )
+    pair = call(
+        pair_kernel, like((rows, half)), keep, lax.ppermute(give, "tp", swap), flops=WAIT
+    )
+    att_half = call(
+        column_kernel, like((rows, half)), *deal([pair] * chips, "tp", 2), flops=WAIT
+    )
     att_other = lax.ppermute(att_half, "tp", swap)
     chunk = -(-ff_dev // (nk * 128)) * 128
-    msg, post = call(
+    sent_width = 2 * chunk + 128
+    *msg, post = call(
         gate_kernel,
-        [like((nk, 2 * rows, 2 * chunk + 128)), like((rows, width), F32)],
+        [like((2 * rows, sent_width))] * nk + [like((rows, width), F32)],
         att_half,
         att_other,
         x_rows,
         gains,
         w_gate.T,
         w_up.T,
-        flops=8 * rows * width * ff_dev,
-    )
-    got = exchange(msg, "kv")
-    msg, s = call(
+        scratch=[pltpu.VMEM((nk, 2 * rows, sent_width), BF)],
+        flops=WAIT,
+    )
+    hidden, s = call(
         functools.partial(hidden_kernel, model_width),
-        [like((nk, rows, chunk)), like((rows, 128), F32)],
-        got,
-    )
-    got = exchange(msg, "kv")
+        [like((rows, chunk)), like((rows, 128), F32)],
+        *deal(msg, "kv"),
+        flops=WAIT,
+    )
     msg = call(
         down_kernel,
         like((nt, own, width)),
-        got,
+        *deal([hidden] * nk, "kv"),
         w_down,
-        flops=2 * rows * ff_dev * width,
+        scratch=[pltpu.VMEM((nk, rows, chunk), BF)],
+        flops=WAIT,
     )
     got = exchange(msg, "tp")
     next_resid = call(last_kernel, like((own, width)), got, resid, post, s)
@@ -711,7 +751,7 @@
     own, width = resid.shape
     latent, heads, nope = key_up.shape
     fits = (
-        own == nk
+        own == nk == 4
         and nt == 8
         and heads == 8
         and 2 * own == nt

time: 118 us -> 95.9 us (0.81)
  blocking collectives: 68.9 us -> 37.5 us
  starting transfers between devices: 6.71 us -> 25 us
  local copies, waits for them, and re-layouts: 14.7 us -> 0.78 us
  waiting for transfers between devices: 16.4 us -> 23.6 us
  Pallas kernels: 9.19 us -> 7.9 us
    all_to_all x7 -> x3, blocking collectives: 68.9 us -> 37.5 us  [exchange(): return lax.all_to_all(message, axis, 0, 0, tiled=True)]
    ppermute x1 -> x20, starting transfers between devices: 0.07 us -> 24.9 us  [the longest x18 24.3 us: deal(): lax.ppermute(blocks[k], axis, [(i, i ^ k * step) for i in range(size)])]
    ppermute x1 -> x20, waiting for transfers between devices: 1.19 us -> 22.4 us  [the longest x18 20.2 us: deal(): lax.ppermute(blocks[k], axis, [(i, i ^ k * step) for i in range(size)])]
    all_to_all x2 -> x0, waiting for transfers between devices: 14 us -> none  [exchange(): lax.all_to_all(message, axis, 0, 0, tiled=True, axis_index_groups=groups)]
    unnamed x48 -> x38, local copies, waits for them, and re-layouts: 14.7 us -> 0.78 us
    all_to_all x2 -> x0, starting transfers between devices: 6.57 us -> none  [exchange(): lax.all_to_all(message, axis, 0, 0, tiled=True, axis_index_groups=groups)]
    pallas_call x12, Pallas kernels: 9.19 us -> 7.9 us  [call(): pl.pallas_call(kernel, out_shape=outs, in_specs=[VMEM] * len(args), out_s...]
  transfers between devices with their start and end apart: 4 -> 21, of which waited for: 4 -> 18; matrix products, arithmetic and copies ran while one was open for 3% -> 0% of each run, Pallas kernels for 0% -> 0%
where the time goes in v2:
time: 95.9 us; the launch traced here: 95.6 us
  blocking collectives  37.5 us (39%)
  starting transfers between devices  25 us (26%)
  waiting for transfers between devices  23.6 us (25%)
  Pallas kernels  7.9 us (8%)
    all_to_all x3, blocking collectives, exchange(): return lax.all_to_all(message, axis, 0, 0, tiled=True)  37.5 us
    ppermute x18, starting transfers between devices, deal(): lax.ppermute(blocks[k], axis, [(i, i ^ k * step) for i in range(size)])  24.3 us
    ppermute x18, waiting for transfers between devices, deal(): lax.ppermute(blocks[k], axis, [(i, i ^ k * step) for i in range(size)])  20.2 us
    pallas_call x12, Pallas kernels, call(): pl.pallas_call(kernel, out_shape=outs, in_specs=[VMEM] * len(args), out_s...  7.9 us
  transfers between devices with their start and end apart: 21, of which 18 were waited for; matrix products, arithmetic and copies ran while one was open for 0% of the time, Pallas kernels for 0%

profile of v2, /device:TPU:0, one launch (start us, length us, event | category | flops | bytes accessed | tf_op | source)
XLA Modules:
  0.0 95.6 jit_solution(8148437593021571279)
XLA Ops:
  3.0 5.0 %collective-permute-start.3 = (bf16[8,1024]{1,0:T(8,128)(2,1)S(1)}, bf16[8,1024]{1,0:T(8,128)(2,1)S(1)}, u32[]{:S(2)}, u32[]{:S(2)}) collective-permute-start(bf16[8,1024]{1,0:T(8,128)(2,1)S(1)} %shard_map.193.b0), channel_id=1, source_target_pairs={{0,6},{1,7},{2,4},{3,5},{4,2},{5,3},{6,0},{7,1},{8,14},{9,15},{10,... | collective-permute-start | bytes 49160 | tf_op jit(solution)/shard_map/ppermute | solution.py:607
  9.7 2.9 %collective-permute-done.2.b2 = bf16[8,1024]{1,0:T(8,128)(2,1)S(1)} collective-permute-done((bf16[8,1024]{1,0:T(8,128)(2,1)S(1)}, bf16[8,1024]{1,0:T(8,128)(2,1)S(1)}, u32[]{:S(2)}, u32[]{:S(2)}) %collective-permute-start.2) | collective-permute-done | bytes 16416 | tf_op jit(solution)/shard_map/ppermute | solution.py:607
  13.6 1.6 %collective-permute-start.4 = (bf16[8,1920]{1,0:T(8,128)(2,1)S(1)}, bf16[8,1920]{1,0:T(8,128)(2,1)S(1)}, u32[]{:S(2)}, u32[]{:S(2)}) collective-permute-start(bf16[8,1920]{1,0:T(8,128)(2,1)S(1)} %get-tuple-element.23), channel_id=1, source_target_pairs={{0,8},{8,0},{16,24},{24,16},{1,9},{9,1},{17,25},{25,17},{2,10},{10... | collective-permute-start | bytes 92168 | tf_op jit(solution)/shard_map/ppermute | solution.py:607
  15.1 1.5 %collective-permute-start.5 = (bf16[8,1920]{1,0:T(8,128)(2,1)S(1)}, bf16[8,1920]{1,0:T(8,128)(2,1)S(1)}, u32[]{:S(2)}, u32[]{:S(2)}) collective-permute-start(bf16[8,1920]{1,0:T(8,128)(2,1)S(1)} %get-tuple-element.24), channel_id=1, source_target_pairs={{0,16},{8,24},{16,0},{24,8},{1,17},{9,25},{17,1},{25,9},{2,18},{10... | collective-permute-start | bytes 92168 | tf_op jit(solution)/shard_map/ppermute | solution.py:607
  17.7 1.5 %collective-permute-done.5.b2 = bf16[8,1920]{1,0:T(8,128)(2,1)S(1)} collective-permute-done((bf16[8,1920]{1,0:T(8,128)(2,1)S(1)}, bf16[8,1920]{1,0:T(8,128)(2,1)S(1)}, u32[]{:S(2)}, u32[]{:S(2)}) %collective-permute-start.5) | collective-permute-done | bytes 30752 | tf_op jit(solution)/shard_map/ppermute | solution.py:607
  19.2 2.3 %collective-permute-done.6.b3 = bf16[8,1920]{1,0:T(8,128)(2,1)S(1)} collective-permute-done((bf16[8,1920]{1,0:T(8,128)(2,1)S(1)}, bf16[8,1920]{1,0:T(8,128)(2,1)S(1)}, u32[]{:S(2)}, u32[]{:S(2)}) %collective-permute-start.6) | collective-permute-done | bytes 30752 | tf_op jit(solution)/shard_map/ppermute | solution.py:607
  22.5 14.2 %all_to_all.15 = bf16[32,8,640]{2,1,0:T(8,128)(2,1)S(1)} all-to-all(bf16[32,8,640]{2,1,0:T(8,128)(2,1)S(1)} %bitcast.11), channel_id=1, replica_groups=mesh['kv'=4,'tp'=8] {'kv','tp'}, dimensions={0} | all-to-all | bytes 655360 | tf_op jit(solution)/shard_map/all_to_all | solution.py:601
  36.7 1.9 %shard_map.196 = bf16[4,64,640]{2,1,0:T(8,128)(2,1)S(1)} custom-call(bf16[4,64,640]{2,1,0:T(8,128)(2,1)S(1)} %bitcast.12, bf16[4,512,512]{2,1,0:T(8,128)(2,1)S(1)} %copy-done.6, bf16[4,64,512]{2,1,0:T(8,128)(2,1)S(1)} %bitcast.18, f32[8,640]{1,0:T(8,128)S(1)} %get-tuple-element.27.own_ref), custom_call_target="tpu_custom_call" | custom-call | flops 4000000000 | bytes 3035136 | tf_op jit(solution)/shard_map/pallas_call | solution.py:272
  38.5 14.1 %all_to_all.16 = bf16[32,8,640]{2,1,0:T(8,128)(2,1)S(1)} all-to-all(bf16[32,8,640]{2,1,0:T(8,128)(2,1)S(1)} %bitcast.13), channel_id=1, replica_groups=mesh['kv'=4,'tp'=8] {'kv','tp'}, dimensions={0} | all-to-all | bytes 655360 | tf_op jit(solution)/shard_map/all_to_all | solution.py:601
  54.4 2.2 %collective-permute-start.7 = (bf16[8,1024]{1,0:T(8,128)(2,1)S(1)}, bf16[8,1024]{1,0:T(8,128)(2,1)S(1)}, u32[]{:S(2)}, u32[]{:S(2)}) collective-permute-start(bf16[8,1024]{1,0:T(8,128)(2,1)S(1)} %shard_map.197.b0), channel_id=1, source_target_pairs={{0,8},{8,0},{16,24},{24,16},{1,9},{9,1},{17,25},{25,17},{2,10},{10... | collective-permute-start | bytes 49160 | tf_op jit(solution)/shard_map/ppermute | solution.py:607
  56.6 1.3 %collective-permute-done.9.b3 = bf16[8,1024]{1,0:T(8,128)(2,1)S(1)} collective-permute-done((bf16[8,1024]{1,0:T(8,128)(2,1)S(1)}, bf16[8,1024]{1,0:T(8,128)(2,1)S(1)}, u32[]{:S(2)}, u32[]{:S(2)}) %collective-permute-start.9) | collective-permute-done | bytes 16416 | tf_op jit(solution)/shard_map/ppermute | solution.py:607
  58.9 1.2 %collective-permute-done.10.got_ref = bf16[32,512]{1,0:T(8,128)(2,1)S(1)} collective-permute-done((bf16[32,512]{1,0:T(8,128)(2,1)S(1)}, bf16[32,512]{1,0:T(8,128)(2,1)S(1)}, u32[]{:S(2)}, u32[]{:S(2)}) %collective-permute-start.10) | collective-permute-done | bytes 32800 | tf_op jit(solution)/shard_map/ppermute | solution.py:709
  60.1 1.6 %collective-permute-start.13 = (bf16[32,512]{1,0:T(8,128)(2,1)S(1)}, bf16[32,512]{1,0:T(8,128)(2,1)S(1)}, u32[]{:S(2)}, u32[]{:S(2)}) collective-permute-start(bf16[32,512]{1,0:T(8,128)(2,1)S(1)} %shard_map.199.b0), channel_id=1, source_target_pairs={{0,6},{1,7},{2,4},{3,5},{4,2},{5,3},{6,0},{7,1},{8,14},{9,15},{10,... | collective-permute-start | bytes 98312 | tf_op jit(solution)/shard_map/ppermute | solution.py:607
  62.1 2.5 %collective-permute-start.11 = (bf16[32,512]{1,0:T(8,128)(2,1)S(1)}, bf16[32,512]{1,0:T(8,128)(2,1)S(1)}, u32[]{:S(2)}, u32[]{:S(2)}) collective-permute-start(bf16[32,512]{1,0:T(8,128)(2,1)S(1)} %shard_map.199.b0), channel_id=1, source_target_pairs={{0,2},{1,3},{2,0},{3,1},{4,6},{5,7},{6,4},{7,5},{8,10},{9,11},{10,... | collective-permute-start | bytes 98312 | tf_op jit(solution)/shard_map/ppermute | solution.py:607
  64.6 1.3 %collective-permute-done.13.b3 = bf16[32,512]{1,0:T(8,128)(2,1)S(1)} collective-permute-done((bf16[32,512]{1,0:T(8,128)(2,1)S(1)}, bf16[32,512]{1,0:T(8,128)(2,1)S(1)}, u32[]{:S(2)}, u32[]{:S(2)}) %collective-permute-start.13) | collective-permute-done | bytes 32800 | tf_op jit(solution)/shard_map/ppermute | solution.py:607
  68.3 1.8 %shard_map.201 = (bf16[64,896]{1,0:T(8,128)(2,1)S(1)}, bf16[64,896]{1,0:T(8,128)(2,1)S(1)}, bf16[64,896]{1,0:T(8,128)(2,1)S(1)}, bf16[64,896]{1,0:T(8,128)(2,1)S(1)}, f32[32,1024]{1,0:T(8,128)S(1)}) custom-call(bf16[32,512]{1,0:T(8,128)(2,1)S(1)} %shard_map.200.half_ref, bf16[32,512]{1,0:T(8,128)(2,1)S(1)} %collective-permute-done.14.other_ref, ...), custom_call_target="tpu_custom_call" | custom-call | flops 4000000000 | bytes 6389760 | tf_op jit(solution)/shard_map/pallas_call | solution.py:272
  70.0 1.6 %collective-permute-start.15 = (bf16[64,896]{1,0:T(8,128)(2,1)S(1)}, bf16[64,896]{1,0:T(8,128)(2,1)S(1)}, u32[]{:S(2)}, u32[]{:S(2)}) collective-permute-start(bf16[64,896]{1,0:T(8,128)(2,1)S(1)} %get-tuple-element.33), channel_id=1, source_target_pairs={{0,8},{8,0},{16,24},{24,16},{1,9},{9,1},{17,25},{25,17},{2,10},{10... | collective-permute-start | bytes 344072 | tf_op jit(solution)/shard_map/ppermute | solution.py:607
  72.4 1.2 %collective-permute-start.17 = (bf16[64,896]{1,0:T(8,128)(2,1)S(1)}, bf16[64,896]{1,0:T(8,128)(2,1)S(1)}, u32[]{:S(2)}, u32[]{:S(2)}) collective-permute-start(bf16[64,896]{1,0:T(8,128)(2,1)S(1)} %get-tuple-element.35), channel_id=1, source_target_pairs={{0,24},{8,16},{16,8},{24,0},{1,25},{9,17},{17,9},{25,1},{2,26},{10... | collective-permute-start | bytes 344072 | tf_op jit(solution)/shard_map/ppermute | solution.py:607
  73.6 1.7 %collective-permute-done.15.b1 = bf16[64,896]{1,0:T(8,128)(2,1)S(1)} collective-permute-done((bf16[64,896]{1,0:T(8,128)(2,1)S(1)}, bf16[64,896]{1,0:T(8,128)(2,1)S(1)}, u32[]{:S(2)}, u32[]{:S(2)}) %collective-permute-start.15) | collective-permute-done | bytes 114720 | tf_op jit(solution)/shard_map/ppermute | solution.py:607
  75.3 3.7 %collective-permute-done.16.b2 = bf16[64,896]{1,0:T(8,128)(2,1)S(1)} collective-permute-done((bf16[64,896]{1,0:T(8,128)(2,1)S(1)}, bf16[64,896]{1,0:T(8,128)(2,1)S(1)}, u32[]{:S(2)}, u32[]{:S(2)}) %collective-permute-start.16) | collective-permute-done | bytes 114720 | tf_op jit(solution)/shard_map/ppermute | solution.py:607
  79.2 1.2 %collective-permute-start.20 = (bf16[32,384]{1,0:T(8,128)(2,1)S(1)}, bf16[32,384]{1,0:T(8,128)(2,1)S(1)}, u32[]{:S(2)}, u32[]{:S(2)}) collective-permute-start(bf16[32,384]{1,0:T(8,128)(2,1)S(1)} %get-tuple-element.36.b0), channel_id=1, source_target_pairs={{0,24},{8,16},{16,8},{24,0},{1,25},{9,17},{17,9},{25,1},{2,26},{10... | collective-permute-start | bytes 73736 | tf_op jit(solution)/shard_map/ppermute | solution.py:607
  81.2 1.5 %collective-permute-start.18 = (bf16[32,384]{1,0:T(8,128)(2,1)S(1)}, bf16[32,384]{1,0:T(8,128)(2,1)S(1)}, u32[]{:S(2)}, u32[]{:S(2)}) collective-permute-start(bf16[32,384]{1,0:T(8,128)(2,1)S(1)} %get-tuple-element.36.b0), channel_id=1, source_target_pairs={{0,8},{8,0},{16,24},{24,16},{1,9},{9,1},{17,25},{25,17},{2,10},{10... | collective-permute-start | bytes 73736 | tf_op jit(solution)/shard_map/ppermute | solution.py:607
  82.7 1.2 %collective-permute-done.20.b3 = bf16[32,384]{1,0:T(8,128)(2,1)S(1)} collective-permute-done((bf16[32,384]{1,0:T(8,128)(2,1)S(1)}, bf16[32,384]{1,0:T(8,128)(2,1)S(1)}, u32[]{:S(2)}, u32[]{:S(2)}) %collective-permute-start.20) | collective-permute-done | bytes 24608 | tf_op jit(solution)/shard_map/ppermute | solution.py:607
  85.7 9.2 %all_to_all.17.got_ref = bf16[8,4,1024]{2,1,0:T(4,128)(2,1)S(1)} all-to-all(bf16[8,4,1024]{2,1,0:T(4,128)(2,1)S(1)} %shard_map.203), channel_id=1, replica_groups=mesh['kv'=4,'tp'=8] {'tp'}, dimensions={0} | all-to-all | bytes 131072 | tf_op jit(solution)/shard_map/all_to_all | solution.py:601
  (72 shorter events, 16.5 us)
Async XLA Ops:
  0.6 1.6 %collective-permute-start = (bf16[4,1024]{1,0:T(4,128)(2,1)}, bf16[4,1024]{1,0:T(4,128)(2,1)S(1)}, u32[]{:S(2)}, u32[]{:S(2)}) collective-permute-start(bf16[4,1024]{1,0:T(4,128)(2,1)} %resid_ref.5), channel_id=1, source_target_pairs={{0,1},{1,0},{2,3},{3,2},{4,5},{5,4},{6,7},{7,6},{8,9},{9,8},{10,11... | collective-permute-start | bytes 24584 | tf_op jit(solution)/shard_map/ppermute | solution.py:649
  3.0 6.7 %collective-permute-start.3 = (bf16[8,1024]{1,0:T(8,128)(2,1)S(1)}, bf16[8,1024]{1,0:T(8,128)(2,1)S(1)}, u32[]{:S(2)}, u32[]{:S(2)}) collective-permute-start(bf16[8,1024]{1,0:T(8,128)(2,1)S(1)} %shard_map.193.b0), channel_id=1, source_target_pairs={{0,6},{1,7},{2,4},{3,5},{4,2},{5,3},{6,0},{7,1},{8,14},{9,15},{10,... | collective-permute-start | bytes 49160 | tf_op jit(solution)/shard_map/ppermute | solution.py:607
  8.0 4.6 %collective-permute-start.2 = (bf16[8,1024]{1,0:T(8,128)(2,1)S(1)}, bf16[8,1024]{1,0:T(8,128)(2,1)S(1)}, u32[]{:S(2)}, u32[]{:S(2)}) collective-permute-start(bf16[8,1024]{1,0:T(8,128)(2,1)S(1)} %shard_map.193.b0), channel_id=1, source_target_pairs={{0,4},{1,5},{2,6},{3,7},{4,0},{5,1},{6,2},{7,3},{8,12},{9,13},{10,... | collective-permute-start | bytes 49160 | tf_op jit(solution)/shard_map/ppermute | solution.py:607
  8.0 4.6 %collective-permute-start.1 = (bf16[8,1024]{1,0:T(8,128)(2,1)S(1)}, bf16[8,1024]{1,0:T(8,128)(2,1)S(1)}, u32[]{:S(2)}, u32[]{:S(2)}) collective-permute-start(bf16[8,1024]{1,0:T(8,128)(2,1)S(1)} %shard_map.193.b0), channel_id=1, source_target_pairs={{0,2},{1,3},{2,0},{3,1},{4,6},{5,7},{6,4},{7,5},{8,10},{9,11},{10,... | collective-permute-start | bytes 49160 | tf_op jit(solution)/shard_map/ppermute | solution.py:607
  13.6 4.1 %collective-permute-start.4 = (bf16[8,1920]{1,0:T(8,128)(2,1)S(1)}, bf16[8,1920]{1,0:T(8,128)(2,1)S(1)}, u32[]{:S(2)}, u32[]{:S(2)}) collective-permute-start(bf16[8,1920]{1,0:T(8,128)(2,1)S(1)} %get-tuple-element.23), channel_id=1, source_target_pairs={{0,8},{8,0},{16,24},{24,16},{1,9},{9,1},{17,25},{25,17},{2,10},{10... | collective-permute-start | bytes 92168 | tf_op jit(solution)/shard_map/ppermute | solution.py:607
  15.1 4.0 %collective-permute-start.5 = (bf16[8,1920]{1,0:T(8,128)(2,1)S(1)}, bf16[8,1920]{1,0:T(8,128)(2,1)S(1)}, u32[]{:S(2)}, u32[]{:S(2)}) collective-permute-start(bf16[8,1920]{1,0:T(8,128)(2,1)S(1)} %get-tuple-element.24), channel_id=1, source_target_pairs={{0,16},{8,24},{16,0},{24,8},{1,17},{9,25},{17,1},{25,9},{2,18},{10... | collective-permute-start | bytes 92168 | tf_op jit(solution)/shard_map/ppermute | solution.py:607
  16.7 4.8 %collective-permute-start.6 = (bf16[8,1920]{1,0:T(8,128)(2,1)S(1)}, bf16[8,1920]{1,0:T(8,128)(2,1)S(1)}, u32[]{:S(2)}, u32[]{:S(2)}) collective-permute-start(bf16[8,1920]{1,0:T(8,128)(2,1)S(1)} %get-tuple-element.25), channel_id=1, source_target_pairs={{0,24},{8,16},{16,8},{24,0},{1,25},{9,17},{17,9},{25,1},{2,26},{10... | collective-permute-start | bytes 92168 | tf_op jit(solution)/shard_map/ppermute | solution.py:607
  21.5 15.2 %copy-start.13 = (bf16[4,512,64]{1,2,0:T(8,128)(2,1)S(1)}, bf16[4,512,64]{1,2,0:T(8,128)(2,1)}, u32[]{:S(2)}) copy-start(bf16[4,512,64]{1,2,0:T(8,128)(2,1)} %param.34) | copy-start | bytes 786436
  36.7 15.9 %copy-start.11 = (bf16[512,8,128]{2,1,0:T(8,128)(2,1)S(1)}, bf16[512,8,128]{2,1,0:T(8,128)(2,1)}, u32[]{:S(2)}) copy-start(bf16[512,8,128]{2,1,0:T(8,128)(2,1)} %vu_ref.1) | copy-start | bytes 3145732
  53.0 4.8 %collective-permute-start.9 = (bf16[8,1024]{1,0:T(8,128)(2,1)S(1)}, bf16[8,1024]{1,0:T(8,128)(2,1)S(1)}, u32[]{:S(2)}, u32[]{:S(2)}) collective-permute-start(bf16[8,1024]{1,0:T(8,128)(2,1)S(1)} %shard_map.197.b0), channel_id=1, source_target_pairs={{0,24},{8,16},{16,8},{24,0},{1,25},{9,17},{17,9},{25,1},{2,26},{10... | collective-permute-start | bytes 49160 | tf_op jit(solution)/shard_map/ppermute | solution.py:607
  53.7 4.2 %collective-permute-start.8 = (bf16[8,1024]{1,0:T(8,128)(2,1)S(1)}, bf16[8,1024]{1,0:T(8,128)(2,1)S(1)}, u32[]{:S(2)}, u32[]{:S(2)}) collective-permute-start(bf16[8,1024]{1,0:T(8,128)(2,1)S(1)} %shard_map.197.b0), channel_id=1, source_target_pairs={{0,16},{8,24},{16,0},{24,8},{1,17},{9,25},{17,1},{25,9},{2,18},{10... | collective-permute-start | bytes 49160 | tf_op jit(solution)/shard_map/ppermute | solution.py:607
  54.4 4.0 %collective-permute-start.7 = (bf16[8,1024]{1,0:T(8,128)(2,1)S(1)}, bf16[8,1024]{1,0:T(8,128)(2,1)S(1)}, u32[]{:S(2)}, u32[]{:S(2)}) collective-permute-start(bf16[8,1024]{1,0:T(8,128)(2,1)S(1)} %shard_map.197.b0), channel_id=1, source_target_pairs={{0,8},{8,0},{16,24},{24,16},{1,9},{9,1},{17,25},{25,17},{2,10},{10... | collective-permute-start | bytes 49160 | tf_op jit(solution)/shard_map/ppermute | solution.py:607
  58.8 1.3 %collective-permute-start.10 = (bf16[32,512]{1,0:T(8,128)(2,1)S(1)}, bf16[32,512]{1,0:T(8,128)(2,1)S(1)}, u32[]{:S(2)}, u32[]{:S(2)}) collective-permute-start(bf16[32,512]{1,0:T(8,128)(2,1)S(1)} %get-tuple-element.29), channel_id=1, source_target_pairs={{0,1},{1,0},{2,3},{3,2},{4,5},{5,4},{6,7},{7,6},{8,9},{9,8},{10,11... | collective-permute-start | bytes 98312 | tf_op jit(solution)/shard_map/ppermute | solution.py:709
  60.1 5.8 %collective-permute-start.13 = (bf16[32,512]{1,0:T(8,128)(2,1)S(1)}, bf16[32,512]{1,0:T(8,128)(2,1)S(1)}, u32[]{:S(2)}, u32[]{:S(2)}) collective-permute-start(bf16[32,512]{1,0:T(8,128)(2,1)S(1)} %shard_map.199.b0), channel_id=1, source_target_pairs={{0,6},{1,7},{2,4},{3,5},{4,2},{5,3},{6,0},{7,1},{8,14},{9,15},{10,... | collective-permute-start | bytes 98312 | tf_op jit(solution)/shard_map/ppermute | solution.py:607
  61.7 5.1 %collective-permute-start.12 = (bf16[32,512]{1,0:T(8,128)(2,1)S(1)}, bf16[32,512]{1,0:T(8,128)(2,1)S(1)}, u32[]{:S(2)}, u32[]{:S(2)}) collective-permute-start(bf16[32,512]{1,0:T(8,128)(2,1)S(1)} %shard_map.199.b0), channel_id=1, source_target_pairs={{0,4},{1,5},{2,6},{3,7},{4,0},{5,1},{6,2},{7,3},{8,12},{9,13},{10,... | collective-permute-start | bytes 98312 | tf_op jit(solution)/shard_map/ppermute | solution.py:607
  62.1 4.9 %collective-permute-start.11 = (bf16[32,512]{1,0:T(8,128)(2,1)S(1)}, bf16[32,512]{1,0:T(8,128)(2,1)S(1)}, u32[]{:S(2)}, u32[]{:S(2)}) collective-permute-start(bf16[32,512]{1,0:T(8,128)(2,1)S(1)} %shard_map.199.b0), channel_id=1, source_target_pairs={{0,2},{1,3},{2,0},{3,1},{4,6},{5,7},{6,4},{7,5},{8,10},{9,11},{10,... | collective-permute-start | bytes 98312 | tf_op jit(solution)/shard_map/ppermute | solution.py:607
  67.0 1.3 %collective-permute-start.14 = (bf16[32,512]{1,0:T(8,128)(2,1)S(1)}, bf16[32,512]{1,0:T(8,128)(2,1)S(1)}, u32[]{:S(2)}, u32[]{:S(2)}) collective-permute-start(bf16[32,512]{1,0:T(8,128)(2,1)S(1)} %shard_map.200.half_ref), channel_id=1, source_target_pairs={{0,1},{1,0},{2,3},{3,2},{4,5},{5,4},{6,7},{7,6},{8,9},{9,8},{10,11... | collective-permute-start | bytes 98312 | tf_op jit(solution)/shard_map/ppermute | solution.py:714
  70.0 5.3 %collective-permute-start.15 = (bf16[64,896]{1,0:T(8,128)(2,1)S(1)}, bf16[64,896]{1,0:T(8,128)(2,1)S(1)}, u32[]{:S(2)}, u32[]{:S(2)}) collective-permute-start(bf16[64,896]{1,0:T(8,128)(2,1)S(1)} %get-tuple-element.33), channel_id=1, source_target_pairs={{0,8},{8,0},{16,24},{24,16},{1,9},{9,1},{17,25},{25,17},{2,10},{10... | collective-permute-start | bytes 344072 | tf_op jit(solution)/shard_map/ppermute | solution.py:607
  71.6 7.4 %collective-permute-start.16 = (bf16[64,896]{1,0:T(8,128)(2,1)S(1)}, bf16[64,896]{1,0:T(8,128)(2,1)S(1)}, u32[]{:S(2)}, u32[]{:S(2)}) collective-permute-start(bf16[64,896]{1,0:T(8,128)(2,1)S(1)} %get-tuple-element.34), channel_id=1, source_target_pairs={{0,16},{8,24},{16,0},{24,8},{1,17},{9,25},{17,1},{25,9},{2,18},{10... | collective-permute-start | bytes 344072 | tf_op jit(solution)/shard_map/ppermute | solution.py:607
  72.4 6.6 %collective-permute-start.17 = (bf16[64,896]{1,0:T(8,128)(2,1)S(1)}, bf16[64,896]{1,0:T(8,128)(2,1)S(1)}, u32[]{:S(2)}, u32[]{:S(2)}) collective-permute-start(bf16[64,896]{1,0:T(8,128)(2,1)S(1)} %get-tuple-element.35), channel_id=1, source_target_pairs={{0,24},{8,16},{16,8},{24,0},{1,25},{9,17},{17,9},{25,1},{2,26},{10... | collective-permute-start | bytes 344072 | tf_op jit(solution)/shard_map/ppermute | solution.py:607
  79.2 15.7 %copy-start.1 = (bf16[4,1024]{1,0:T(4,128)(2,1)S(1)}, bf16[4,1024]{1,0:T(4,128)(2,1)}, u32[]{:S(2)}) copy-start(bf16[4,1024]{1,0:T(4,128)(2,1)} %resid_ref.5) | copy-start | bytes 24580
  79.2 4.8 %collective-permute-start.20 = (bf16[32,384]{1,0:T(8,128)(2,1)S(1)}, bf16[32,384]{1,0:T(8,128)(2,1)S(1)}, u32[]{:S(2)}, u32[]{:S(2)}) collective-permute-start(bf16[32,384]{1,0:T(8,128)(2,1)S(1)} %get-tuple-element.36.b0), channel_id=1, source_target_pairs={{0,24},{8,16},{16,8},{24,0},{1,25},{9,17},{17,9},{25,1},{2,26},{10... | collective-permute-start | bytes 73736 | tf_op jit(solution)/shard_map/ppermute | solution.py:607
  80.4 3.8 %collective-permute-start.19 = (bf16[32,384]{1,0:T(8,128)(2,1)S(1)}, bf16[32,384]{1,0:T(8,128)(2,1)S(1)}, u32[]{:S(2)}, u32[]{:S(2)}) collective-permute-start(bf16[32,384]{1,0:T(8,128)(2,1)S(1)} %get-tuple-element.36.b0), channel_id=1, source_target_pairs={{0,16},{8,24},{16,0},{24,8},{1,17},{9,25},{17,1},{25,9},{2,18},{10... | collective-permute-start | bytes 73736 | tf_op jit(solution)/shard_map/ppermute | solution.py:607
  81.2 3.8 %collective-permute-start.18 = (bf16[32,384]{1,0:T(8,128)(2,1)S(1)}, bf16[32,384]{1,0:T(8,128)(2,1)S(1)}, u32[]{:S(2)}, u32[]{:S(2)}) collective-permute-start(bf16[32,384]{1,0:T(8,128)(2,1)S(1)} %get-tuple-element.36.b0), channel_id=1, source_target_pairs={{0,8},{8,0},{16,24},{24,16},{1,9},{9,1},{17,25},{25,17},{2,10},{10... | collective-permute-start | bytes 73736 | tf_op jit(solution)/shard_map/ppermute | solution.py:607
  (16 other events, 134.0 us)

commit v3 on v2

--- a/solution.py
+++ b/solution.py
@@ -7,6 +7,7 @@
 from jax.experimental import pallas as pl
 from jax.experimental.pallas import tpu as pltpu
 from jax.sharding import PartitionSpec as P
+
 
 EPS = 1e-06
 THETA = 10000.0
@@ -326,34 +327,38 @@
     return jnp.bitwise_xor(lax.div(lax.axis_index(axis), step), k)
 
 
-def start_kernel(resid_ref, got_ref, out_ref):
-    first = lax.rem(lax.axis_index("tp"), 2) == 0
-    mine, theirs = resid_ref[...].astype(F32), got_ref[...].astype(F32)
+def unit_kernel(out_ref):
+    row = lax.rem(lax.broadcasted_iota(jnp.int32, out_ref.shape, 0), out_ref.shape[1] // 2)
+    out_ref[...] = jnp.where(row == lane_of(out_ref.shape), 1.0, 0.0).astype(BF)
+
+
+def flat_kernel(in_ref, out_ref):
+    out_ref[...] = in_ref[...].reshape(out_ref.shape)
+
+
+def start_kernel(b0, b1, b2, b3, unit_ref, out_ref, held_ref):
+    chips, own, _ = held_ref.shape
+    for k, ref in enumerate((b0, b1, b2, b3)):
+        held_ref[other("tp", k, 2)] = ref[...].astype(F32)
     out_ref[...] = jnp.concatenate(
-        [jnp.where(first, mine, theirs), jnp.where(first, theirs, mine)], axis=0
+        [held_ref[z, r : r + 1, :] for r in range(own) for z in range(chips)], axis=0
     ).astype(BF)
 
 
 def query_kernel(
-    b0, b1, b2, b3, resid_ref, ga_ref, gp_ref, gm_ref, wn_ref, wr_ref, wl_ref, wk_ref,
-    m0, m1, m2, m3, rows_ref, gains_ref, held_ref, sent_ref,
+    half_ref, other_ref, resid_ref, ga_ref, gp_ref, gm_ref, wn_ref, wr_ref, wl_ref, wk_ref,
+    m3, m2, m1, m0, rows_ref, gains_ref, sent_ref,
 ):
     own, width = resid_ref.shape
-    chips = held_ref.shape[0]
-    nt = 2 * chips
+    nt = rows_ref.shape[0] // own
     latent = wl_ref.shape[1]
     rope = wk_ref.shape[0]
     nope_dev, rope_dev = wn_ref.shape[1], wr_ref.shape[1]
-    for k, ref in enumerate((b0, b1, b2, b3)):
-        held_ref[other("tp", k, 2)] = ref[...].astype(F32)
+    first = lax.rem(lax.axis_index("tp"), 2) == 0
+    mine, theirs = half_ref[...].astype(F32), other_ref[...].astype(F32)
+    cores = (jnp.where(first, mine, theirs), jnp.where(first, theirs, mine))
     x = jnp.concatenate(
-        [
-            held_ref[z, c * own + r : c * own + r + 1, :]
-            for r in range(own)
-            for z in range(chips)
-            for c in range(2)
-        ],
-        axis=0,
+        [core[i : i + 1] for i in range(mine.shape[0]) for core in cores], axis=0
     )
     rows_ref[...] = x.astype(BF)
     tiles = width // 128
@@ -397,11 +402,14 @@
 
 
 def latent_kernel(
-    model_width, b0, b1, b2, b3, ku_ref, gain_ref, table_ref, msg_ref, lat_ref, key_ref, own_ref
+    model_width, b0, b1, b2, b3, ku_ref, gain_ref, table_ref, unit_ref,
+    msg_ref, lat_ref, key_ref, own_ref,
 ):
-    nk, nt = msg_ref.shape[0], b0.shape[0]
-    latent, heads, nope = ku_ref.shape
-    nope_dev = heads * nope
+    nk, pairs, _ = msg_ref.shape
+    nt = b0.shape[0]
+    heads = pairs // nt
+    latent, nope_dev = ku_ref.shape
+    nope = nope_dev // heads
     own, rope = key_ref.shape
     rope_dev = heads * rope
     total = four((b0, b1, b2, b3))
@@ -431,12 +439,9 @@
         return jnp.where(keep, spread_q, 0.0).reshape(nt * heads, heads * size).astype(BF)
 
     q_lat = lax.dot_general(
-        diagonal(qn, nope), ku_ref[...].reshape(latent, nope_dev), NT, preferred_element_type=F32
+        diagonal(qn, nope), ku_ref[...], NT, preferred_element_type=F32
     ).astype(BF)
-    shape = (rope_dev, 128)
-    row = lax.rem(lax.broadcasted_iota(jnp.int32, shape, 0), rope)
-    unit = jnp.where(row == lane_of(shape), 1.0, 0.0).astype(BF)
-    q_rope = jnp.dot(diagonal(qr, rope), unit, preferred_element_type=F32).astype(BF)
+    q_rope = jnp.dot(diagonal(qr, rope), unit_ref[...], preferred_element_type=F32).astype(BF)
     for j in range(nk):
         msg_ref[j, :, :latent] = q_lat
         msg_ref[j, :, latent:] = q_rope
@@ -470,10 +475,10 @@
         msg_ref[r, :, latent:] = placed(columns, (all_heads, 128)).astype(BF)
 
 
-def value_kernel(got_ref, vu_ref, out_ref):
+def value_kernel(heads, got_ref, vu_ref, a0, a1, a2, a3, m3, m2, m1, m0):
     nk, pairs, _ = got_ref.shape
-    latent, heads, size = vu_ref.shape
-    value_dev = heads * size
+    latent, value_dev = vu_ref.shape
+    size = value_dev // heads
     nt = pairs // heads
     stats = [got_ref[j, :, latent:].astype(F32) for j in range(nk)]
     peaks = [picked(s, 0, 3) for s in stats]
@@ -482,18 +487,24 @@
     total = sum(picked(s, 3, 3) * f for s, f in zip(stats, factors))
     value = sum(got_ref[j, :, :latent].astype(F32) * f for j, f in enumerate(factors))
     o_lat = (value / total).astype(BF)
-    full = jnp.dot(o_lat, vu_ref[...].reshape(latent, value_dev), preferred_element_type=F32)
+    full = jnp.dot(o_lat, vu_ref[...], preferred_element_type=F32)
     shape = (nt, heads, value_dev)
     head = lax.broadcasted_iota(jnp.int32, shape, 1)
     lane = lax.broadcasted_iota(jnp.int32, shape, 2)
     keep = (lane >= head * size) & (lane < (head + 1) * size)
-    out_ref[...] = jnp.sum(jnp.where(keep, full.reshape(shape), 0.0), axis=1).astype(BF)
-
-
-def out_kernel(b0, b1, b2, b3, w_ref, keep_ref, give_ref, held_ref):
+    o_heads = jnp.sum(jnp.where(keep, full.reshape(shape), 0.0), axis=1).astype(BF)
+    for a, m in ((a3, m3), (a2, m2), (a1, m1), (a0, m0)):
+        m[:nt] = o_heads
+        m[nt:, : a.shape[1]] = a[...]
+
+
+def out_kernel(b0, b1, b2, b3, w_ref, keep_ref, give_ref, base_ref, held_ref):
     half = keep_ref.shape[1]
+    nt, wide = held_ref.shape[1], base_ref.shape[1]
     for k, ref in enumerate((b0, b1, b2, b3)):
-        held_ref[other("kv", k)] = ref[...].astype(F32)
+        held_ref[other("kv", k)] = ref[:nt].astype(F32)
+    a, b, c, d = (ref[nt:, :wide].astype(F32) for ref in (b0, b1, b2, b3))
+    base_ref[...] = (a + b) + (c + d)
     first = lax.rem(lax.axis_index("tp"), 2) == 0
     o_heads = held_ref[...].reshape(keep_ref.shape[0], w_ref.shape[0]).astype(BF)
     out = jnp.dot(o_heads, w_ref[...], preferred_element_type=F32)
@@ -509,13 +520,39 @@
     out_ref[...] = four((b0, b1, b2, b3)).astype(BF)
 
 
+def added(a, b):
+    return jnp.sum(a * b, axis=1, keepdims=True)
+
+
+def send_parts(left, wg_ref, wu_ref, sums, refs, msg_ref):
+    nk, rows, wide = msg_ref.shape
+    ff_dev, chunk = wg_ref.shape[0], (wide - 128) // 2
+    columns = list(enumerate(t for value in sums for t in terms(value, 2)))
+    stat = placed(columns, (rows, 128)).astype(BF)
+    for k, w_ref in enumerate((wg_ref, wu_ref)):
+        part = lax.dot_general(left, w_ref[...], NT, preferred_element_type=F32)
+        for j in range(nk):
+            lo, hi = j * chunk, min((j + 1) * chunk, ff_dev)
+            size = max(hi - lo, 0)
+            if size < chunk:
+                msg_ref[j, :, k * chunk : (k + 1) * chunk] = jnp.zeros((rows, chunk), BF)
+            if size > 0:
+                msg_ref[j, :, k * chunk : k * chunk + size] = part[:, lo:hi].astype(BF)
+    for j in range(nk):
+        msg_ref[j, :, 2 * chunk :] = stat
+    for k, ref in enumerate(refs):
+        ref[...] = msg_ref[other("kv", k)]
+
+
+def base_kernel(rows_ref, gains_ref, wg_ref, wu_ref, m3, m2, m1, m0, msg_ref):
+    x = rows_ref[...].astype(F32)
+    left = (x * gains_ref[2:3, :]).astype(BF)
+    send_parts(left, wg_ref, wu_ref, [added(x, x)], (m0, m1, m2, m3), msg_ref)
+
+
 def gate_kernel(
-    half_ref, other_ref, rows_ref, gains_ref, wg_ref, wu_ref, m0, m1, m2, m3, post_ref, msg_ref
+    half_ref, other_ref, rows_ref, gains_ref, wg_ref, wu_ref, m3, m2, m1, m0, post_ref, msg_ref
 ):
-    nk, both, _ = msg_ref.shape
-    rows = both // 2
-    ff_dev = wg_ref.shape[0]
-    chunk = (msg_ref.shape[2] - 128) // 2
     first = lax.rem(lax.axis_index("tp"), 2) == 0
     mine, theirs = half_ref[...].astype(F32), other_ref[...].astype(F32)
     att = jnp.concatenate(
@@ -524,54 +561,31 @@
     x = rows_ref[...].astype(F32)
     post = att * gains_ref[1:2, :]
     post_ref[...] = post
-    gain = gains_ref[2:3, :]
-    stacked = jnp.concatenate([x * gain, post * gain], axis=0).astype(BF)
-
-    def added(a, b):
-        return jnp.sum(a * b, axis=1, keepdims=True)
-
-    top = terms(added(att, att), 2) + terms(added(x, post), 2)
-    low = terms(added(x, x), 2) + terms(added(post, post), 2)
-    stat = placed(
-        [(i, jnp.concatenate([a, b], axis=0)) for i, (a, b) in enumerate(zip(top, low))],
-        (both, 128),
-    ).astype(BF)
-    for k, w_ref in enumerate((wg_ref, wu_ref)):
-        part = lax.dot_general(stacked, w_ref[...], NT, preferred_element_type=F32)
-        for j in range(nk):
-            lo, hi = j * chunk, min((j + 1) * chunk, ff_dev)
-            size = max(hi - lo, 0)
-            if size < chunk:
-                msg_ref[j, :, k * chunk : (k + 1) * chunk] = jnp.zeros((both, chunk), BF)
-            if size > 0:
-                msg_ref[j, :, k * chunk : k * chunk + size] = part[:, lo:hi].astype(BF)
-    for j in range(nk):
-        msg_ref[j, :, 2 * chunk :] = stat
-    for k, ref in enumerate((m0, m1, m2, m3)):
-        ref[...] = msg_ref[other("kv", k)]
-
-
-def hidden_kernel(model_width, b0, b1, b2, b3, out_ref, s_ref):
-    rows, chunk = out_ref.shape
-    total = four((b0, b1, b2, b3))
+    left = (post * gains_ref[2:3, :]).astype(BF)
+    sums = [added(att, att), added(x, post), added(post, post)]
+    send_parts(left, wg_ref, wu_ref, sums, (m0, m1, m2, m3), msg_ref)
+
+
+def hidden_kernel(model_width, b0, b1, b2, b3, base_ref, out_ref, s_ref):
+    _, chunk = out_ref.shape
+    total, base = four((b0, b1, b2, b3)), base_ref[...]
     stat = total[:, 2 * chunk :]
-    one, two = picked(stat, 0, 2), picked(stat, 2, 2)
-    att_square, x_square, cross, post_square = one[:rows], one[rows:], two[:rows], two[rows:]
+    x_square = picked(base[:, 2 * chunk :], 0, 2)
+    att_square, cross, post_square = (picked(stat, 2 * i, 2) for i in range(3))
     s = lax.rsqrt(att_square / model_width + EPS)
     mid = jnp.maximum(x_square + 2.0 * s * cross + s * s * post_square, 0.0)
     scale = lax.rsqrt(mid / model_width + EPS)
     s_ref[...] = jnp.broadcast_to(s, s_ref.shape)
-    mixed = (total[:rows, : 2 * chunk] + s * total[rows:, : 2 * chunk]) * scale
+    mixed = (base[:, : 2 * chunk] + s * total[:, : 2 * chunk]) * scale
     gate, up = mixed[:, :chunk], mixed[:, chunk:]
     out_ref[...] = (gate / (1.0 + jnp.exp(-gate)) * up).astype(BF)
 
 
-def down_kernel(b0, b1, b2, b3, w_ref, msg_ref, held_ref):
-    nk, rows, chunk = held_ref.shape
+def down_kernel(b0, b1, b2, b3, w_ref, keep_ref, give_ref, held_ref, total_ref):
+    nk, _, chunk = held_ref.shape
     for k, ref in enumerate((b0, b1, b2, b3)):
         held_ref[other("kv", k)] = ref[...]
     ff_dev = w_ref.shape[0]
-    nt, own, _ = msg_ref.shape
     total = None
     for j in range(nk):
         lo, hi = j * chunk, min((j + 1) * chunk, ff_dev)
@@ -580,16 +594,23 @@
                 held_ref[j, :, : hi - lo], w_ref[lo:hi, :], preferred_element_type=F32
             )
             total = part if total is None else total + part
-    total = total.reshape(own, nt, total.shape[1])
-    for t in range(nt):
-        msg_ref[t] = total[:, t, :].astype(BF)
-
-
-def last_kernel(got_ref, resid_ref, post_ref, s_ref, out_ref):
-    nt, own, width = got_ref.shape
-    total = got_ref[0].astype(F32)
-    for t in range(1, nt):
-        total = total + got_ref[t].astype(F32)
+    total_ref[...] = total.reshape(total_ref.shape)
+    core = lax.rem(lax.axis_index("tp"), 2)
+    for k in range(keep_ref.shape[0]):
+        at = 2 * other("tp", k, 2)
+        keep_ref[k] = total_ref[:, at + core, :]
+        give_ref[k] = total_ref[:, at + 1 - core, :].astype(BF)
+
+
+def chips_kernel(keep_ref, got_ref, m3, m2, m1, m0):
+    for k, ref in enumerate((m0, m1, m2, m3)):
+        ref[...] = (keep_ref[k] + got_ref[k].astype(F32)).astype(BF)
+
+
+def last_kernel(b0, b1, b2, b3, resid_ref, post_ref, s_ref, out_ref):
+    own, width = resid_ref.shape
+    nt = post_ref.shape[0] // own
+    total = four((b0, b1, b2, b3))
     added = (post_ref[...] * s_ref[:, 0:1]).reshape(own, nt, width)
     here = lax.broadcasted_iota(jnp.int32, added.shape, 1) == lax.axis_index("tp")
     mine = jnp.sum(jnp.where(here, added, 0.0), axis=1)
@@ -603,10 +624,10 @@
 
 def deal(blocks, axis, step=1):
     size = lax.axis_size(axis)
-    return [blocks[0]] + [
-        lax.ppermute(blocks[k], axis, [(i, i ^ (k * step)) for i in range(size)])
-        for k in range(1, len(blocks))
-    ]
+    out = list(blocks)
+    for k in reversed(range(1, len(blocks))):
+        out[k] = lax.ppermute(blocks[k], axis, [(i, i ^ (k * step)) for i in range(size)])
+    return out
 
 
 def kernel_body(
@@ -646,23 +667,47 @@
     table[1] = np.tile(np.concatenate([-sin, sin]), heads)
 
     swap = [(i, i ^ 1) for i in range(nt)]
-    both = call(start_kernel, like((nt, width)), resid, lax.ppermute(resid, "tp", swap), flops=WAIT)
     chips = nt // 2
+    unit = call(unit_kernel, like((rope_dev, 2 * rope)), flops=WAIT)
+    value_dev = heads * value_up.shape[2]
+    key_flat = call(flat_kernel, like((latent, nope_dev)), key_up, flops=WAIT)
+    value_flat = call(flat_kernel, like((latent, value_dev)), value_up, flops=WAIT)
+    column = call(
+        start_kernel,
+        like((own * chips, width)),
+        *deal([resid] * chips, "tp", 2),
+        unit,
+        scratch=[pltpu.VMEM((chips, own, width), F32)],
+        flops=WAIT,
+    )
     sent_width = nope_dev + rope_dev + latent // 2 + 128
     *msg, x_rows, gains = call(
         query_kernel,
         [like((nt, sent_width))] * nk + [like((rows, width)), like((8, width), F32)],
-        *deal([both] * chips, "tp", 2),
+        column,
+        lax.ppermute(column, "tp", swap),
         resid,
         *[g.reshape(-1, 128) for g in (attn_gain, post_gain, mlp_gain)],
         w_query_nope,
         w_query_rope,
         w_latent,
         w_key_rope.T,
-        scratch=[pltpu.VMEM((chips, 2 * own, width), F32), pltpu.VMEM((nk, nt, sent_width), BF)],
+        scratch=[pltpu.VMEM((nk, nt, sent_width), BF)],
         flops=WAIT,
     )
     pairs = nt * heads
+    chunk = -(-ff_dev // (nk * 128)) * 128
+    wide = 2 * chunk + 128
+    base_parts = call(
+        base_kernel,
+        [like((rows, wide))] * nk,
+        x_rows,
+        gains,
+        w_gate.T,
+        w_up.T,
+        scratch=[pltpu.VMEM((nk, rows, wide), BF)],
+        flops=WAIT,
+    )[::-1]
     msg, new_latent, new_rope_key, own_block = call(
         functools.partial(latent_kernel, model_width),
         [
@@ -671,10 +716,11 @@
             like((own, rope)),
             like((nt, latent + 128), F32),
         ],
-        *deal(msg, "kv"),
-        key_up,
+        *deal(msg[::-1], "kv"),
+        key_flat,
         latent_gain.reshape(1, latent),
         jnp.asarray(table),
+        unit,
         flops=WAIT,
     )
     got = exchange(msg.reshape(nk * nt, heads, latent + 128), ("kv", "tp"))
@@ -688,19 +734,19 @@
         flops=WAIT,
     )
     got = exchange(msg.reshape(nk * nt, heads, latent + 128), ("kv", "tp"))
-    value_dev = heads * value_up.shape[2]
-    o_heads = call(
-        value_kernel,
-        like((nt, value_dev)),
+    msg = call(
+        functools.partial(value_kernel, heads),
+        [like((nt + rows, value_dev))] * nk,
         got.reshape(nk, pairs, latent + 128),
-        value_up,
+        value_flat,
+        *base_parts,
         flops=WAIT,
     )
     half = width // 2
-    keep, give = call(
+    keep, give, base = call(
         out_kernel,
-        [like((rows, half), F32), like((rows, half))],
-        *deal([o_heads] * nk, "kv"),
+        [like((rows, half), F32), like((rows, half)), like((rows, wide), F32)],
+        *deal(msg[::-1], "kv"),
         w_out,
         scratch=[pltpu.VMEM((nk, nt, value_dev), F32)],
         flops=WAIT,
@@ -708,40 +754,45 @@
     pair = call(
         pair_kernel, like((rows, half)), keep, lax.ppermute(give, "tp", swap), flops=WAIT
     )
-    att_half = call(
-        column_kernel, like((rows, half)), *deal([pair] * chips, "tp", 2), flops=WAIT
-    )
+    att_half = call(column_kernel, like((rows, half)), *deal([pair] * chips, "tp", 2), flops=WAIT)
     att_other = lax.ppermute(att_half, "tp", swap)
-    chunk = -(-ff_dev // (nk * 128)) * 128
-    sent_width = 2 * chunk + 128
     *msg, post = call(
         gate_kernel,
-        [like((2 * rows, sent_width))] * nk + [like((rows, width), F32)],
+        [like((rows, wide))] * nk + [like((rows, width), F32)],
         att_half,
         att_other,
         x_rows,
         gains,
         w_gate.T,
         w_up.T,
-        scratch=[pltpu.VMEM((nk, 2 * rows, sent_width), BF)],
+        scratch=[pltpu.VMEM((nk, rows, wide), BF)],
         flops=WAIT,
     )
     hidden, s = call(
         functools.partial(hidden_kernel, model_width),
         [like((rows, chunk)), like((rows, 128), F32)],
-        *deal(msg, "kv"),
-        flops=WAIT,
-    )
-    msg = call(
+        *deal(msg[::-1], "kv"),
+        base,
+        flops=WAIT,
+    )
+    keep, give = call(
         down_kernel,
-        like((nt, own, width)),
+        [like((chips, own, width), F32), like((chips, own, width))],
         *deal([hidden] * nk, "kv"),
         w_down,
-        scratch=[pltpu.VMEM((nk, rows, chunk), BF)],
-        flops=WAIT,
-    )
-    got = exchange(msg, "tp")
-    next_resid = call(last_kernel, like((own, width)), got, resid, post, s)
+        scratch=[pltpu.VMEM((nk, rows, chunk), BF), pltpu.VMEM((own, nt, width), F32)],
+        flops=WAIT,
+    )
+    msg = call(
+        chips_kernel,
+        [like((own, width))] * chips,
+        keep,
+        lax.ppermute(give, "tp", swap),
+        flops=WAIT,
+    )
+    next_resid = call(
+        last_kernel, like((own, width)), *deal(msg[::-1], "tp", 2), resid, post, s, flops=WAIT
+    )
     return (next_resid, new_latent, new_rope_key)
 
 
@@ -757,11 +808,14 @@
         and 2 * own == nt
         and width % 1024 == 0
         and latent % 256 == 0
+        and heads * args[8].shape[2] >= 2 * (-(-args[12].shape[1] // (nk * 128)) * 128) + 128
         and nope % 128 == 0
         and cache.shape[1] % 128 == 0
         and args[16].shape[2] == 64
     )
-    return kernel_body(*args) if fits else plain_body(*args)
+    if not fits:
+        return plain_body(*args)
+    return kernel_body(*args)
 
 
 def solution(mesh):

time: 95.9 us -> 97.8 us (1.020)
  blocking collectives: 37.5 us -> 14.2 us
  waiting for transfers between devices: 23.6 us -> 34.5 us
  starting transfers between devices: 25 us -> 31.8 us
  local copies, waits for them, and re-layouts: 0.78 us -> 5.55 us
  Pallas kernels: 7.9 us -> 10.6 us
    all_to_all x3 -> x1, blocking collectives: 37.5 us -> 14.2 us  [exchange(): return lax.all_to_all(message, axis, 0, 0, tiled=True)]
    all_to_all x0 -> x1, waiting for transfers between devices: none -> 6.09 us  [exchange(): return lax.all_to_all(message, axis, 0, 0, tiled=True)]
    unnamed x38 -> x42, local copies, waits for them, and re-layouts: 0.78 us -> 5.55 us
    ppermute x18 -> x21, starting transfers between devices: 24.3 us -> 28.9 us  [deal(): lax.ppermute(blocks[k], axis, [(i, i ^ k * step) for i in range(size)])]
    ppermute x18 -> x21, waiting for transfers between devices: 20.2 us -> 23.6 us  [deal(): lax.ppermute(blocks[k], axis, [(i, i ^ k * step) for i in range(size)])]
    pallas_call x12 -> x17, Pallas kernels: 7.9 us -> 10.6 us  [call(): pl.pallas_call(kernel, out_shape=outs, in_specs=[VMEM] * len(args), out_s...]
    all_to_all x0 -> x1, starting transfers between devices: none -> 2.59 us  [exchange(): return lax.all_to_all(message, axis, 0, 0, tiled=True)]
    ppermute x1 -> x2, waiting for transfers between devices: 1.19 us -> 2.39 us  [kernel_body(): lax.ppermute(give, 'tp', swap)]
  transfers between devices with their start and end apart: 21 -> 26, of which waited for: 18 -> 23; matrix products, arithmetic and copies ran while one was open for 0% -> 0% of each run, Pallas kernels for 0% -> 2%
where the time goes in v3:
time: 97.8 us; the launch traced here: 97.5 us
  waiting for transfers between devices  34.5 us (35%)
  starting transfers between devices  31.8 us (33%)
  blocking collectives  14.2 us (15%)
  Pallas kernels  10.6 us (11%)
  local copies, waits for them, and re-layouts  5.55 us (6%)
    ppermute x21, starting transfers between devices, deal(): lax.ppermute(blocks[k], axis, [(i, i ^ k * step) for i in range(size)])  28.9 us
    ppermute x21, waiting for transfers between devices, deal(): lax.ppermute(blocks[k], axis, [(i, i ^ k * step) for i in range(size)])  23.6 us
    all_to_all x1, blocking collectives, exchange(): return lax.all_to_all(message, axis, 0, 0, tiled=True)  14.2 us
    pallas_call x17, Pallas kernels, call(): pl.pallas_call(kernel, out_shape=outs, in_specs=[VMEM] * len(args), out_s...  10.6 us
    all_to_all x1, waiting for transfers between devices, exchange(): return lax.all_to_all(message, axis, 0, 0, tiled=True)  6.09 us
    unnamed x42, local copies, waits for them, and re-layouts  5.55 us
    all_to_all x1, starting transfers between devices, exchange(): return lax.all_to_all(message, axis, 0, 0, tiled=True)  2.59 us
    ppermute x2, waiting for transfers between devices, kernel_body(): lax.ppermute(give, 'tp', swap)  2.39 us
  transfers between devices with their start and end apart: 26, of which 23 were waited for; matrix products, arithmetic and copies ran while one was open for 0% of the time, Pallas kernels for 2%

profile of v3, /device:TPU:0, one launch (start us, length us, event | category | flops | bytes accessed | tf_op | source)
XLA Modules:
  0.0 97.5 jit_solution(13140531859429178515)
XLA Ops:
  0.6 5.1 %collective-permute-start.2 = (bf16[4,1024]{1,0:T(4,128)(2,1)}, bf16[4,1024]{1,0:T(4,128)(2,1)S(1)}, u32[]{:S(2)}, u32[]{:S(2)}) collective-permute-start(bf16[4,1024]{1,0:T(4,128)(2,1)} %resid_ref.3), channel_id=1, source_target_pairs={{0,6},{1,7},{2,4},{3,5},{4,2},{5,3},{6,0},{7,1},{8,14},{9,15},{10,... | collective-permute-start | bytes 24584 | tf_op jit(solution)/shard_map/ppermute | solution.py:629
  7.6 2.9 %collective-permute-done.1.b2 = bf16[4,1024]{1,0:T(4,128)(2,1)S(1)} collective-permute-done((bf16[4,1024]{1,0:T(4,128)(2,1)}, bf16[4,1024]{1,0:T(4,128)(2,1)S(1)}, u32[]{:S(2)}, u32[]{:S(2)}) %collective-permute-start.1) | collective-permute-done | bytes 8224 | tf_op jit(solution)/shard_map/ppermute | solution.py:629
  12.7 1.6 %collective-permute-start.4 = (bf16[8,1920]{1,0:T(8,128)(2,1)S(1)}, bf16[8,1920]{1,0:T(8,128)(2,1)S(1)}, u32[]{:S(2)}, u32[]{:S(2)}) collective-permute-start(bf16[8,1920]{1,0:T(8,128)(2,1)S(1)} %get-tuple-element.38), channel_id=1, source_target_pairs={{0,8},{8,0},{16,24},{24,16},{1,9},{9,1},{17,25},{25,17},{2,10},{10... | collective-permute-start | bytes 92168 | tf_op jit(solution)/shard_map/ppermute | solution.py:629
  14.3 1.5 %collective-permute-start.5 = (bf16[8,1920]{1,0:T(8,128)(2,1)S(1)}, bf16[8,1920]{1,0:T(8,128)(2,1)S(1)}, u32[]{:S(2)}, u32[]{:S(2)}) collective-permute-start(bf16[8,1920]{1,0:T(8,128)(2,1)S(1)} %get-tuple-element.39), channel_id=1, source_target_pairs={{0,16},{8,24},{16,0},{24,8},{1,17},{9,25},{17,1},{25,9},{2,18},{10... | collective-permute-start | bytes 92168 | tf_op jit(solution)/shard_map/ppermute | solution.py:629
  16.7 1.5 %collective-permute-done.5.b2 = bf16[8,1920]{1,0:T(8,128)(2,1)S(1)} collective-permute-done((bf16[8,1920]{1,0:T(8,128)(2,1)S(1)}, bf16[8,1920]{1,0:T(8,128)(2,1)S(1)}, u32[]{:S(2)}, u32[]{:S(2)}) %collective-permute-start.5) | collective-permute-done | bytes 30752 | tf_op jit(solution)/shard_map/ppermute | solution.py:629
  18.2 2.4 %collective-permute-done.6.b3 = bf16[8,1920]{1,0:T(8,128)(2,1)S(1)} collective-permute-done((bf16[8,1920]{1,0:T(8,128)(2,1)S(1)}, bf16[8,1920]{1,0:T(8,128)(2,1)S(1)}, u32[]{:S(2)}, u32[]{:S(2)}) %collective-permute-start.6) | collective-permute-done | bytes 30752 | tf_op jit(solution)/shard_map/ppermute | solution.py:629
  21.6 14.2 %all_to_all.10 = bf16[32,8,640]{2,1,0:T(8,128)(2,1)S(1)} all-to-all(bf16[32,8,640]{2,1,0:T(8,128)(2,1)S(1)} %bitcast.12), channel_id=1, replica_groups=mesh['kv'=4,'tp'=8] {'kv','tp'}, dimensions={0} | all-to-all | bytes 655360 | tf_op jit(solution)/shard_map/all_to_all | solution.py:622
  35.8 2.6 %shard_map.198 = bf16[4,64,640]{2,1,0:T(8,128)(2,1)} custom-call(bf16[4,64,640]{2,1,0:T(8,128)(2,1)S(1)} %bitcast.13, bf16[4,512,512]{2,1,0:T(8,128)(2,1)S(1)} %copy-done.5, bf16[4,64,512]{2,1,0:T(8,128)(2,1)S(1)} %bitcast.19, f32[8,640]{1,0:T(8,128)S(1)} %get-tuple-element.42.own_ref), custom_call_target="tpu_custom_call" | custom-call | flops 4000000000 | bytes 3035136 | tf_op jit(solution)/shard_map/pallas_call | solution.py:273
  38.5 2.6 %all-to-all-start.1 = ((bf16[32,8,640]{2,1,0:T(8,128)(2,1)}), bf16[32,8,640]{2,1,0:T(8,128)(2,1)S(1)}, u32[]{:S(2)}, u32[]{:S(2)}) async-start(bf16[32,8,640]{2,1,0:T(8,128)(2,1)} %bitcast.7), calls=%async_computation.1 | async-start | bytes 655360 | tf_op jit(solution)/shard_map/all_to_all | solution.py:622
  45.3 1.7 %shard_map.200 = (bf16[32,896]{1,0:T(8,128)(2,1)S(1)}, bf16[32,896]{1,0:T(8,128)(2,1)S(1)}, bf16[32,896]{1,0:T(8,128)(2,1)S(1)}, bf16[32,896]{1,0:T(8,128)(2,1)S(1)}) custom-call(bf16[32,1024]{1,0:T(8,128)(2,1)S(1)} %get-tuple-element.43.rows_ref, f32[8,1024]{1,0:T(8,128)S(1)} %get-tuple-element.44.gains_ref, bf16[1376,1024]{1,0:T(8,128)(2,1)S(1)} %bitcast.14, ...), custom_call_target="tpu_custom_call" | custom-call | flops 4000000000 | bytes 5963776 | tf_op jit(solution)/shard_map/pallas_call | solution.py:273
  47.0 6.1 %all-to-all-done.1 = bf16[32,8,640]{2,1,0:T(8,128)(2,1)S(1)} async-done(((bf16[32,8,640]{2,1,0:T(8,128)(2,1)}), bf16[32,8,640]{2,1,0:T(8,128)(2,1)S(1)}, u32[]{:S(2)}, u32[]{:S(2)}) %all-to-all-start.1) | async-done | bytes 327712 | tf_op jit(solution)/shard_map/all_to_all | solution.py:622
  56.0 2.3 %collective-permute-start.9 = (bf16[40,1024]{1,0:T(8,128)(2,1)S(1)}, bf16[40,1024]{1,0:T(8,128)(2,1)S(1)}, u32[]{:S(2)}, u32[]{:S(2)}) collective-permute-start(bf16[40,1024]{1,0:T(8,128)(2,1)S(1)} %get-tuple-element.52), channel_id=1, source_target_pairs={{0,24},{8,16},{16,8},{24,0},{1,25},{9,17},{17,9},{25,1},{2,26},{10... | collective-permute-start | bytes 245768 | tf_op jit(solution)/shard_map/ppermute | solution.py:629
  59.3 2.3 %collective-permute-done.8.b2 = bf16[40,1024]{1,0:T(8,128)(2,1)S(1)} collective-permute-done((bf16[40,1024]{1,0:T(8,128)(2,1)S(1)}, bf16[40,1024]{1,0:T(8,128)(2,1)S(1)}, u32[]{:S(2)}, u32[]{:S(2)}) %collective-permute-start.8) | collective-permute-done | bytes 81952 | tf_op jit(solution)/shard_map/ppermute | solution.py:629
  63.4 1.5 %collective-permute-start.13 = (bf16[32,512]{1,0:T(8,128)(2,1)S(1)}, bf16[32,512]{1,0:T(8,128)(2,1)S(1)}, u32[]{:S(2)}, u32[]{:S(2)}) collective-permute-start(bf16[32,512]{1,0:T(8,128)(2,1)S(1)} %shard_map.203.b0), channel_id=1, source_target_pairs={{0,6},{1,7},{2,4},{3,5},{4,2},{5,3},{6,0},{7,1},{8,14},{9,15},{10,... | collective-permute-start | bytes 98312 | tf_op jit(solution)/shard_map/ppermute | solution.py:629
  65.0 2.8 %collective-permute-start.11 = (bf16[32,512]{1,0:T(8,128)(2,1)S(1)}, bf16[32,512]{1,0:T(8,128)(2,1)S(1)}, u32[]{:S(2)}, u32[]{:S(2)}) collective-permute-start(bf16[32,512]{1,0:T(8,128)(2,1)S(1)} %shard_map.203.b0), channel_id=1, source_target_pairs={{0,2},{1,3},{2,0},{3,1},{4,6},{5,7},{6,4},{7,5},{8,10},{9,11},{10,... | collective-permute-start | bytes 98312 | tf_op jit(solution)/shard_map/ppermute | solution.py:629
  67.9 1.3 %collective-permute-done.13.b3 = bf16[32,512]{1,0:T(8,128)(2,1)S(1)} collective-permute-done((bf16[32,512]{1,0:T(8,128)(2,1)S(1)}, bf16[32,512]{1,0:T(8,128)(2,1)S(1)}, u32[]{:S(2)}, u32[]{:S(2)}) %collective-permute-start.13) | collective-permute-done | bytes 32800 | tf_op jit(solution)/shard_map/ppermute | solution.py:629
  71.6 1.7 %shard_map.205 = (bf16[32,896]{1,0:T(8,128)(2,1)S(1)}, bf16[32,896]{1,0:T(8,128)(2,1)S(1)}, bf16[32,896]{1,0:T(8,128)(2,1)S(1)}, bf16[32,896]{1,0:T(8,128)(2,1)S(1)}, f32[32,1024]{1,0:T(8,128)S(1)}) custom-call(bf16[32,512]{1,0:T(8,128)(2,1)S(1)} %shard_map.204.half_ref, bf16[32,512]{1,0:T(8,128)(2,1)S(1)} %collective-permute-done.14.other_ref, ...), custom_call_target="tpu_custom_call" | custom-call | flops 4000000000 | bytes 6160384 | tf_op jit(solution)/shard_map/pallas_call | solution.py:273
  75.4 1.4 %collective-permute-start.17 = (bf16[32,896]{1,0:T(8,128)(2,1)S(1)}, bf16[32,896]{1,0:T(8,128)(2,1)S(1)}, u32[]{:S(2)}, u32[]{:S(2)}) collective-permute-start(bf16[32,896]{1,0:T(8,128)(2,1)S(1)} %get-tuple-element.58), channel_id=1, source_target_pairs={{0,24},{8,16},{16,8},{24,0},{1,25},{9,17},{17,9},{25,1},{2,26},{10... | collective-permute-start | bytes 172040 | tf_op jit(solution)/shard_map/ppermute | solution.py:629
  78.4 2.1 %collective-permute-done.17.b3 = bf16[32,896]{1,0:T(8,128)(2,1)S(1)} collective-permute-done((bf16[32,896]{1,0:T(8,128)(2,1)S(1)}, bf16[32,896]{1,0:T(8,128)(2,1)S(1)}, u32[]{:S(2)}, u32[]{:S(2)}) %collective-permute-start.17) | collective-permute-done | bytes 57376 | tf_op jit(solution)/shard_map/ppermute | solution.py:629
  80.6 1.5 %collective-permute-start.20 = (bf16[32,384]{1,0:T(8,128)(2,1)S(1)}, bf16[32,384]{1,0:T(8,128)(2,1)S(1)}, u32[]{:S(2)}, u32[]{:S(2)}) collective-permute-start(bf16[32,384]{1,0:T(8,128)(2,1)S(1)} %get-tuple-element.60.b0), channel_id=1, source_target_pairs={{0,24},{8,16},{16,8},{24,0},{1,25},{9,17},{17,9},{25,1},{2,26},{10... | collective-permute-start | bytes 73736 | tf_op jit(solution)/shard_map/ppermute | solution.py:629
  88.9 1.5 %collective-permute-start.22 = (bf16[4,1024]{1,0:T(4,128)(2,1)S(1)}, bf16[4,1024]{1,0:T(4,128)(2,1)S(1)}, u32[]{:S(2)}, u32[]{:S(2)}) collective-permute-start(bf16[4,1024]{1,0:T(4,128)(2,1)S(1)} %get-tuple-element.64), channel_id=1, source_target_pairs={{0,2},{1,3},{2,0},{3,1},{4,6},{5,7},{6,4},{7,5},{8,10},{9,11},{10,... | collective-permute-start | bytes 24584 | tf_op jit(solution)/shard_map/ppermute | solution.py:629
  91.3 2.1 %collective-permute-start.24 = (bf16[4,1024]{1,0:T(4,128)(2,1)S(1)}, bf16[4,1024]{1,0:T(4,128)(2,1)S(1)}, u32[]{:S(2)}, u32[]{:S(2)}) collective-permute-start(bf16[4,1024]{1,0:T(4,128)(2,1)S(1)} %get-tuple-element.66), channel_id=1, source_target_pairs={{0,6},{1,7},{2,4},{3,5},{4,2},{5,3},{6,0},{7,1},{8,14},{9,15},{10,... | collective-permute-start | bytes 24584 | tf_op jit(solution)/shard_map/ppermute | solution.py:629
  93.4 1.6 %collective-permute-done.23.b2 = bf16[4,1024]{1,0:T(4,128)(2,1)S(1)} collective-permute-done((bf16[4,1024]{1,0:T(4,128)(2,1)S(1)}, bf16[4,1024]{1,0:T(4,128)(2,1)S(1)}, u32[]{:S(2)}, u32[]{:S(2)}) %collective-permute-start.23) | collective-permute-done | bytes 8224 | tf_op jit(solution)/shard_map/ppermute | solution.py:629
  95.0 1.8 %collective-permute-done.24.b3 = bf16[4,1024]{1,0:T(4,128)(2,1)S(1)} collective-permute-done((bf16[4,1024]{1,0:T(4,128)(2,1)S(1)}, bf16[4,1024]{1,0:T(4,128)(2,1)S(1)}, u32[]{:S(2)}, u32[]{:S(2)}) %collective-permute-start.24) | collective-permute-done | bytes 8224 | tf_op jit(solution)/shard_map/ppermute | solution.py:629
  (89 shorter events, 30.4 us)
Async XLA Ops:
  0.6 7.0 %collective-permute-start.2 = (bf16[4,1024]{1,0:T(4,128)(2,1)}, bf16[4,1024]{1,0:T(4,128)(2,1)S(1)}, u32[]{:S(2)}, u32[]{:S(2)}) collective-permute-start(bf16[4,1024]{1,0:T(4,128)(2,1)} %resid_ref.3), channel_id=1, source_target_pairs={{0,6},{1,7},{2,4},{3,5},{4,2},{5,3},{6,0},{7,1},{8,14},{9,15},{10,... | collective-permute-start | bytes 24584 | tf_op jit(solution)/shard_map/ppermute | solution.py:629
  5.8 4.8 %collective-permute-start.1 = (bf16[4,1024]{1,0:T(4,128)(2,1)}, bf16[4,1024]{1,0:T(4,128)(2,1)S(1)}, u32[]{:S(2)}, u32[]{:S(2)}) collective-permute-start(bf16[4,1024]{1,0:T(4,128)(2,1)} %resid_ref.3), channel_id=1, source_target_pairs={{0,4},{1,5},{2,6},{3,7},{4,0},{5,1},{6,2},{7,3},{8,12},{9,13},{10,... | collective-permute-start | bytes 24584 | tf_op jit(solution)/shard_map/ppermute | solution.py:629
  5.8 4.8 %collective-permute-start = (bf16[4,1024]{1,0:T(4,128)(2,1)}, bf16[4,1024]{1,0:T(4,128)(2,1)S(1)}, u32[]{:S(2)}, u32[]{:S(2)}) collective-permute-start(bf16[4,1024]{1,0:T(4,128)(2,1)} %resid_ref.3), channel_id=1, source_target_pairs={{0,2},{1,3},{2,0},{3,1},{4,6},{5,7},{6,4},{7,5},{8,10},{9,11},{10,... | collective-permute-start | bytes 24584 | tf_op jit(solution)/shard_map/ppermute | solution.py:629
  10.6 1.3 %collective-permute-start.3 = (bf16[16,1024]{1,0:T(8,128)(2,1)S(1)}, bf16[16,1024]{1,0:T(8,128)(2,1)S(1)}, u32[]{:S(2)}, u32[]{:S(2)}) collective-permute-start(bf16[16,1024]{1,0:T(8,128)(2,1)S(1)} %shard_map.194.half_ref), channel_id=1, source_target_pairs={{0,1},{1,0},{2,3},{3,2},{4,5},{5,4},{6,7},{7,6},{8,9},{9,8},{10,11... | collective-permute-start | bytes 98312 | tf_op jit(solution)/shard_map/ppermute | solution.py:688
  12.7 4.0 %collective-permute-start.4 = (bf16[8,1920]{1,0:T(8,128)(2,1)S(1)}, bf16[8,1920]{1,0:T(8,128)(2,1)S(1)}, u32[]{:S(2)}, u32[]{:S(2)}) collective-permute-start(bf16[8,1920]{1,0:T(8,128)(2,1)S(1)} %get-tuple-element.38), channel_id=1, source_target_pairs={{0,8},{8,0},{16,24},{24,16},{1,9},{9,1},{17,25},{25,17},{2,10},{10... | collective-permute-start | bytes 92168 | tf_op jit(solution)/shard_map/ppermute | solution.py:629
  14.3 3.9 %collective-permute-start.5 = (bf16[8,1920]{1,0:T(8,128)(2,1)S(1)}, bf16[8,1920]{1,0:T(8,128)(2,1)S(1)}, u32[]{:S(2)}, u32[]{:S(2)}) collective-permute-start(bf16[8,1920]{1,0:T(8,128)(2,1)S(1)} %get-tuple-element.39), channel_id=1, source_target_pairs={{0,16},{8,24},{16,0},{24,8},{1,17},{9,25},{17,1},{25,9},{2,18},{10... | collective-permute-start | bytes 92168 | tf_op jit(solution)/shard_map/ppermute | solution.py:629
  15.8 4.8 %collective-permute-start.6 = (bf16[8,1920]{1,0:T(8,128)(2,1)S(1)}, bf16[8,1920]{1,0:T(8,128)(2,1)S(1)}, u32[]{:S(2)}, u32[]{:S(2)}) collective-permute-start(bf16[8,1920]{1,0:T(8,128)(2,1)S(1)} %get-tuple-element.40), channel_id=1, source_target_pairs={{0,24},{8,16},{16,8},{24,0},{1,25},{9,17},{17,9},{25,1},{2,26},{10... | collective-permute-start | bytes 92168 | tf_op jit(solution)/shard_map/ppermute | solution.py:629
  38.5 14.6 %all-to-all-start.1 = ((bf16[32,8,640]{2,1,0:T(8,128)(2,1)}), bf16[32,8,640]{2,1,0:T(8,128)(2,1)S(1)}, u32[]{:S(2)}, u32[]{:S(2)}) async-start(bf16[32,8,640]{2,1,0:T(8,128)(2,1)} %bitcast.7), calls=%async_computation.1 | async-start | bytes 655360 | tf_op jit(solution)/shard_map/all_to_all | solution.py:622
  54.7 4.5 %collective-permute-start.7 = (bf16[40,1024]{1,0:T(8,128)(2,1)S(1)}, bf16[40,1024]{1,0:T(8,128)(2,1)S(1)}, u32[]{:S(2)}, u32[]{:S(2)}) collective-permute-start(bf16[40,1024]{1,0:T(8,128)(2,1)S(1)} %get-tuple-element.50), channel_id=1, source_target_pairs={{0,8},{8,0},{16,24},{24,16},{1,9},{9,1},{17,25},{25,17},{2,10},{10... | collective-permute-start | bytes 245768 | tf_op jit(solution)/shard_map/ppermute | solution.py:629
  54.8 6.8 %collective-permute-start.8 = (bf16[40,1024]{1,0:T(8,128)(2,1)S(1)}, bf16[40,1024]{1,0:T(8,128)(2,1)S(1)}, u32[]{:S(2)}, u32[]{:S(2)}) collective-permute-start(bf16[40,1024]{1,0:T(8,128)(2,1)S(1)} %get-tuple-element.51), channel_id=1, source_target_pairs={{0,16},{8,24},{16,0},{24,8},{1,17},{9,25},{17,1},{25,9},{2,18},{10... | collective-permute-start | bytes 245768 | tf_op jit(solution)/shard_map/ppermute | solution.py:629
  56.0 5.6 %collective-permute-start.9 = (bf16[40,1024]{1,0:T(8,128)(2,1)S(1)}, bf16[40,1024]{1,0:T(8,128)(2,1)S(1)}, u32[]{:S(2)}, u32[]{:S(2)}) collective-permute-start(bf16[40,1024]{1,0:T(8,128)(2,1)S(1)} %get-tuple-element.52), channel_id=1, source_target_pairs={{0,24},{8,16},{16,8},{24,0},{1,25},{9,17},{17,9},{25,1},{2,26},{10... | collective-permute-start | bytes 245768 | tf_op jit(solution)/shard_map/ppermute | solution.py:629
  63.4 5.8 %collective-permute-start.13 = (bf16[32,512]{1,0:T(8,128)(2,1)S(1)}, bf16[32,512]{1,0:T(8,128)(2,1)S(1)}, u32[]{:S(2)}, u32[]{:S(2)}) collective-permute-start(bf16[32,512]{1,0:T(8,128)(2,1)S(1)} %shard_map.203.b0), channel_id=1, source_target_pairs={{0,6},{1,7},{2,4},{3,5},{4,2},{5,3},{6,0},{7,1},{8,14},{9,15},{10,... | collective-permute-start | bytes 98312 | tf_op jit(solution)/shard_map/ppermute | solution.py:629
  64.9 5.2 %collective-permute-start.12 = (bf16[32,512]{1,0:T(8,128)(2,1)S(1)}, bf16[32,512]{1,0:T(8,128)(2,1)S(1)}, u32[]{:S(2)}, u32[]{:S(2)}) collective-permute-start(bf16[32,512]{1,0:T(8,128)(2,1)S(1)} %shard_map.203.b0), channel_id=1, source_target_pairs={{0,4},{1,5},{2,6},{3,7},{4,0},{5,1},{6,2},{7,3},{8,12},{9,13},{10,... | collective-permute-start | bytes 98312 | tf_op jit(solution)/shard_map/ppermute | solution.py:629
  65.0 5.3 %collective-permute-start.11 = (bf16[32,512]{1,0:T(8,128)(2,1)S(1)}, bf16[32,512]{1,0:T(8,128)(2,1)S(1)}, u32[]{:S(2)}, u32[]{:S(2)}) collective-permute-start(bf16[32,512]{1,0:T(8,128)(2,1)S(1)} %shard_map.203.b0), channel_id=1, source_target_pairs={{0,2},{1,3},{2,0},{3,1},{4,6},{5,7},{6,4},{7,5},{8,10},{9,11},{10,... | collective-permute-start | bytes 98312 | tf_op jit(solution)/shard_map/ppermute | solution.py:629
  70.4 1.3 %collective-permute-start.14 = (bf16[32,512]{1,0:T(8,128)(2,1)S(1)}, bf16[32,512]{1,0:T(8,128)(2,1)S(1)}, u32[]{:S(2)}, u32[]{:S(2)}) collective-permute-start(bf16[32,512]{1,0:T(8,128)(2,1)S(1)} %shard_map.204.half_ref), channel_id=1, source_target_pairs={{0,1},{1,0},{2,3},{3,2},{4,5},{5,4},{6,7},{7,6},{8,9},{9,8},{10,11... | collective-permute-start | bytes 98312 | tf_op jit(solution)/shard_map/ppermute | solution.py:758
  73.3 4.2 %collective-permute-start.15 = (bf16[32,896]{1,0:T(8,128)(2,1)S(1)}, bf16[32,896]{1,0:T(8,128)(2,1)S(1)}, u32[]{:S(2)}, u32[]{:S(2)}) collective-permute-start(bf16[32,896]{1,0:T(8,128)(2,1)S(1)} %get-tuple-element.56), channel_id=1, source_target_pairs={{0,8},{8,0},{16,24},{24,16},{1,9},{9,1},{17,25},{25,17},{2,10},{10... | collective-permute-start | bytes 172040 | tf_op jit(solution)/shard_map/ppermute | solution.py:629
  74.3 4.2 %collective-permute-start.16 = (bf16[32,896]{1,0:T(8,128)(2,1)S(1)}, bf16[32,896]{1,0:T(8,128)(2,1)S(1)}, u32[]{:S(2)}, u32[]{:S(2)}) collective-permute-start(bf16[32,896]{1,0:T(8,128)(2,1)S(1)} %get-tuple-element.57), channel_id=1, source_target_pairs={{0,16},{8,24},{16,0},{24,8},{1,17},{9,25},{17,1},{25,9},{2,18},{10... | collective-permute-start | bytes 172040 | tf_op jit(solution)/shard_map/ppermute | solution.py:629
  75.4 5.1 %collective-permute-start.17 = (bf16[32,896]{1,0:T(8,128)(2,1)S(1)}, bf16[32,896]{1,0:T(8,128)(2,1)S(1)}, u32[]{:S(2)}, u32[]{:S(2)}) collective-permute-start(bf16[32,896]{1,0:T(8,128)(2,1)S(1)} %get-tuple-element.58), channel_id=1, source_target_pairs={{0,24},{8,16},{16,8},{24,0},{1,25},{9,17},{17,9},{25,1},{2,26},{10... | collective-permute-start | bytes 172040 | tf_op jit(solution)/shard_map/ppermute | solution.py:629
  80.6 4.8 %collective-permute-start.20 = (bf16[32,384]{1,0:T(8,128)(2,1)S(1)}, bf16[32,384]{1,0:T(8,128)(2,1)S(1)}, u32[]{:S(2)}, u32[]{:S(2)}) collective-permute-start(bf16[32,384]{1,0:T(8,128)(2,1)S(1)} %get-tuple-element.60.b0), channel_id=1, source_target_pairs={{0,24},{8,16},{16,8},{24,0},{1,25},{9,17},{17,9},{25,1},{2,26},{10... | collective-permute-start | bytes 73736 | tf_op jit(solution)/shard_map/ppermute | solution.py:629
  82.1 3.8 %collective-permute-start.19 = (bf16[32,384]{1,0:T(8,128)(2,1)S(1)}, bf16[32,384]{1,0:T(8,128)(2,1)S(1)}, u32[]{:S(2)}, u32[]{:S(2)}) collective-permute-start(bf16[32,384]{1,0:T(8,128)(2,1)S(1)} %get-tuple-element.60.b0), channel_id=1, source_target_pairs={{0,16},{8,24},{16,0},{24,8},{1,17},{9,25},{17,1},{25,9},{2,18},{10... | collective-permute-start | bytes 73736 | tf_op jit(solution)/shard_map/ppermute | solution.py:629
  83.1 3.8 %collective-permute-start.18 = (bf16[32,384]{1,0:T(8,128)(2,1)S(1)}, bf16[32,384]{1,0:T(8,128)(2,1)S(1)}, u32[]{:S(2)}, u32[]{:S(2)}) collective-permute-start(bf16[32,384]{1,0:T(8,128)(2,1)S(1)} %get-tuple-element.60.b0), channel_id=1, source_target_pairs={{0,8},{8,0},{16,24},{24,16},{1,9},{9,1},{17,25},{25,17},{2,10},{10... | collective-permute-start | bytes 73736 | tf_op jit(solution)/shard_map/ppermute | solution.py:629
  88.9 4.5 %collective-permute-start.22 = (bf16[4,1024]{1,0:T(4,128)(2,1)S(1)}, bf16[4,1024]{1,0:T(4,128)(2,1)S(1)}, u32[]{:S(2)}, u32[]{:S(2)}) collective-permute-start(bf16[4,1024]{1,0:T(4,128)(2,1)S(1)} %get-tuple-element.64), channel_id=1, source_target_pairs={{0,2},{1,3},{2,0},{3,1},{4,6},{5,7},{6,4},{7,5},{8,10},{9,11},{10,... | collective-permute-start | bytes 24584 | tf_op jit(solution)/shard_map/ppermute | solution.py:629
  90.4 4.6 %collective-permute-start.23 = (bf16[4,1024]{1,0:T(4,128)(2,1)S(1)}, bf16[4,1024]{1,0:T(4,128)(2,1)S(1)}, u32[]{:S(2)}, u32[]{:S(2)}) collective-permute-start(bf16[4,1024]{1,0:T(4,128)(2,1)S(1)} %get-tuple-element.65), channel_id=1, source_target_pairs={{0,4},{1,5},{2,6},{3,7},{4,0},{5,1},{6,2},{7,3},{8,12},{9,13},{10,... | collective-permute-start | bytes 24584 | tf_op jit(solution)/shard_map/ppermute | solution.py:629
  91.3 5.4 %collective-permute-start.24 = (bf16[4,1024]{1,0:T(4,128)(2,1)S(1)}, bf16[4,1024]{1,0:T(4,128)(2,1)S(1)}, u32[]{:S(2)}, u32[]{:S(2)}) collective-permute-start(bf16[4,1024]{1,0:T(4,128)(2,1)S(1)} %get-tuple-element.66), channel_id=1, source_target_pairs={{0,6},{1,7},{2,4},{3,5},{4,2},{5,3},{6,0},{7,1},{8,14},{9,15},{10,... | collective-permute-start | bytes 24584 | tf_op jit(solution)/shard_map/ppermute | solution.py:629
  (23 other events, 121.0 us)

commit v4 on v3

--- a/solution.py
+++ b/solution.py
@@ -453,25 +453,37 @@
     rope = rope_ref.shape[1]
     holds_own = lax.axis_index("kv") == 0
     lat, key = own_ref[:, :latent], own_ref[:, latent : latent + rope]
-    for r in range(own):
-        q_lat = q_ref[r, :, :latent]
-        q_rope = q_ref[r, :, latent : latent + rope]
-        keys = cache_ref[r]
-        scores = (
-            lax.dot_general(q_lat, keys, NT, preferred_element_type=F32)
-            + jnp.dot(q_rope, rope_ref[r], preferred_element_type=F32)
-        ) * score_scale
-        own_score = (
-            jnp.sum(q_lat.astype(F32) * lat[r : r + 1], axis=1, keepdims=True)
-            + jnp.sum(q_rope.astype(F32) * key[r : r + 1], axis=1, keepdims=True)
-        ) * score_scale
-        peak = jnp.maximum(jnp.max(scores, axis=1, keepdims=True), own_score)
-        probs = jnp.exp(scores - peak)
-        own_prob = jnp.where(holds_own, jnp.exp(own_score - peak), 0.0)
-        total = jnp.sum(probs, axis=1, keepdims=True) + own_prob
-        value = jnp.dot(probs.astype(BF), keys, preferred_element_type=F32)
-        msg_ref[r, :, :latent] = (value + own_prob * lat[r : r + 1]).astype(BF)
-        columns = list(enumerate(terms(peak, 3) + terms(total, 3)))
+    seqs = range(own)
+    q_lat = [q_ref[r, :, :latent] for r in seqs]
+    q_rope = [q_ref[r, :, latent : latent + rope] for r in seqs]
+    scores = [
+        (
+            lax.dot_general(q_lat[r], cache_ref[r], NT, preferred_element_type=F32)
+            + jnp.dot(q_rope[r], rope_ref[r], preferred_element_type=F32)
+        )
+        * score_scale
+        for r in seqs
+    ]
+    own_scores = [
+        (
+            jnp.sum(q_lat[r].astype(F32) * lat[r : r + 1], axis=1, keepdims=True)
+            + jnp.sum(q_rope[r].astype(F32) * key[r : r + 1], axis=1, keepdims=True)
+        )
+        * score_scale
+        for r in seqs
+    ]
+    peaks = [
+        jnp.maximum(jnp.max(scores[r], axis=1, keepdims=True), own_scores[r]) for r in seqs
+    ]
+    probs = [jnp.exp(scores[r] - peaks[r]) for r in seqs]
+    values = [
+        jnp.dot(probs[r].astype(BF), cache_ref[r], preferred_element_type=F32) for r in seqs
+    ]
+    for r in seqs:
+        own_prob = jnp.where(holds_own, jnp.exp(own_scores[r] - peaks[r]), 0.0)
+        total = jnp.sum(probs[r], axis=1, keepdims=True) + own_prob
+        msg_ref[r, :, :latent] = (values[r] + own_prob * lat[r : r + 1]).astype(BF)
+        columns = list(enumerate(terms(peaks[r], 3) + terms(total, 3)))
         msg_ref[r, :, latent:] = placed(columns, (all_heads, 128)).astype(BF)
 
 
@@ -493,18 +505,23 @@
     lane = lax.broadcasted_iota(jnp.int32, shape, 2)
     keep = (lane >= head * size) & (lane < (head + 1) * size)
     o_heads = jnp.sum(jnp.where(keep, full.reshape(shape), 0.0), axis=1).astype(BF)
+    rows, wide = a0.shape
     for a, m in ((a3, m3), (a2, m2), (a1, m1), (a0, m0)):
-        m[:nt] = o_heads
-        m[nt:, : a.shape[1]] = a[...]
+        m[:, :value_dev] = o_heads
+        for g in range(rows // nt):
+            m[:, value_dev + g * wide : value_dev + (g + 1) * wide] = a[g * nt : (g + 1) * nt]
 
 
 def out_kernel(b0, b1, b2, b3, w_ref, keep_ref, give_ref, base_ref, held_ref):
     half = keep_ref.shape[1]
-    nt, wide = held_ref.shape[1], base_ref.shape[1]
+    _, nt, value_dev = held_ref.shape
+    rows, wide = base_ref.shape
     for k, ref in enumerate((b0, b1, b2, b3)):
-        held_ref[other("kv", k)] = ref[:nt].astype(F32)
-    a, b, c, d = (ref[nt:, :wide].astype(F32) for ref in (b0, b1, b2, b3))
-    base_ref[...] = (a + b) + (c + d)
+        held_ref[other("kv", k)] = ref[:, :value_dev].astype(F32)
+    for g in range(rows // nt):
+        lo = value_dev + g * wide
+        a, b, c, d = (ref[:, lo : lo + wide].astype(F32) for ref in (b0, b1, b2, b3))
+        base_ref[g * nt : (g + 1) * nt] = (a + b) + (c + d)
     first = lax.rem(lax.axis_index("tp"), 2) == 0
     o_heads = held_ref[...].reshape(keep_ref.shape[0], w_ref.shape[0]).astype(BF)
     out = jnp.dot(o_heads, w_ref[...], preferred_element_type=F32)
@@ -524,13 +541,13 @@
     return jnp.sum(a * b, axis=1, keepdims=True)
 
 
-def send_parts(left, wg_ref, wu_ref, sums, refs, msg_ref):
+def send_parts(parts, sums, refs, msg_ref):
     nk, rows, wide = msg_ref.shape
-    ff_dev, chunk = wg_ref.shape[0], (wide - 128) // 2
+    chunk = (wide - 128) // 2
     columns = list(enumerate(t for value in sums for t in terms(value, 2)))
     stat = placed(columns, (rows, 128)).astype(BF)
-    for k, w_ref in enumerate((wg_ref, wu_ref)):
-        part = lax.dot_general(left, w_ref[...], NT, preferred_element_type=F32)
+    for k, part in enumerate(parts):
+        ff_dev = part.shape[1]
         for j in range(nk):
             lo, hi = j * chunk, min((j + 1) * chunk, ff_dev)
             size = max(hi - lo, 0)
@@ -547,23 +564,44 @@
 def base_kernel(rows_ref, gains_ref, wg_ref, wu_ref, m3, m2, m1, m0, msg_ref):
     x = rows_ref[...].astype(F32)
     left = (x * gains_ref[2:3, :]).astype(BF)
-    send_parts(left, wg_ref, wu_ref, [added(x, x)], (m0, m1, m2, m3), msg_ref)
+    parts = [
+        lax.dot_general(left, w[...], NT, preferred_element_type=F32) for w in (wg_ref, wu_ref)
+    ]
+    send_parts(parts, [added(x, x)], (m0, m1, m2, m3), msg_ref)
+
+
+def half_products(half_ref, core, gains_ref, wg_ref, wu_ref):
+    half = half_ref.shape[1]
+    at = pl.ds(pl.multiple_of(core * half, half), half)
+    gain = gains_ref[1:3, at]
+    left = (half_ref[...].astype(F32) * gain[0:1] * gain[1:2]).astype(BF)
+    return [
+        lax.dot_general(left, w[:, at], NT, preferred_element_type=F32) for w in (wg_ref, wu_ref)
+    ]
+
+
+def early_kernel(half_ref, gains_ref, wg_ref, wu_ref, gate_ref, up_ref):
+    core = lax.rem(lax.axis_index("tp"), 2)
+    gate_ref[...], up_ref[...] = half_products(half_ref, core, gains_ref, wg_ref, wu_ref)
 
 
 def gate_kernel(
-    half_ref, other_ref, rows_ref, gains_ref, wg_ref, wu_ref, m3, m2, m1, m0, post_ref, msg_ref
+    half_ref, other_ref, gate_ref, up_ref, rows_ref, gains_ref, wg_ref, wu_ref,
+    m3, m2, m1, m0, post_ref, msg_ref,
 ):
-    first = lax.rem(lax.axis_index("tp"), 2) == 0
+    core = lax.rem(lax.axis_index("tp"), 2)
+    late = half_products(other_ref, 1 - core, gains_ref, wg_ref, wu_ref)
+    parts = [gate_ref[...] + late[0], up_ref[...] + late[1]]
     mine, theirs = half_ref[...].astype(F32), other_ref[...].astype(F32)
+    first = core == 0
     att = jnp.concatenate(
         [jnp.where(first, mine, theirs), jnp.where(first, theirs, mine)], axis=1
     )
     x = rows_ref[...].astype(F32)
     post = att * gains_ref[1:2, :]
     post_ref[...] = post
-    left = (post * gains_ref[2:3, :]).astype(BF)
     sums = [added(att, att), added(x, post), added(post, post)]
-    send_parts(left, wg_ref, wu_ref, sums, (m0, m1, m2, m3), msg_ref)
+    send_parts(parts, sums, (m0, m1, m2, m3), msg_ref)
 
 
 def hidden_kernel(model_width, b0, b1, b2, b3, base_ref, out_ref, s_ref):
@@ -736,7 +774,7 @@
     got = exchange(msg.reshape(nk * nt, heads, latent + 128), ("kv", "tp"))
     msg = call(
         functools.partial(value_kernel, heads),
-        [like((nt + rows, value_dev))] * nk,
+        [like((nt, value_dev + own * wide))] * nk,
         got.reshape(nk, pairs, latent + 128),
         value_flat,
         *base_parts,
@@ -756,11 +794,21 @@
     )
     att_half = call(column_kernel, like((rows, half)), *deal([pair] * chips, "tp", 2), flops=WAIT)
     att_other = lax.ppermute(att_half, "tp", swap)
+    early = call(
+        early_kernel,
+        [like((rows, ff_dev), F32)] * 2,
+        att_half,
+        gains,
+        w_gate.T,
+        w_up.T,
+        flops=WAIT,
+    )
     *msg, post = call(
         gate_kernel,
         [like((rows, wide))] * nk + [like((rows, width), F32)],
         att_half,
         att_other,
+        *early,
         x_rows,
         gains,
         w_gate.T,
@@ -808,7 +856,6 @@
         and 2 * own == nt
         and width % 1024 == 0
         and latent % 256 == 0
-        and heads * args[8].shape[2] >= 2 * (-(-args[12].shape[1] // (nk * 128)) * 128) + 128
         and nope % 128 == 0
         and cache.shape[1] % 128 == 0
         and args[16].shape[2] == 64

time: 97.8 us -> 96.2 us (0.984)
  waiting for transfers between devices: 34.5 us -> 33.4 us
    pallas_call x17 -> x18, Pallas kernels: 10.6 us -> 10.1 us  [call(): pl.pallas_call(kernel, out_shape=outs, in_specs=[VMEM] * len(args), out_s...]
  transfers between devices with their start and end apart: 26 -> 26, of which waited for: 23 -> 23; matrix products, arithmetic and copies ran while one was open for 0% -> 0% of each run, Pallas kernels for 2% -> 3%
where the time goes in v4:
time: 96.2 us; the launch traced here: 95.9 us
  waiting for transfers between devices  33.4 us (35%)
  starting transfers between devices  31.8 us (33%)
  blocking collectives  14.2 us (15%)
  Pallas kernels  10.1 us (10%)
  local copies, waits for them, and re-layouts  5.55 us (6%)
    ppermute x21, starting transfers between devices, deal(): lax.ppermute(blocks[k], axis, [(i, i ^ k * step) for i in range(size)])  28.9 us
    ppermute x21, waiting for transfers between devices, deal(): lax.ppermute(blocks[k], axis, [(i, i ^ k * step) for i in range(size)])  23.4 us
    all_to_all x1, blocking collectives, exchange(): return lax.all_to_all(message, axis, 0, 0, tiled=True)  14.2 us
    pallas_call x18, Pallas kernels, call(): pl.pallas_call(kernel, out_shape=outs, in_specs=[VMEM] * len(args), out_s...  10.1 us
    all_to_all x1, waiting for transfers between devices, exchange(): return lax.all_to_all(message, axis, 0, 0, tiled=True)  6.09 us
    unnamed x42, local copies, waits for them, and re-layouts  5.55 us
    all_to_all x1, starting transfers between devices, exchange(): return lax.all_to_all(message, axis, 0, 0, tiled=True)  2.59 us
    ppermute x2, waiting for transfers between devices, kernel_body(): lax.ppermute(give, 'tp', swap)  2.39 us
  transfers between devices with their start and end apart: 26, of which 23 were waited for; matrix products, arithmetic and copies ran while one was open for 0% of the time, Pallas kernels for 3%

profile of v4, /device:TPU:0, one launch (start us, length us, event | category | flops | bytes accessed | tf_op | source)
XLA Modules:
  0.0 95.9 jit_solution(17209821543050694381)
XLA Ops:
  0.6 5.1 %collective-permute-start.2 = (bf16[4,1024]{1,0:T(4,128)(2,1)}, bf16[4,1024]{1,0:T(4,128)(2,1)S(1)}, u32[]{:S(2)}, u32[]{:S(2)}) collective-permute-start(bf16[4,1024]{1,0:T(4,128)(2,1)} %resid_ref.3), channel_id=1, source_target_pairs={{0,6},{1,7},{2,4},{3,5},{4,2},{5,3},{6,0},{7,1},{8,14},{9,15},{10,... | collective-permute-start | bytes 24584 | tf_op jit(solution)/shard_map/ppermute | solution.py:667
  7.6 2.9 %collective-permute-done.1.b2 = bf16[4,1024]{1,0:T(4,128)(2,1)S(1)} collective-permute-done((bf16[4,1024]{1,0:T(4,128)(2,1)}, bf16[4,1024]{1,0:T(4,128)(2,1)S(1)}, u32[]{:S(2)}, u32[]{:S(2)}) %collective-permute-start.1) | collective-permute-done | bytes 8224 | tf_op jit(solution)/shard_map/ppermute | solution.py:667
  12.7 1.6 %collective-permute-start.4 = (bf16[8,1920]{1,0:T(8,128)(2,1)S(1)}, bf16[8,1920]{1,0:T(8,128)(2,1)S(1)}, u32[]{:S(2)}, u32[]{:S(2)}) collective-permute-start(bf16[8,1920]{1,0:T(8,128)(2,1)S(1)} %get-tuple-element.40), channel_id=1, source_target_pairs={{0,8},{8,0},{16,24},{24,16},{1,9},{9,1},{17,25},{25,17},{2,10},{10... | collective-permute-start | bytes 92168 | tf_op jit(solution)/shard_map/ppermute | solution.py:667
  14.3 1.5 %collective-permute-start.5 = (bf16[8,1920]{1,0:T(8,128)(2,1)S(1)}, bf16[8,1920]{1,0:T(8,128)(2,1)S(1)}, u32[]{:S(2)}, u32[]{:S(2)}) collective-permute-start(bf16[8,1920]{1,0:T(8,128)(2,1)S(1)} %get-tuple-element.41), channel_id=1, source_target_pairs={{0,16},{8,24},{16,0},{24,8},{1,17},{9,25},{17,1},{25,9},{2,18},{10... | collective-permute-start | bytes 92168 | tf_op jit(solution)/shard_map/ppermute | solution.py:667
  16.7 1.5 %collective-permute-done.5.b2 = bf16[8,1920]{1,0:T(8,128)(2,1)S(1)} collective-permute-done((bf16[8,1920]{1,0:T(8,128)(2,1)S(1)}, bf16[8,1920]{1,0:T(8,128)(2,1)S(1)}, u32[]{:S(2)}, u32[]{:S(2)}) %collective-permute-start.5) | collective-permute-done | bytes 30752 | tf_op jit(solution)/shard_map/ppermute | solution.py:667
  18.2 2.4 %collective-permute-done.6.b3 = bf16[8,1920]{1,0:T(8,128)(2,1)S(1)} collective-permute-done((bf16[8,1920]{1,0:T(8,128)(2,1)S(1)}, bf16[8,1920]{1,0:T(8,128)(2,1)S(1)}, u32[]{:S(2)}, u32[]{:S(2)}) %collective-permute-start.6) | collective-permute-done | bytes 30752 | tf_op jit(solution)/shard_map/ppermute | solution.py:667
  21.6 14.2 %all_to_all.10 = bf16[32,8,640]{2,1,0:T(8,128)(2,1)S(1)} all-to-all(bf16[32,8,640]{2,1,0:T(8,128)(2,1)S(1)} %bitcast.12), channel_id=1, replica_groups=mesh['kv'=4,'tp'=8] {'kv','tp'}, dimensions={0} | all-to-all | bytes 655360 | tf_op jit(solution)/shard_map/all_to_all | solution.py:660
  35.8 2.0 %shard_map.198 = bf16[4,64,640]{2,1,0:T(8,128)(2,1)} custom-call(bf16[4,64,640]{2,1,0:T(8,128)(2,1)S(1)} %bitcast.13, bf16[4,512,512]{2,1,0:T(8,128)(2,1)S(1)} %copy-done.5, bf16[4,64,512]{2,1,0:T(8,128)(2,1)S(1)} %bitcast.21, f32[8,640]{1,0:T(8,128)S(1)} %get-tuple-element.44.own_ref), custom_call_target="tpu_custom_call" | custom-call | flops 4000000000 | bytes 3035136 | tf_op jit(solution)/shard_map/pallas_call | solution.py:273
  37.8 2.6 %all-to-all-start.1 = ((bf16[32,8,640]{2,1,0:T(8,128)(2,1)}), bf16[32,8,640]{2,1,0:T(8,128)(2,1)S(1)}, u32[]{:S(2)}, u32[]{:S(2)}) async-start(bf16[32,8,640]{2,1,0:T(8,128)(2,1)} %bitcast.7), calls=%async_computation.1 | async-start | bytes 655360 | tf_op jit(solution)/shard_map/all_to_all | solution.py:660
  44.7 1.7 %shard_map.200 = (bf16[32,896]{1,0:T(8,128)(2,1)S(1)}, bf16[32,896]{1,0:T(8,128)(2,1)S(1)}, bf16[32,896]{1,0:T(8,128)(2,1)S(1)}, bf16[32,896]{1,0:T(8,128)(2,1)S(1)}) custom-call(bf16[32,1024]{1,0:T(8,128)(2,1)S(1)} %get-tuple-element.45.rows_ref, f32[8,1024]{1,0:T(8,128)S(1)} %get-tuple-element.46.gains_ref, bf16[1376,1024]{1,0:T(8,128)(2,1)S(1)} %bitcast.14, ...), custom_call_target="tpu_custom_call" | custom-call | flops 4000000000 | bytes 5963776 | tf_op jit(solution)/shard_map/pallas_call | solution.py:273
  46.4 6.1 %all-to-all-done.1 = bf16[32,8,640]{2,1,0:T(8,128)(2,1)S(1)} async-done(((bf16[32,8,640]{2,1,0:T(8,128)(2,1)}), bf16[32,8,640]{2,1,0:T(8,128)(2,1)S(1)}, u32[]{:S(2)}, u32[]{:S(2)}) %all-to-all-start.1) | async-done | bytes 327712 | tf_op jit(solution)/shard_map/all_to_all | solution.py:660
  55.3 2.3 %collective-permute-start.9 = (bf16[8,4608]{1,0:T(8,128)(2,1)S(1)}, bf16[8,4608]{1,0:T(8,128)(2,1)S(1)}, u32[]{:S(2)}, u32[]{:S(2)}) collective-permute-start(bf16[8,4608]{1,0:T(8,128)(2,1)S(1)} %get-tuple-element.54), channel_id=1, source_target_pairs={{0,24},{8,16},{16,8},{24,0},{1,25},{9,17},{17,9},{25,1},{2,26},{10... | collective-permute-start | bytes 221192 | tf_op jit(solution)/shard_map/ppermute | solution.py:667
  58.5 2.1 %collective-permute-done.8.b2 = bf16[8,4608]{1,0:T(8,128)(2,1)S(1)} collective-permute-done((bf16[8,4608]{1,0:T(8,128)(2,1)S(1)}, bf16[8,4608]{1,0:T(8,128)(2,1)S(1)}, u32[]{:S(2)}, u32[]{:S(2)}) %collective-permute-start.8) | collective-permute-done | bytes 73760 | tf_op jit(solution)/shard_map/ppermute | solution.py:667
  62.4 1.8 %collective-permute-start.13 = (bf16[32,512]{1,0:T(8,128)(2,1)S(1)}, bf16[32,512]{1,0:T(8,128)(2,1)S(1)}, u32[]{:S(2)}, u32[]{:S(2)}) collective-permute-start(bf16[32,512]{1,0:T(8,128)(2,1)S(1)} %shard_map.203.b0), channel_id=1, source_target_pairs={{0,6},{1,7},{2,4},{3,5},{4,2},{5,3},{6,0},{7,1},{8,14},{9,15},{10,... | collective-permute-start | bytes 98312 | tf_op jit(solution)/shard_map/ppermute | solution.py:667
  64.2 2.6 %collective-permute-start.11 = (bf16[32,512]{1,0:T(8,128)(2,1)S(1)}, bf16[32,512]{1,0:T(8,128)(2,1)S(1)}, u32[]{:S(2)}, u32[]{:S(2)}) collective-permute-start(bf16[32,512]{1,0:T(8,128)(2,1)S(1)} %shard_map.203.b0), channel_id=1, source_target_pairs={{0,2},{1,3},{2,0},{3,1},{4,6},{5,7},{6,4},{7,5},{8,10},{9,11},{10,... | collective-permute-start | bytes 98312 | tf_op jit(solution)/shard_map/ppermute | solution.py:667
  66.9 1.3 %collective-permute-done.13.b3 = bf16[32,512]{1,0:T(8,128)(2,1)S(1)} collective-permute-done((bf16[32,512]{1,0:T(8,128)(2,1)S(1)}, bf16[32,512]{1,0:T(8,128)(2,1)S(1)}, u32[]{:S(2)}, u32[]{:S(2)}) %collective-permute-start.13) | collective-permute-done | bytes 32800 | tf_op jit(solution)/shard_map/ppermute | solution.py:667
  72.6 1.3 %collective-permute-start.16 = (bf16[32,896]{1,0:T(8,128)(2,1)S(1)}, bf16[32,896]{1,0:T(8,128)(2,1)S(1)}, u32[]{:S(2)}, u32[]{:S(2)}) collective-permute-start(bf16[32,896]{1,0:T(8,128)(2,1)S(1)} %get-tuple-element.61), channel_id=1, source_target_pairs={{0,16},{8,24},{16,0},{24,8},{1,17},{9,25},{17,1},{25,9},{2,18},{10... | collective-permute-start | bytes 172040 | tf_op jit(solution)/shard_map/ppermute | solution.py:667
  76.8 2.2 %collective-permute-done.17.b3 = bf16[32,896]{1,0:T(8,128)(2,1)S(1)} collective-permute-done((bf16[32,896]{1,0:T(8,128)(2,1)S(1)}, bf16[32,896]{1,0:T(8,128)(2,1)S(1)}, u32[]{:S(2)}, u32[]{:S(2)}) %collective-permute-start.17) | collective-permute-done | bytes 57376 | tf_op jit(solution)/shard_map/ppermute | solution.py:667
  79.2 1.2 %collective-permute-start.20 = (bf16[32,384]{1,0:T(8,128)(2,1)S(1)}, bf16[32,384]{1,0:T(8,128)(2,1)S(1)}, u32[]{:S(2)}, u32[]{:S(2)}) collective-permute-start(bf16[32,384]{1,0:T(8,128)(2,1)S(1)} %get-tuple-element.64.b0), channel_id=1, source_target_pairs={{0,24},{8,16},{16,8},{24,0},{1,25},{9,17},{17,9},{25,1},{2,26},{10... | collective-permute-start | bytes 73736 | tf_op jit(solution)/shard_map/ppermute | solution.py:667
  81.5 1.3 %collective-permute-start.18 = (bf16[32,384]{1,0:T(8,128)(2,1)S(1)}, bf16[32,384]{1,0:T(8,128)(2,1)S(1)}, u32[]{:S(2)}, u32[]{:S(2)}) collective-permute-start(bf16[32,384]{1,0:T(8,128)(2,1)S(1)} %get-tuple-element.64.b0), channel_id=1, source_target_pairs={{0,8},{8,0},{16,24},{24,16},{1,9},{9,1},{17,25},{25,17},{2,10},{10... | collective-permute-start | bytes 73736 | tf_op jit(solution)/shard_map/ppermute | solution.py:667
  87.3 1.5 %collective-permute-start.22 = (bf16[4,1024]{1,0:T(4,128)(2,1)S(1)}, bf16[4,1024]{1,0:T(4,128)(2,1)S(1)}, u32[]{:S(2)}, u32[]{:S(2)}) collective-permute-start(bf16[4,1024]{1,0:T(4,128)(2,1)S(1)} %get-tuple-element.68), channel_id=1, source_target_pairs={{0,2},{1,3},{2,0},{3,1},{4,6},{5,7},{6,4},{7,5},{8,10},{9,11},{10,... | collective-permute-start | bytes 24584 | tf_op jit(solution)/shard_map/ppermute | solution.py:667
  89.7 2.1 %collective-permute-start.24 = (bf16[4,1024]{1,0:T(4,128)(2,1)S(1)}, bf16[4,1024]{1,0:T(4,128)(2,1)S(1)}, u32[]{:S(2)}, u32[]{:S(2)}) collective-permute-start(bf16[4,1024]{1,0:T(4,128)(2,1)S(1)} %get-tuple-element.70), channel_id=1, source_target_pairs={{0,6},{1,7},{2,4},{3,5},{4,2},{5,3},{6,0},{7,1},{8,14},{9,15},{10,... | collective-permute-start | bytes 24584 | tf_op jit(solution)/shard_map/ppermute | solution.py:667
  91.8 1.6 %collective-permute-done.23.b2 = bf16[4,1024]{1,0:T(4,128)(2,1)S(1)} collective-permute-done((bf16[4,1024]{1,0:T(4,128)(2,1)S(1)}, bf16[4,1024]{1,0:T(4,128)(2,1)S(1)}, u32[]{:S(2)}, u32[]{:S(2)}) %collective-permute-start.23) | collective-permute-done | bytes 8224 | tf_op jit(solution)/shard_map/ppermute | solution.py:667
  93.4 1.8 %collective-permute-done.24.b3 = bf16[4,1024]{1,0:T(4,128)(2,1)S(1)} collective-permute-done((bf16[4,1024]{1,0:T(4,128)(2,1)S(1)}, bf16[4,1024]{1,0:T(4,128)(2,1)S(1)}, u32[]{:S(2)}, u32[]{:S(2)}) %collective-permute-start.24) | collective-permute-done | bytes 8224 | tf_op jit(solution)/shard_map/ppermute | solution.py:667
  (90 shorter events, 30.2 us)
Async XLA Ops:
  0.6 7.0 %collective-permute-start.2 = (bf16[4,1024]{1,0:T(4,128)(2,1)}, bf16[4,1024]{1,0:T(4,128)(2,1)S(1)}, u32[]{:S(2)}, u32[]{:S(2)}) collective-permute-start(bf16[4,1024]{1,0:T(4,128)(2,1)} %resid_ref.3), channel_id=1, source_target_pairs={{0,6},{1,7},{2,4},{3,5},{4,2},{5,3},{6,0},{7,1},{8,14},{9,15},{10,... | collective-permute-start | bytes 24584 | tf_op jit(solution)/shard_map/ppermute | solution.py:667
  5.8 4.8 %collective-permute-start.1 = (bf16[4,1024]{1,0:T(4,128)(2,1)}, bf16[4,1024]{1,0:T(4,128)(2,1)S(1)}, u32[]{:S(2)}, u32[]{:S(2)}) collective-permute-start(bf16[4,1024]{1,0:T(4,128)(2,1)} %resid_ref.3), channel_id=1, source_target_pairs={{0,4},{1,5},{2,6},{3,7},{4,0},{5,1},{6,2},{7,3},{8,12},{9,13},{10,... | collective-permute-start | bytes 24584 | tf_op jit(solution)/shard_map/ppermute | solution.py:667
  5.8 4.8 %collective-permute-start = (bf16[4,1024]{1,0:T(4,128)(2,1)}, bf16[4,1024]{1,0:T(4,128)(2,1)S(1)}, u32[]{:S(2)}, u32[]{:S(2)}) collective-permute-start(bf16[4,1024]{1,0:T(4,128)(2,1)} %resid_ref.3), channel_id=1, source_target_pairs={{0,2},{1,3},{2,0},{3,1},{4,6},{5,7},{6,4},{7,5},{8,10},{9,11},{10,... | collective-permute-start | bytes 24584 | tf_op jit(solution)/shard_map/ppermute | solution.py:667
  10.6 1.3 %collective-permute-start.3 = (bf16[16,1024]{1,0:T(8,128)(2,1)S(1)}, bf16[16,1024]{1,0:T(8,128)(2,1)S(1)}, u32[]{:S(2)}, u32[]{:S(2)}) collective-permute-start(bf16[16,1024]{1,0:T(8,128)(2,1)S(1)} %shard_map.194.half_ref), channel_id=1, source_target_pairs={{0,1},{1,0},{2,3},{3,2},{4,5},{5,4},{6,7},{7,6},{8,9},{9,8},{10,11... | collective-permute-start | bytes 98312 | tf_op jit(solution)/shard_map/ppermute | solution.py:726
  12.7 4.0 %collective-permute-start.4 = (bf16[8,1920]{1,0:T(8,128)(2,1)S(1)}, bf16[8,1920]{1,0:T(8,128)(2,1)S(1)}, u32[]{:S(2)}, u32[]{:S(2)}) collective-permute-start(bf16[8,1920]{1,0:T(8,128)(2,1)S(1)} %get-tuple-element.40), channel_id=1, source_target_pairs={{0,8},{8,0},{16,24},{24,16},{1,9},{9,1},{17,25},{25,17},{2,10},{10... | collective-permute-start | bytes 92168 | tf_op jit(solution)/shard_map/ppermute | solution.py:667
  14.3 3.9 %collective-permute-start.5 = (bf16[8,1920]{1,0:T(8,128)(2,1)S(1)}, bf16[8,1920]{1,0:T(8,128)(2,1)S(1)}, u32[]{:S(2)}, u32[]{:S(2)}) collective-permute-start(bf16[8,1920]{1,0:T(8,128)(2,1)S(1)} %get-tuple-element.41), channel_id=1, source_target_pairs={{0,16},{8,24},{16,0},{24,8},{1,17},{9,25},{17,1},{25,9},{2,18},{10... | collective-permute-start | bytes 92168 | tf_op jit(solution)/shard_map/ppermute | solution.py:667
  15.8 4.8 %collective-permute-start.6 = (bf16[8,1920]{1,0:T(8,128)(2,1)S(1)}, bf16[8,1920]{1,0:T(8,128)(2,1)S(1)}, u32[]{:S(2)}, u32[]{:S(2)}) collective-permute-start(bf16[8,1920]{1,0:T(8,128)(2,1)S(1)} %get-tuple-element.42), channel_id=1, source_target_pairs={{0,24},{8,16},{16,8},{24,0},{1,25},{9,17},{17,9},{25,1},{2,26},{10... | collective-permute-start | bytes 92168 | tf_op jit(solution)/shard_map/ppermute | solution.py:667
  37.8 14.6 %all-to-all-start.1 = ((bf16[32,8,640]{2,1,0:T(8,128)(2,1)}), bf16[32,8,640]{2,1,0:T(8,128)(2,1)S(1)}, u32[]{:S(2)}, u32[]{:S(2)}) async-start(bf16[32,8,640]{2,1,0:T(8,128)(2,1)} %bitcast.7), calls=%async_computation.1 | async-start | bytes 655360 | tf_op jit(solution)/shard_map/all_to_all | solution.py:660
  54.1 4.4 %collective-permute-start.7 = (bf16[8,4608]{1,0:T(8,128)(2,1)S(1)}, bf16[8,4608]{1,0:T(8,128)(2,1)S(1)}, u32[]{:S(2)}, u32[]{:S(2)}) collective-permute-start(bf16[8,4608]{1,0:T(8,128)(2,1)S(1)} %get-tuple-element.52), channel_id=1, source_target_pairs={{0,8},{8,0},{16,24},{24,16},{1,9},{9,1},{17,25},{25,17},{2,10},{10... | collective-permute-start | bytes 221192 | tf_op jit(solution)/shard_map/ppermute | solution.py:667
  54.2 6.4 %collective-permute-start.8 = (bf16[8,4608]{1,0:T(8,128)(2,1)S(1)}, bf16[8,4608]{1,0:T(8,128)(2,1)S(1)}, u32[]{:S(2)}, u32[]{:S(2)}) collective-permute-start(bf16[8,4608]{1,0:T(8,128)(2,1)S(1)} %get-tuple-element.53), channel_id=1, source_target_pairs={{0,16},{8,24},{16,0},{24,8},{1,17},{9,25},{17,1},{25,9},{2,18},{10... | collective-permute-start | bytes 221192 | tf_op jit(solution)/shard_map/ppermute | solution.py:667
  55.3 5.3 %collective-permute-start.9 = (bf16[8,4608]{1,0:T(8,128)(2,1)S(1)}, bf16[8,4608]{1,0:T(8,128)(2,1)S(1)}, u32[]{:S(2)}, u32[]{:S(2)}) collective-permute-start(bf16[8,4608]{1,0:T(8,128)(2,1)S(1)} %get-tuple-element.54), channel_id=1, source_target_pairs={{0,24},{8,16},{16,8},{24,0},{1,25},{9,17},{17,9},{25,1},{2,26},{10... | collective-permute-start | bytes 221192 | tf_op jit(solution)/shard_map/ppermute | solution.py:667
  61.1 1.3 %collective-permute-start.10 = (bf16[32,512]{1,0:T(8,128)(2,1)S(1)}, bf16[32,512]{1,0:T(8,128)(2,1)S(1)}, u32[]{:S(2)}, u32[]{:S(2)}) collective-permute-start(bf16[32,512]{1,0:T(8,128)(2,1)S(1)} %get-tuple-element.56), channel_id=1, source_target_pairs={{0,1},{1,0},{2,3},{3,2},{4,5},{5,4},{6,7},{7,6},{8,9},{9,8},{10,11... | collective-permute-start | bytes 98312 | tf_op jit(solution)/shard_map/ppermute | solution.py:793
  62.4 5.8 %collective-permute-start.13 = (bf16[32,512]{1,0:T(8,128)(2,1)S(1)}, bf16[32,512]{1,0:T(8,128)(2,1)S(1)}, u32[]{:S(2)}, u32[]{:S(2)}) collective-permute-start(bf16[32,512]{1,0:T(8,128)(2,1)S(1)} %shard_map.203.b0), channel_id=1, source_target_pairs={{0,6},{1,7},{2,4},{3,5},{4,2},{5,3},{6,0},{7,1},{8,14},{9,15},{10,... | collective-permute-start | bytes 98312 | tf_op jit(solution)/shard_map/ppermute | solution.py:667
  64.2 4.9 %collective-permute-start.12 = (bf16[32,512]{1,0:T(8,128)(2,1)S(1)}, bf16[32,512]{1,0:T(8,128)(2,1)S(1)}, u32[]{:S(2)}, u32[]{:S(2)}) collective-permute-start(bf16[32,512]{1,0:T(8,128)(2,1)S(1)} %shard_map.203.b0), channel_id=1, source_target_pairs={{0,4},{1,5},{2,6},{3,7},{4,0},{5,1},{6,2},{7,3},{8,12},{9,13},{10,... | collective-permute-start | bytes 98312 | tf_op jit(solution)/shard_map/ppermute | solution.py:667
  64.2 5.1 %collective-permute-start.11 = (bf16[32,512]{1,0:T(8,128)(2,1)S(1)}, bf16[32,512]{1,0:T(8,128)(2,1)S(1)}, u32[]{:S(2)}, u32[]{:S(2)}) collective-permute-start(bf16[32,512]{1,0:T(8,128)(2,1)S(1)} %shard_map.203.b0), channel_id=1, source_target_pairs={{0,2},{1,3},{2,0},{3,1},{4,6},{5,7},{6,4},{7,5},{8,10},{9,11},{10,... | collective-permute-start | bytes 98312 | tf_op jit(solution)/shard_map/ppermute | solution.py:667
  71.6 4.2 %collective-permute-start.15 = (bf16[32,896]{1,0:T(8,128)(2,1)S(1)}, bf16[32,896]{1,0:T(8,128)(2,1)S(1)}, u32[]{:S(2)}, u32[]{:S(2)}) collective-permute-start(bf16[32,896]{1,0:T(8,128)(2,1)S(1)} %get-tuple-element.60), channel_id=1, source_target_pairs={{0,8},{8,0},{16,24},{24,16},{1,9},{9,1},{17,25},{25,17},{2,10},{10... | collective-permute-start | bytes 172040 | tf_op jit(solution)/shard_map/ppermute | solution.py:667
  72.6 4.2 %collective-permute-start.16 = (bf16[32,896]{1,0:T(8,128)(2,1)S(1)}, bf16[32,896]{1,0:T(8,128)(2,1)S(1)}, u32[]{:S(2)}, u32[]{:S(2)}) collective-permute-start(bf16[32,896]{1,0:T(8,128)(2,1)S(1)} %get-tuple-element.61), channel_id=1, source_target_pairs={{0,16},{8,24},{16,0},{24,8},{1,17},{9,25},{17,1},{25,9},{2,18},{10... | collective-permute-start | bytes 172040 | tf_op jit(solution)/shard_map/ppermute | solution.py:667
  73.9 5.1 %collective-permute-start.17 = (bf16[32,896]{1,0:T(8,128)(2,1)S(1)}, bf16[32,896]{1,0:T(8,128)(2,1)S(1)}, u32[]{:S(2)}, u32[]{:S(2)}) collective-permute-start(bf16[32,896]{1,0:T(8,128)(2,1)S(1)} %get-tuple-element.62), channel_id=1, source_target_pairs={{0,24},{8,16},{16,8},{24,0},{1,25},{9,17},{17,9},{25,1},{2,26},{10... | collective-permute-start | bytes 172040 | tf_op jit(solution)/shard_map/ppermute | solution.py:667
  79.2 4.8 %collective-permute-start.20 = (bf16[32,384]{1,0:T(8,128)(2,1)S(1)}, bf16[32,384]{1,0:T(8,128)(2,1)S(1)}, u32[]{:S(2)}, u32[]{:S(2)}) collective-permute-start(bf16[32,384]{1,0:T(8,128)(2,1)S(1)} %get-tuple-element.64.b0), channel_id=1, source_target_pairs={{0,24},{8,16},{16,8},{24,0},{1,25},{9,17},{17,9},{25,1},{2,26},{10... | collective-permute-start | bytes 73736 | tf_op jit(solution)/shard_map/ppermute | solution.py:667
  80.4 3.8 %collective-permute-start.19 = (bf16[32,384]{1,0:T(8,128)(2,1)S(1)}, bf16[32,384]{1,0:T(8,128)(2,1)S(1)}, u32[]{:S(2)}, u32[]{:S(2)}) collective-permute-start(bf16[32,384]{1,0:T(8,128)(2,1)S(1)} %get-tuple-element.64.b0), channel_id=1, source_target_pairs={{0,16},{8,24},{16,0},{24,8},{1,17},{9,25},{17,1},{25,9},{2,18},{10... | collective-permute-start | bytes 73736 | tf_op jit(solution)/shard_map/ppermute | solution.py:667
  81.5 3.8 %collective-permute-start.18 = (bf16[32,384]{1,0:T(8,128)(2,1)S(1)}, bf16[32,384]{1,0:T(8,128)(2,1)S(1)}, u32[]{:S(2)}, u32[]{:S(2)}) collective-permute-start(bf16[32,384]{1,0:T(8,128)(2,1)S(1)} %get-tuple-element.64.b0), channel_id=1, source_target_pairs={{0,8},{8,0},{16,24},{24,16},{1,9},{9,1},{17,25},{25,17},{2,10},{10... | collective-permute-start | bytes 73736 | tf_op jit(solution)/shard_map/ppermute | solution.py:667
  87.3 4.5 %collective-permute-start.22 = (bf16[4,1024]{1,0:T(4,128)(2,1)S(1)}, bf16[4,1024]{1,0:T(4,128)(2,1)S(1)}, u32[]{:S(2)}, u32[]{:S(2)}) collective-permute-start(bf16[4,1024]{1,0:T(4,128)(2,1)S(1)} %get-tuple-element.68), channel_id=1, source_target_pairs={{0,2},{1,3},{2,0},{3,1},{4,6},{5,7},{6,4},{7,5},{8,10},{9,11},{10,... | collective-permute-start | bytes 24584 | tf_op jit(solution)/shard_map/ppermute | solution.py:667
  88.8 4.6 %collective-permute-start.23 = (bf16[4,1024]{1,0:T(4,128)(2,1)S(1)}, bf16[4,1024]{1,0:T(4,128)(2,1)S(1)}, u32[]{:S(2)}, u32[]{:S(2)}) collective-permute-start(bf16[4,1024]{1,0:T(4,128)(2,1)S(1)} %get-tuple-element.69), channel_id=1, source_target_pairs={{0,4},{1,5},{2,6},{3,7},{4,0},{5,1},{6,2},{7,3},{8,12},{9,13},{10,... | collective-permute-start | bytes 24584 | tf_op jit(solution)/shard_map/ppermute | solution.py:667
  89.7 5.4 %collective-permute-start.24 = (bf16[4,1024]{1,0:T(4,128)(2,1)S(1)}, bf16[4,1024]{1,0:T(4,128)(2,1)S(1)}, u32[]{:S(2)}, u32[]{:S(2)}) collective-permute-start(bf16[4,1024]{1,0:T(4,128)(2,1)S(1)} %get-tuple-element.70), channel_id=1, source_target_pairs={{0,6},{1,7},{2,4},{3,5},{4,2},{5,3},{6,0},{7,1},{8,14},{9,15},{10,... | collective-permute-start | bytes 24584 | tf_op jit(solution)/shard_map/ppermute | solution.py:667
  (23 other events, 119.3 us)

commit v5 on v4

--- a/solution.py
+++ b/solution.py
@@ -332,10 +332,6 @@
     out_ref[...] = jnp.where(row == lane_of(out_ref.shape), 1.0, 0.0).astype(BF)
 
 
-def flat_kernel(in_ref, out_ref):
-    out_ref[...] = in_ref[...].reshape(out_ref.shape)
-
-
 def start_kernel(b0, b1, b2, b3, unit_ref, out_ref, held_ref):
     chips, own, _ = held_ref.shape
     for k, ref in enumerate((b0, b1, b2, b3)):
@@ -345,14 +341,34 @@
     ).astype(BF)
 
 
+def own_kernel(resid_ref, ga_ref, gp_ref, gm_ref, wl_ref, wk_ref, gains_ref, own_ref):
+    own, width = resid_ref.shape
+    nt = own_ref.shape[0]
+    latent, rope = wl_ref.shape[1], wk_ref.shape[0]
+    tiles = width // 128
+    at = pl.multiple_of(lax.axis_index("kv") * tiles, tiles)
+    gains = []
+    for ref in (ga_ref, gp_ref, gm_ref):
+        block = ref[pl.ds(at, tiles), :].astype(F32)
+        gains.append(jnp.concatenate([block[i : i + 1] for i in range(tiles)], axis=1))
+    gains_ref[...] = jnp.concatenate(gains + [jnp.zeros((8 - len(gains), width), F32)], axis=0)
+    mine = jnp.concatenate([resid_ref[...].astype(F32), jnp.zeros((nt - own, width), F32)], axis=0)
+    own_normed = (mine * gains[0]).astype(BF)
+    lat = jnp.dot(own_normed, wl_ref[...], preferred_element_type=F32)
+    at = pl.multiple_of(lax.axis_index("kv") * width, width)
+    key = lax.dot_general(own_normed, wk_ref[:, pl.ds(at, width)], NT, preferred_element_type=F32)
+    half = latent // 2
+    own_ref[:, :half] = lat[:, :half] + pltpu.roll(lat[:, half:], own, 0)
+    key = jnp.concatenate([key, jnp.zeros((nt, 128 - rope), F32)], axis=1)
+    squares = terms(jnp.sum(mine * mine, axis=1, keepdims=True), 2)
+    stat = placed([(rope + i, c) for i, c in enumerate(squares)], key.shape)
+    own_ref[:, half:] = jnp.where(lane_of(key.shape) < rope, key, stat)
+
+
 def query_kernel(
-    half_ref, other_ref, resid_ref, ga_ref, gp_ref, gm_ref, wn_ref, wr_ref, wl_ref, wk_ref,
-    m3, m2, m1, m0, rows_ref, gains_ref, sent_ref,
+    rope, half_ref, other_ref, gains_ref, own_ref, wn_ref, wr_ref, m3, m2, m1, m0, rows_ref, sent_ref
 ):
-    own, width = resid_ref.shape
-    nt = rows_ref.shape[0] // own
-    latent = wl_ref.shape[1]
-    rope = wk_ref.shape[0]
+    nt = own_ref.shape[0]
     nope_dev, rope_dev = wn_ref.shape[1], wr_ref.shape[1]
     first = lax.rem(lax.axis_index("tp"), 2) == 0
     mine, theirs = half_ref[...].astype(F32), other_ref[...].astype(F32)
@@ -361,37 +377,24 @@
         [core[i : i + 1] for i in range(mine.shape[0]) for core in cores], axis=0
     )
     rows_ref[...] = x.astype(BF)
-    tiles = width // 128
-    at = pl.multiple_of(lax.axis_index("kv") * tiles, tiles)
-    gains = []
-    for ref in (ga_ref, gp_ref, gm_ref):
-        block = ref[pl.ds(at, tiles), :].astype(F32)
-        gains.append(jnp.concatenate([block[i : i + 1] for i in range(tiles)], axis=1))
-    gain = gains[0]
-    gains_ref[...] = jnp.concatenate(gains + [jnp.zeros((8 - len(gains), width), F32)], axis=0)
+    gain = gains_ref[0:1, :]
     normed = (x * gain).astype(BF)
     qn = jnp.dot(normed, wn_ref[...], preferred_element_type=F32)
     qr = jnp.dot(normed, wr_ref[...], preferred_element_type=F32)
     square = jnp.sum(x * x, axis=1, keepdims=True)
-    mine = jnp.concatenate([resid_ref[...].astype(F32), jnp.zeros((nt - own, width), F32)], axis=0)
-    own_square = jnp.sum(mine * mine, axis=1, keepdims=True)
-    own_normed = (mine * gain).astype(BF)
-    lat = jnp.dot(own_normed, wl_ref[...], preferred_element_type=F32)
-    at = pl.multiple_of(lax.axis_index("kv") * width, width)
-    key = lax.dot_general(own_normed, wk_ref[:, pl.ds(at, width)], NT, preferred_element_type=F32)
-    half = latent // 2
-    lat = lat[:, :half] + pltpu.roll(lat[:, half:], own, 0)
-    key = jnp.concatenate([key, jnp.zeros((nt, 128 - rope), F32)], axis=1)
-    own_terms = terms(own_square, 2)
+    half = own_ref.shape[1] - 128
+    lat, key = own_ref[:, :half], own_ref[:, half:]
+    lane = lane_of(key.shape)
     for r in range(sent_ref.shape[0]):
         part = slice(r * nt, (r + 1) * nt)
         sent_ref[r, :, :nope_dev] = qn[part].astype(BF)
         sent_ref[r, :, nope_dev : nope_dev + rope_dev] = qr[part].astype(BF)
         base = nope_dev + rope_dev
         sent_ref[r, :, base : base + half] = lat.astype(BF)
-        columns = [(rope + i, c) for i, c in enumerate(own_terms + terms(square[part], 2))]
-        stat = placed(columns, key.shape)
-        sent_ref[r, :, base + half :] = jnp.where(lane_of(key.shape) < rope, key, stat).astype(BF)
+        block = key
+        for i, column in enumerate(terms(square[part], 2)):
+            block = jnp.where(lane == rope + 2 + i, column, block)
+        sent_ref[r, :, base + half :] = block.astype(BF)
     for k, ref in enumerate((m0, m1, m2, m3)):
         ref[...] = sent_ref[other("kv", k)]
 
@@ -408,8 +411,8 @@
     nk, pairs, _ = msg_ref.shape
     nt = b0.shape[0]
     heads = pairs // nt
-    latent, nope_dev = ku_ref.shape
-    nope = nope_dev // heads
+    latent, _, nope = ku_ref.shape
+    nope_dev = heads * nope
     own, rope = key_ref.shape
     rope_dev = heads * rope
     total = four((b0, b1, b2, b3))
@@ -427,7 +430,7 @@
     key_ref[...] = key[:own, :rope]
     own_ref[:, :latent] = lat.astype(F32)
     own_ref[:, latent:] = key.astype(F32)
-    qn = (total[:, :nope_dev] * scale).astype(BF).astype(F32)
+    qn = total[:, :nope_dev].astype(BF).astype(F32)
     qr = turned(total[:, nope_dev:base] * scale, table, rope // 2).astype(BF).astype(F32)
 
     def diagonal(q, size):
@@ -438,9 +441,11 @@
         spread_q = jnp.broadcast_to(q[:, None, :], shape)
         return jnp.where(keep, spread_q, 0.0).reshape(nt * heads, heads * size).astype(BF)
 
-    q_lat = lax.dot_general(
-        diagonal(qn, nope), ku_ref[...], NT, preferred_element_type=F32
-    ).astype(BF)
+    raw = lax.dot_general(
+        diagonal(qn, nope), ku_ref[...].reshape(latent, nope_dev), NT, preferred_element_type=F32
+    )
+    scales = jnp.broadcast_to(scale[:, None, :], (nt, heads, latent)).reshape(pairs, latent)
+    q_lat = (raw * scales).astype(BF)
     q_rope = jnp.dot(diagonal(qr, rope), unit_ref[...], preferred_element_type=F32).astype(BF)
     for j in range(nk):
         msg_ref[j, :, :latent] = q_lat
@@ -489,8 +494,8 @@
 
 def value_kernel(heads, got_ref, vu_ref, a0, a1, a2, a3, m3, m2, m1, m0):
     nk, pairs, _ = got_ref.shape
-    latent, value_dev = vu_ref.shape
-    size = value_dev // heads
+    latent, _, size = vu_ref.shape
+    value_dev = heads * size
     nt = pairs // heads
     stats = [got_ref[j, :, latent:].astype(F32) for j in range(nk)]
     peaks = [picked(s, 0, 3) for s in stats]
@@ -499,7 +504,7 @@
     total = sum(picked(s, 3, 3) * f for s, f in zip(stats, factors))
     value = sum(got_ref[j, :, :latent].astype(F32) * f for j, f in enumerate(factors))
     o_lat = (value / total).astype(BF)
-    full = jnp.dot(o_lat, vu_ref[...], preferred_element_type=F32)
+    full = jnp.dot(o_lat, vu_ref[...].reshape(latent, value_dev), preferred_element_type=F32)
     shape = (nt, heads, value_dev)
     head = lax.broadcasted_iota(jnp.int32, shape, 1)
     lane = lax.broadcasted_iota(jnp.int32, shape, 2)
@@ -543,20 +548,12 @@
 
 def send_parts(parts, sums, refs, msg_ref):
     nk, rows, wide = msg_ref.shape
-    chunk = (wide - 128) // 2
-    columns = list(enumerate(t for value in sums for t in terms(value, 2)))
-    stat = placed(columns, (rows, 128)).astype(BF)
-    for k, part in enumerate(parts):
-        ff_dev = part.shape[1]
-        for j in range(nk):
-            lo, hi = j * chunk, min((j + 1) * chunk, ff_dev)
-            size = max(hi - lo, 0)
-            if size < chunk:
-                msg_ref[j, :, k * chunk : (k + 1) * chunk] = jnp.zeros((rows, chunk), BF)
-            if size > 0:
-                msg_ref[j, :, k * chunk : k * chunk + size] = part[:, lo:hi].astype(BF)
+    chunk = parts[0].shape[1] // nk
+    columns = list(enumerate(t for value in sums for t in terms(value, 3)))
+    stat = placed(columns, (rows, 128))[:, : wide - 2 * chunk]
     for j in range(nk):
-        msg_ref[j, :, 2 * chunk :] = stat
+        block = slice(j * chunk, (j + 1) * chunk)
+        msg_ref[j] = jnp.concatenate([part[:, block] for part in parts] + [stat], axis=1).astype(BF)
     for k, ref in enumerate(refs):
         ref[...] = msg_ref[other("kv", k)]
 
@@ -607,31 +604,33 @@
 def hidden_kernel(model_width, b0, b1, b2, b3, base_ref, out_ref, s_ref):
     _, chunk = out_ref.shape
     total, base = four((b0, b1, b2, b3)), base_ref[...]
-    stat = total[:, 2 * chunk :]
-    x_square = picked(base[:, 2 * chunk :], 0, 2)
-    att_square, cross, post_square = (picked(stat, 2 * i, 2) for i in range(3))
+    tail = total.shape[1] - 128
+    at = 2 * chunk - tail
+    x_square = picked(base[:, tail:], at, 3)
+    att_square, cross, post_square = (picked(total[:, tail:], at + 3 * i, 3) for i in range(3))
     s = lax.rsqrt(att_square / model_width + EPS)
     mid = jnp.maximum(x_square + 2.0 * s * cross + s * s * post_square, 0.0)
     scale = lax.rsqrt(mid / model_width + EPS)
     s_ref[...] = jnp.broadcast_to(s, s_ref.shape)
     mixed = (base[:, : 2 * chunk] + s * total[:, : 2 * chunk]) * scale
-    gate, up = mixed[:, :chunk], mixed[:, chunk:]
+    gate, up = mixed[:, :chunk], mixed[:, chunk : 2 * chunk]
     out_ref[...] = (gate / (1.0 + jnp.exp(-gate)) * up).astype(BF)
 
 
-def down_kernel(b0, b1, b2, b3, w_ref, keep_ref, give_ref, held_ref, total_ref):
-    nk, _, chunk = held_ref.shape
-    for k, ref in enumerate((b0, b1, b2, b3)):
-        held_ref[other("kv", k)] = ref[...]
-    ff_dev = w_ref.shape[0]
-    total = None
-    for j in range(nk):
-        lo, hi = j * chunk, min((j + 1) * chunk, ff_dev)
-        if hi > lo:
-            part = jnp.dot(
-                held_ref[j, :, : hi - lo], w_ref[lo:hi, :], preferred_element_type=F32
-            )
-            total = part if total is None else total + part
+def down_part(hidden_ref, w_ref, k):
+    chunk = hidden_ref.shape[1]
+    at = pl.multiple_of(other("kv", k) * chunk, 8)
+    return jnp.dot(hidden_ref[...], w_ref[pl.ds(at, chunk), :], preferred_element_type=F32)
+
+
+def first_kernel(hidden_ref, w_ref, out_ref):
+    out_ref[...] = down_part(hidden_ref, w_ref, 0)
+
+
+def down_kernel(first_ref, b1, b2, b3, w_ref, keep_ref, give_ref, total_ref):
+    total = first_ref[...]
+    for k, ref in ((1, b1), (2, b2), (3, b3)):
+        total = total + down_part(ref, w_ref, k)
     total_ref[...] = total.reshape(total_ref.shape)
     core = lax.rem(lax.axis_index("tp"), 2)
     for k in range(keep_ref.shape[0]):
@@ -708,8 +707,15 @@
     chips = nt // 2
     unit = call(unit_kernel, like((rope_dev, 2 * rope)), flops=WAIT)
     value_dev = heads * value_up.shape[2]
-    key_flat = call(flat_kernel, like((latent, nope_dev)), key_up, flops=WAIT)
-    value_flat = call(flat_kernel, like((latent, value_dev)), value_up, flops=WAIT)
+    gains, own_rows = call(
+        own_kernel,
+        [like((8, width), F32), like((nt, latent // 2 + 128), F32)],
+        resid,
+        *[g.reshape(-1, 128) for g in (attn_gain, post_gain, mlp_gain)],
+        w_latent,
+        w_key_rope.T,
+        flops=WAIT,
+    )
     column = call(
         start_kernel,
         like((own * chips, width)),
@@ -719,23 +725,21 @@
         flops=WAIT,
     )
     sent_width = nope_dev + rope_dev + latent // 2 + 128
-    *msg, x_rows, gains = call(
-        query_kernel,
-        [like((nt, sent_width))] * nk + [like((rows, width)), like((8, width), F32)],
+    *msg, x_rows = call(
+        functools.partial(query_kernel, rope),
+        [like((nt, sent_width))] * nk + [like((rows, width))],
         column,
         lax.ppermute(column, "tp", swap),
-        resid,
-        *[g.reshape(-1, 128) for g in (attn_gain, post_gain, mlp_gain)],
+        gains,
+        own_rows,
         w_query_nope,
         w_query_rope,
-        w_latent,
-        w_key_rope.T,
         scratch=[pltpu.VMEM((nk, nt, sent_width), BF)],
         flops=WAIT,
     )
     pairs = nt * heads
-    chunk = -(-ff_dev // (nk * 128)) * 128
-    wide = 2 * chunk + 128
+    chunk = ff_dev // nk
+    wide = -(-(2 * chunk + 9) // 128) * 128
     base_parts = call(
         base_kernel,
         [like((rows, wide))] * nk,
@@ -755,7 +759,7 @@
             like((nt, latent + 128), F32),
         ],
         *deal(msg[::-1], "kv"),
-        key_flat,
+        key_up,
         latent_gain.reshape(1, latent),
         jnp.asarray(table),
         unit,
@@ -776,7 +780,7 @@
         functools.partial(value_kernel, heads),
         [like((nt, value_dev + own * wide))] * nk,
         got.reshape(nk, pairs, latent + 128),
-        value_flat,
+        value_up,
         *base_parts,
         flops=WAIT,
     )
@@ -823,12 +827,14 @@
         base,
         flops=WAIT,
     )
+    first = call(first_kernel, like((rows, width), F32), hidden, w_down, flops=WAIT)
     keep, give = call(
         down_kernel,
         [like((chips, own, width), F32), like((chips, own, width))],
-        *deal([hidden] * nk, "kv"),
+        first,
+        *deal([hidden] * nk, "kv")[1:],
         w_down,
-        scratch=[pltpu.VMEM((nk, rows, chunk), BF), pltpu.VMEM((own, nt, width), F32)],
+        scratch=[pltpu.VMEM((own, nt, width), F32)],
         flops=WAIT,
     )
     msg = call(
@@ -856,6 +862,8 @@
         and 2 * own == nt
         and width % 1024 == 0
         and latent % 256 == 0
+        and args[12].shape[1] % (8 * nk) == 0
+        and args[12].shape[1] // nk >= 64
         and nope % 128 == 0
         and cache.shape[1] % 128 == 0
         and args[16].shape[2] == 64

time: 96.2 us -> 96.4 us (level)
  local copies, waits for them, and re-layouts: 5.55 us -> 3.81 us
  waiting for transfers between devices: 33.4 us -> 35.1 us
    all_to_all x1, waiting for transfers between devices: 6.09 us -> 8.46 us  [exchange(): return lax.all_to_all(message, axis, 0, 0, tiled=True)]
    unnamed x42 -> x38, local copies, waits for them, and re-layouts: 5.55 us -> 3.81 us
  transfers between devices with their start and end apart: 26 -> 26, of which waited for: 23 -> 24; matrix products, arithmetic and copies ran while one was open for 0% -> 0% of each run, Pallas kernels for 3% -> 3%
where the time goes in v5:
time: 96.4 us; the launch traced here: 96.1 us
  waiting for transfers between devices  35.1 us (36%)
  starting transfers between devices  31.8 us (33%)
  blocking collectives  14.2 us (15%)
  Pallas kernels  10.3 us (11%)
  local copies, waits for them, and re-layouts  3.81 us (4%)
    ppermute x21, starting transfers between devices, deal(): lax.ppermute(blocks[k], axis, [(i, i ^ k * step) for i in range(size)])  28.9 us
    ppermute x21, waiting for transfers between devices, deal(): lax.ppermute(blocks[k], axis, [(i, i ^ k * step) for i in range(size)])  23.1 us
    all_to_all x1, blocking collectives, exchange(): return lax.all_to_all(message, axis, 0, 0, tiled=True)  14.2 us
    pallas_call x18, Pallas kernels, call(): pl.pallas_call(kernel, out_shape=outs, in_specs=[VMEM] * len(args), out_s...  10.3 us
    all_to_all x1, waiting for transfers between devices, exchange(): return lax.all_to_all(message, axis, 0, 0, tiled=True)  8.46 us
    unnamed x38, local copies, waits for them, and re-layouts  3.81 us
    all_to_all x1, starting transfers between devices, exchange(): return lax.all_to_all(message, axis, 0, 0, tiled=True)  2.59 us
    ppermute x2, waiting for transfers between devices, kernel_body(): lax.ppermute(give, 'tp', swap)  2.39 us
  transfers between devices with their start and end apart: 26, of which 24 were waited for; matrix products, arithmetic and copies ran while one was open for 0% of the time, Pallas kernels for 3%

profile of v5, /device:TPU:0, one launch (start us, length us, event | category | flops | bytes accessed | tf_op | source)
XLA Modules:
  0.0 96.1 jit_solution(12605190327565352193)
XLA Ops:
  0.6 5.1 %collective-permute-start.2 = (bf16[4,1024]{1,0:T(4,128)(2,1)}, bf16[4,1024]{1,0:T(4,128)(2,1)S(1)}, u32[]{:S(2)}, u32[]{:S(2)}) collective-permute-start(bf16[4,1024]{1,0:T(4,128)(2,1)} %resid_ref.3), channel_id=1, source_target_pairs={{0,6},{1,7},{2,4},{3,5},{4,2},{5,3},{6,0},{7,1},{8,14},{9,15},{10,... | collective-permute-start | bytes 24584 | tf_op jit(solution)/shard_map/ppermute | solution.py:666
  7.6 2.9 %collective-permute-done.1.b2 = bf16[4,1024]{1,0:T(4,128)(2,1)S(1)} collective-permute-done((bf16[4,1024]{1,0:T(4,128)(2,1)}, bf16[4,1024]{1,0:T(4,128)(2,1)S(1)}, u32[]{:S(2)}, u32[]{:S(2)}) %collective-permute-start.1) | collective-permute-done | bytes 8224 | tf_op jit(solution)/shard_map/ppermute | solution.py:666
  13.3 1.6 %collective-permute-start.4 = (bf16[8,1920]{1,0:T(8,128)(2,1)S(1)}, bf16[8,1920]{1,0:T(8,128)(2,1)S(1)}, u32[]{:S(2)}, u32[]{:S(2)}) collective-permute-start(bf16[8,1920]{1,0:T(8,128)(2,1)S(1)} %get-tuple-element.43), channel_id=1, source_target_pairs={{0,8},{8,0},{16,24},{24,16},{1,9},{9,1},{17,25},{25,17},{2,10},{10... | collective-permute-start | bytes 92168 | tf_op jit(solution)/shard_map/ppermute | solution.py:666
  14.8 1.5 %collective-permute-start.5 = (bf16[8,1920]{1,0:T(8,128)(2,1)S(1)}, bf16[8,1920]{1,0:T(8,128)(2,1)S(1)}, u32[]{:S(2)}, u32[]{:S(2)}) collective-permute-start(bf16[8,1920]{1,0:T(8,128)(2,1)S(1)} %get-tuple-element.44), channel_id=1, source_target_pairs={{0,16},{8,24},{16,0},{24,8},{1,17},{9,25},{17,1},{25,9},{2,18},{10... | collective-permute-start | bytes 92168 | tf_op jit(solution)/shard_map/ppermute | solution.py:666
  17.2 1.5 %collective-permute-done.5.b2 = bf16[8,1920]{1,0:T(8,128)(2,1)S(1)} collective-permute-done((bf16[8,1920]{1,0:T(8,128)(2,1)S(1)}, bf16[8,1920]{1,0:T(8,128)(2,1)S(1)}, u32[]{:S(2)}, u32[]{:S(2)}) %collective-permute-start.5) | collective-permute-done | bytes 30752 | tf_op jit(solution)/shard_map/ppermute | solution.py:666
  18.7 2.4 %collective-permute-done.6.b3 = bf16[8,1920]{1,0:T(8,128)(2,1)S(1)} collective-permute-done((bf16[8,1920]{1,0:T(8,128)(2,1)S(1)}, bf16[8,1920]{1,0:T(8,128)(2,1)S(1)}, u32[]{:S(2)}, u32[]{:S(2)}) %collective-permute-start.6) | collective-permute-done | bytes 30752 | tf_op jit(solution)/shard_map/ppermute | solution.py:666
  22.1 14.2 %all_to_all.10 = bf16[32,8,640]{2,1,0:T(8,128)(2,1)S(1)} all-to-all(bf16[32,8,640]{2,1,0:T(8,128)(2,1)S(1)} %bitcast.12), channel_id=1, replica_groups=mesh['kv'=4,'tp'=8] {'kv','tp'}, dimensions={0} | all-to-all | bytes 655360 | tf_op jit(solution)/shard_map/all_to_all | solution.py:659
  36.3 2.0 %shard_map.198 = bf16[4,64,640]{2,1,0:T(8,128)(2,1)} custom-call(bf16[4,64,640]{2,1,0:T(8,128)(2,1)S(1)} %bitcast.13, bf16[4,512,512]{2,1,0:T(8,128)(2,1)S(1)} %copy-done.5, bf16[4,64,512]{2,1,0:T(8,128)(2,1)S(1)} %bitcast.21, f32[8,640]{1,0:T(8,128)S(1)} %get-tuple-element.47.own_ref), custom_call_target="tpu_custom_call" | custom-call | flops 4000000000 | bytes 3035136 | tf_op jit(solution)/shard_map/pallas_call | solution.py:273
  38.3 2.6 %all-to-all-start.1 = ((bf16[32,8,640]{2,1,0:T(8,128)(2,1)}), bf16[32,8,640]{2,1,0:T(8,128)(2,1)S(1)}, u32[]{:S(2)}, u32[]{:S(2)}) async-start(bf16[32,8,640]{2,1,0:T(8,128)(2,1)} %bitcast.7), calls=%async_computation.1 | async-start | bytes 655360 | tf_op jit(solution)/shard_map/all_to_all | solution.py:659
  40.9 1.8 %copy-done.1 = bf16[1024,1376]{0,1:T(8,128)(2,1)S(1)} copy-done((bf16[1024,1376]{0,1:T(8,128)(2,1)S(1)}, bf16[1024,1376]{0,1:T(8,128)(2,1)}, u32[]{:S(2)}) %copy-start.1) | copy-done | bytes 2818072
  42.7 1.7 %shard_map.199 = (bf16[32,768]{1,0:T(8,128)(2,1)S(1)}, bf16[32,768]{1,0:T(8,128)(2,1)S(1)}, bf16[32,768]{1,0:T(8,128)(2,1)S(1)}, bf16[32,768]{1,0:T(8,128)(2,1)S(1)}) custom-call(bf16[32,1024]{1,0:T(8,128)(2,1)S(1)} %get-tuple-element.48.rows_ref, f32[8,1024]{1,0:T(8,128)S(1)} %get-tuple-element.40.gains_ref, bf16[1376,1024]{1,0:T(8,128)(2,1)S(1)} %bitcast.14, ...), custom_call_target="tpu_custom_call" | custom-call | flops 4000000000 | bytes 5931008 | tf_op jit(solution)/shard_map/pallas_call | solution.py:273
  44.4 8.5 %all-to-all-done.1 = bf16[32,8,640]{2,1,0:T(8,128)(2,1)S(1)} async-done(((bf16[32,8,640]{2,1,0:T(8,128)(2,1)}), bf16[32,8,640]{2,1,0:T(8,128)(2,1)S(1)}, u32[]{:S(2)}, u32[]{:S(2)}) %all-to-all-start.1) | async-done | bytes 327712 | tf_op jit(solution)/shard_map/all_to_all | solution.py:659
  52.9 1.2 %copy-done.10 = bf16[512,8,128]{2,1,0:T(8,128)(2,1)S(1)} copy-done((bf16[512,8,128]{2,1,0:T(8,128)(2,1)S(1)}, bf16[512,8,128]{2,1,0:T(8,128)(2,1)}, u32[]{:S(2)}) %copy-start.10) | copy-done | bytes 1048600
  55.8 2.3 %collective-permute-start.9 = (bf16[8,4096]{1,0:T(8,128)(2,1)S(1)}, bf16[8,4096]{1,0:T(8,128)(2,1)S(1)}, u32[]{:S(2)}, u32[]{:S(2)}) collective-permute-start(bf16[8,4096]{1,0:T(8,128)(2,1)S(1)} %get-tuple-element.56), channel_id=1, source_target_pairs={{0,24},{8,16},{16,8},{24,0},{1,25},{9,17},{17,9},{25,1},{2,26},{10... | collective-permute-start | bytes 196616 | tf_op jit(solution)/shard_map/ppermute | solution.py:666
  62.8 1.8 %collective-permute-start.13 = (bf16[32,512]{1,0:T(8,128)(2,1)S(1)}, bf16[32,512]{1,0:T(8,128)(2,1)S(1)}, u32[]{:S(2)}, u32[]{:S(2)}) collective-permute-start(bf16[32,512]{1,0:T(8,128)(2,1)S(1)} %shard_map.202.b0), channel_id=1, source_target_pairs={{0,6},{1,7},{2,4},{3,5},{4,2},{5,3},{6,0},{7,1},{8,14},{9,15},{10,... | collective-permute-start | bytes 98312 | tf_op jit(solution)/shard_map/ppermute | solution.py:666
  64.6 2.6 %collective-permute-start.11 = (bf16[32,512]{1,0:T(8,128)(2,1)S(1)}, bf16[32,512]{1,0:T(8,128)(2,1)S(1)}, u32[]{:S(2)}, u32[]{:S(2)}) collective-permute-start(bf16[32,512]{1,0:T(8,128)(2,1)S(1)} %shard_map.202.b0), channel_id=1, source_target_pairs={{0,2},{1,3},{2,0},{3,1},{4,6},{5,7},{6,4},{7,5},{8,10},{9,11},{10,... | collective-permute-start | bytes 98312 | tf_op jit(solution)/shard_map/ppermute | solution.py:666
  67.2 1.3 %collective-permute-done.13.b3 = bf16[32,512]{1,0:T(8,128)(2,1)S(1)} collective-permute-done((bf16[32,512]{1,0:T(8,128)(2,1)S(1)}, bf16[32,512]{1,0:T(8,128)(2,1)S(1)}, u32[]{:S(2)}, u32[]{:S(2)}) %collective-permute-start.13) | collective-permute-done | bytes 32800 | tf_op jit(solution)/shard_map/ppermute | solution.py:666
  73.0 1.4 %collective-permute-start.16 = (bf16[32,768]{1,0:T(8,128)(2,1)S(1)}, bf16[32,768]{1,0:T(8,128)(2,1)S(1)}, u32[]{:S(2)}, u32[]{:S(2)}) collective-permute-start(bf16[32,768]{1,0:T(8,128)(2,1)S(1)} %get-tuple-element.63), channel_id=1, source_target_pairs={{0,16},{8,24},{16,0},{24,8},{1,17},{9,25},{17,1},{25,9},{2,18},{10... | collective-permute-start | bytes 147464 | tf_op jit(solution)/shard_map/ppermute | solution.py:666
  77.1 2.3 %collective-permute-done.17.b3 = bf16[32,768]{1,0:T(8,128)(2,1)S(1)} collective-permute-done((bf16[32,768]{1,0:T(8,128)(2,1)S(1)}, bf16[32,768]{1,0:T(8,128)(2,1)S(1)}, u32[]{:S(2)}, u32[]{:S(2)}) %collective-permute-start.17) | collective-permute-done | bytes 49184 | tf_op jit(solution)/shard_map/ppermute | solution.py:666
  81.8 1.4 %collective-permute-start.18 = (bf16[32,344]{1,0:T(8,128)(2,1)S(1)}, bf16[32,344]{1,0:T(8,128)(2,1)S(1)}, u32[]{:S(2)}, u32[]{:S(2)}) collective-permute-start(bf16[32,344]{1,0:T(8,128)(2,1)S(1)} %get-tuple-element.66.hidden_ref), channel_id=1, source_target_pairs={{0,8},{8,0},{16,24},{24,16},{1,9},{9,1},{17,25},{25,17},{2,10},{10... | collective-permute-start | bytes 66056 | tf_op jit(solution)/shard_map/ppermute | solution.py:666
  87.5 1.5 %collective-permute-start.22 = (bf16[4,1024]{1,0:T(4,128)(2,1)S(1)}, bf16[4,1024]{1,0:T(4,128)(2,1)S(1)}, u32[]{:S(2)}, u32[]{:S(2)}) collective-permute-start(bf16[4,1024]{1,0:T(4,128)(2,1)S(1)} %get-tuple-element.70), channel_id=1, source_target_pairs={{0,2},{1,3},{2,0},{3,1},{4,6},{5,7},{6,4},{7,5},{8,10},{9,11},{10,... | collective-permute-start | bytes 24584 | tf_op jit(solution)/shard_map/ppermute | solution.py:666
  89.9 2.0 %collective-permute-start.24 = (bf16[4,1024]{1,0:T(4,128)(2,1)S(1)}, bf16[4,1024]{1,0:T(4,128)(2,1)S(1)}, u32[]{:S(2)}, u32[]{:S(2)}) collective-permute-start(bf16[4,1024]{1,0:T(4,128)(2,1)S(1)} %get-tuple-element.72), channel_id=1, source_target_pairs={{0,6},{1,7},{2,4},{3,5},{4,2},{5,3},{6,0},{7,1},{8,14},{9,15},{10,... | collective-permute-start | bytes 24584 | tf_op jit(solution)/shard_map/ppermute | solution.py:666
  91.9 1.7 %collective-permute-done.23.b2 = bf16[4,1024]{1,0:T(4,128)(2,1)S(1)} collective-permute-done((bf16[4,1024]{1,0:T(4,128)(2,1)S(1)}, bf16[4,1024]{1,0:T(4,128)(2,1)S(1)}, u32[]{:S(2)}, u32[]{:S(2)}) %collective-permute-start.23) | collective-permute-done | bytes 8224 | tf_op jit(solution)/shard_map/ppermute | solution.py:666
  93.6 1.7 %collective-permute-done.24.b3 = bf16[4,1024]{1,0:T(4,128)(2,1)S(1)} collective-permute-done((bf16[4,1024]{1,0:T(4,128)(2,1)S(1)}, bf16[4,1024]{1,0:T(4,128)(2,1)S(1)}, u32[]{:S(2)}, u32[]{:S(2)}) %collective-permute-start.24) | collective-permute-done | bytes 8224 | tf_op jit(solution)/shard_map/ppermute | solution.py:666
  (86 shorter events, 28.0 us)
Async XLA Ops:
  0.6 7.0 %collective-permute-start.2 = (bf16[4,1024]{1,0:T(4,128)(2,1)}, bf16[4,1024]{1,0:T(4,128)(2,1)S(1)}, u32[]{:S(2)}, u32[]{:S(2)}) collective-permute-start(bf16[4,1024]{1,0:T(4,128)(2,1)} %resid_ref.3), channel_id=1, source_target_pairs={{0,6},{1,7},{2,4},{3,5},{4,2},{5,3},{6,0},{7,1},{8,14},{9,15},{10,... | collective-permute-start | bytes 24584 | tf_op jit(solution)/shard_map/ppermute | solution.py:666
  5.8 4.8 %collective-permute-start.1 = (bf16[4,1024]{1,0:T(4,128)(2,1)}, bf16[4,1024]{1,0:T(4,128)(2,1)S(1)}, u32[]{:S(2)}, u32[]{:S(2)}) collective-permute-start(bf16[4,1024]{1,0:T(4,128)(2,1)} %resid_ref.3), channel_id=1, source_target_pairs={{0,4},{1,5},{2,6},{3,7},{4,0},{5,1},{6,2},{7,3},{8,12},{9,13},{10,... | collective-permute-start | bytes 24584 | tf_op jit(solution)/shard_map/ppermute | solution.py:666
  5.8 4.8 %collective-permute-start = (bf16[4,1024]{1,0:T(4,128)(2,1)}, bf16[4,1024]{1,0:T(4,128)(2,1)S(1)}, u32[]{:S(2)}, u32[]{:S(2)}) collective-permute-start(bf16[4,1024]{1,0:T(4,128)(2,1)} %resid_ref.3), channel_id=1, source_target_pairs={{0,2},{1,3},{2,0},{3,1},{4,6},{5,7},{6,4},{7,5},{8,10},{9,11},{10,... | collective-permute-start | bytes 24584 | tf_op jit(solution)/shard_map/ppermute | solution.py:666
  10.6 1.3 %collective-permute-start.3 = (bf16[16,1024]{1,0:T(8,128)(2,1)S(1)}, bf16[16,1024]{1,0:T(8,128)(2,1)S(1)}, u32[]{:S(2)}, u32[]{:S(2)}) collective-permute-start(bf16[16,1024]{1,0:T(8,128)(2,1)S(1)} %shard_map.194.half_ref), channel_id=1, source_target_pairs={{0,1},{1,0},{2,3},{3,2},{4,5},{5,4},{6,7},{7,6},{8,9},{9,8},{10,11... | collective-permute-start | bytes 98312 | tf_op jit(solution)/shard_map/ppermute | solution.py:732
  13.3 4.0 %collective-permute-start.4 = (bf16[8,1920]{1,0:T(8,128)(2,1)S(1)}, bf16[8,1920]{1,0:T(8,128)(2,1)S(1)}, u32[]{:S(2)}, u32[]{:S(2)}) collective-permute-start(bf16[8,1920]{1,0:T(8,128)(2,1)S(1)} %get-tuple-element.43), channel_id=1, source_target_pairs={{0,8},{8,0},{16,24},{24,16},{1,9},{9,1},{17,25},{25,17},{2,10},{10... | collective-permute-start | bytes 92168 | tf_op jit(solution)/shard_map/ppermute | solution.py:666
  14.8 3.9 %collective-permute-start.5 = (bf16[8,1920]{1,0:T(8,128)(2,1)S(1)}, bf16[8,1920]{1,0:T(8,128)(2,1)S(1)}, u32[]{:S(2)}, u32[]{:S(2)}) collective-permute-start(bf16[8,1920]{1,0:T(8,128)(2,1)S(1)} %get-tuple-element.44), channel_id=1, source_target_pairs={{0,16},{8,24},{16,0},{24,8},{1,17},{9,25},{17,1},{25,9},{2,18},{10... | collective-permute-start | bytes 92168 | tf_op jit(solution)/shard_map/ppermute | solution.py:666
  16.3 4.8 %collective-permute-start.6 = (bf16[8,1920]{1,0:T(8,128)(2,1)S(1)}, bf16[8,1920]{1,0:T(8,128)(2,1)S(1)}, u32[]{:S(2)}, u32[]{:S(2)}) collective-permute-start(bf16[8,1920]{1,0:T(8,128)(2,1)S(1)} %get-tuple-element.45), channel_id=1, source_target_pairs={{0,24},{8,16},{16,8},{24,0},{1,25},{9,17},{17,9},{25,1},{2,26},{10... | collective-permute-start | bytes 92168 | tf_op jit(solution)/shard_map/ppermute | solution.py:666
  38.3 14.6 %all-to-all-start.1 = ((bf16[32,8,640]{2,1,0:T(8,128)(2,1)}), bf16[32,8,640]{2,1,0:T(8,128)(2,1)S(1)}, u32[]{:S(2)}, u32[]{:S(2)}) async-start(bf16[32,8,640]{2,1,0:T(8,128)(2,1)} %bitcast.7), calls=%async_computation.1 | async-start | bytes 655360 | tf_op jit(solution)/shard_map/all_to_all | solution.py:659
  54.6 4.3 %collective-permute-start.7 = (bf16[8,4096]{1,0:T(8,128)(2,1)S(1)}, bf16[8,4096]{1,0:T(8,128)(2,1)S(1)}, u32[]{:S(2)}, u32[]{:S(2)}) collective-permute-start(bf16[8,4096]{1,0:T(8,128)(2,1)S(1)} %get-tuple-element.54), channel_id=1, source_target_pairs={{0,8},{8,0},{16,24},{24,16},{1,9},{9,1},{17,25},{25,17},{2,10},{10... | collective-permute-start | bytes 196616 | tf_op jit(solution)/shard_map/ppermute | solution.py:666
  54.7 5.4 %collective-permute-start.8 = (bf16[8,4096]{1,0:T(8,128)(2,1)S(1)}, bf16[8,4096]{1,0:T(8,128)(2,1)S(1)}, u32[]{:S(2)}, u32[]{:S(2)}) collective-permute-start(bf16[8,4096]{1,0:T(8,128)(2,1)S(1)} %get-tuple-element.55), channel_id=1, source_target_pairs={{0,16},{8,24},{16,0},{24,8},{1,17},{9,25},{17,1},{25,9},{2,18},{10... | collective-permute-start | bytes 196616 | tf_op jit(solution)/shard_map/ppermute | solution.py:666
  55.8 5.2 %collective-permute-start.9 = (bf16[8,4096]{1,0:T(8,128)(2,1)S(1)}, bf16[8,4096]{1,0:T(8,128)(2,1)S(1)}, u32[]{:S(2)}, u32[]{:S(2)}) collective-permute-start(bf16[8,4096]{1,0:T(8,128)(2,1)S(1)} %get-tuple-element.56), channel_id=1, source_target_pairs={{0,24},{8,16},{16,8},{24,0},{1,25},{9,17},{17,9},{25,1},{2,26},{10... | collective-permute-start | bytes 196616 | tf_op jit(solution)/shard_map/ppermute | solution.py:666
  61.5 1.3 %collective-permute-start.10 = (bf16[32,512]{1,0:T(8,128)(2,1)S(1)}, bf16[32,512]{1,0:T(8,128)(2,1)S(1)}, u32[]{:S(2)}, u32[]{:S(2)}) collective-permute-start(bf16[32,512]{1,0:T(8,128)(2,1)S(1)} %get-tuple-element.58), channel_id=1, source_target_pairs={{0,1},{1,0},{2,3},{3,2},{4,5},{5,4},{6,7},{7,6},{8,9},{9,8},{10,11... | collective-permute-start | bytes 98312 | tf_op jit(solution)/shard_map/ppermute | solution.py:797
  62.8 5.8 %collective-permute-start.13 = (bf16[32,512]{1,0:T(8,128)(2,1)S(1)}, bf16[32,512]{1,0:T(8,128)(2,1)S(1)}, u32[]{:S(2)}, u32[]{:S(2)}) collective-permute-start(bf16[32,512]{1,0:T(8,128)(2,1)S(1)} %shard_map.202.b0), channel_id=1, source_target_pairs={{0,6},{1,7},{2,4},{3,5},{4,2},{5,3},{6,0},{7,1},{8,14},{9,15},{10,... | collective-permute-start | bytes 98312 | tf_op jit(solution)/shard_map/ppermute | solution.py:666
  64.6 4.9 %collective-permute-start.12 = (bf16[32,512]{1,0:T(8,128)(2,1)S(1)}, bf16[32,512]{1,0:T(8,128)(2,1)S(1)}, u32[]{:S(2)}, u32[]{:S(2)}) collective-permute-start(bf16[32,512]{1,0:T(8,128)(2,1)S(1)} %shard_map.202.b0), channel_id=1, source_target_pairs={{0,4},{1,5},{2,6},{3,7},{4,0},{5,1},{6,2},{7,3},{8,12},{9,13},{10,... | collective-permute-start | bytes 98312 | tf_op jit(solution)/shard_map/ppermute | solution.py:666
  64.6 5.1 %collective-permute-start.11 = (bf16[32,512]{1,0:T(8,128)(2,1)S(1)}, bf16[32,512]{1,0:T(8,128)(2,1)S(1)}, u32[]{:S(2)}, u32[]{:S(2)}) collective-permute-start(bf16[32,512]{1,0:T(8,128)(2,1)S(1)} %shard_map.202.b0), channel_id=1, source_target_pairs={{0,2},{1,3},{2,0},{3,1},{4,6},{5,7},{6,4},{7,5},{8,10},{9,11},{10,... | collective-permute-start | bytes 98312 | tf_op jit(solution)/shard_map/ppermute | solution.py:666
  72.0 4.2 %collective-permute-start.15 = (bf16[32,768]{1,0:T(8,128)(2,1)S(1)}, bf16[32,768]{1,0:T(8,128)(2,1)S(1)}, u32[]{:S(2)}, u32[]{:S(2)}) collective-permute-start(bf16[32,768]{1,0:T(8,128)(2,1)S(1)} %get-tuple-element.62), channel_id=1, source_target_pairs={{0,8},{8,0},{16,24},{24,16},{1,9},{9,1},{17,25},{25,17},{2,10},{10... | collective-permute-start | bytes 147464 | tf_op jit(solution)/shard_map/ppermute | solution.py:666
  73.0 4.1 %collective-permute-start.16 = (bf16[32,768]{1,0:T(8,128)(2,1)S(1)}, bf16[32,768]{1,0:T(8,128)(2,1)S(1)}, u32[]{:S(2)}, u32[]{:S(2)}) collective-permute-start(bf16[32,768]{1,0:T(8,128)(2,1)S(1)} %get-tuple-element.63), channel_id=1, source_target_pairs={{0,16},{8,24},{16,0},{24,8},{1,17},{9,25},{17,1},{25,9},{2,18},{10... | collective-permute-start | bytes 147464 | tf_op jit(solution)/shard_map/ppermute | solution.py:666
  74.4 5.0 %collective-permute-start.17 = (bf16[32,768]{1,0:T(8,128)(2,1)S(1)}, bf16[32,768]{1,0:T(8,128)(2,1)S(1)}, u32[]{:S(2)}, u32[]{:S(2)}) collective-permute-start(bf16[32,768]{1,0:T(8,128)(2,1)S(1)} %get-tuple-element.64), channel_id=1, source_target_pairs={{0,24},{8,16},{16,8},{24,0},{1,25},{9,17},{17,9},{25,1},{2,26},{10... | collective-permute-start | bytes 147464 | tf_op jit(solution)/shard_map/ppermute | solution.py:666
  79.6 4.8 %collective-permute-start.20 = (bf16[32,344]{1,0:T(8,128)(2,1)S(1)}, bf16[32,344]{1,0:T(8,128)(2,1)S(1)}, u32[]{:S(2)}, u32[]{:S(2)}) collective-permute-start(bf16[32,344]{1,0:T(8,128)(2,1)S(1)} %get-tuple-element.66.hidden_ref), channel_id=1, source_target_pairs={{0,24},{8,16},{16,8},{24,0},{1,25},{9,17},{17,9},{25,1},{2,26},{10... | collective-permute-start | bytes 66056 | tf_op jit(solution)/shard_map/ppermute | solution.py:666
  80.8 3.8 %collective-permute-start.19 = (bf16[32,344]{1,0:T(8,128)(2,1)S(1)}, bf16[32,344]{1,0:T(8,128)(2,1)S(1)}, u32[]{:S(2)}, u32[]{:S(2)}) collective-permute-start(bf16[32,344]{1,0:T(8,128)(2,1)S(1)} %get-tuple-element.66.hidden_ref), channel_id=1, source_target_pairs={{0,16},{8,24},{16,0},{24,8},{1,17},{9,25},{17,1},{25,9},{2,18},{10... | collective-permute-start | bytes 66056 | tf_op jit(solution)/shard_map/ppermute | solution.py:666
  81.8 3.8 %collective-permute-start.18 = (bf16[32,344]{1,0:T(8,128)(2,1)S(1)}, bf16[32,344]{1,0:T(8,128)(2,1)S(1)}, u32[]{:S(2)}, u32[]{:S(2)}) collective-permute-start(bf16[32,344]{1,0:T(8,128)(2,1)S(1)} %get-tuple-element.66.hidden_ref), channel_id=1, source_target_pairs={{0,8},{8,0},{16,24},{24,16},{1,9},{9,1},{17,25},{25,17},{2,10},{10... | collective-permute-start | bytes 66056 | tf_op jit(solution)/shard_map/ppermute | solution.py:666
  87.5 4.5 %collective-permute-start.22 = (bf16[4,1024]{1,0:T(4,128)(2,1)S(1)}, bf16[4,1024]{1,0:T(4,128)(2,1)S(1)}, u32[]{:S(2)}, u32[]{:S(2)}) collective-permute-start(bf16[4,1024]{1,0:T(4,128)(2,1)S(1)} %get-tuple-element.70), channel_id=1, source_target_pairs={{0,2},{1,3},{2,0},{3,1},{4,6},{5,7},{6,4},{7,5},{8,10},{9,11},{10,... | collective-permute-start | bytes 24584 | tf_op jit(solution)/shard_map/ppermute | solution.py:666
  89.0 4.6 %collective-permute-start.23 = (bf16[4,1024]{1,0:T(4,128)(2,1)S(1)}, bf16[4,1024]{1,0:T(4,128)(2,1)S(1)}, u32[]{:S(2)}, u32[]{:S(2)}) collective-permute-start(bf16[4,1024]{1,0:T(4,128)(2,1)S(1)} %get-tuple-element.71), channel_id=1, source_target_pairs={{0,4},{1,5},{2,6},{3,7},{4,0},{5,1},{6,2},{7,3},{8,12},{9,13},{10,... | collective-permute-start | bytes 24584 | tf_op jit(solution)/shard_map/ppermute | solution.py:666
  89.9 5.4 %collective-permute-start.24 = (bf16[4,1024]{1,0:T(4,128)(2,1)S(1)}, bf16[4,1024]{1,0:T(4,128)(2,1)S(1)}, u32[]{:S(2)}, u32[]{:S(2)}) collective-permute-start(bf16[4,1024]{1,0:T(4,128)(2,1)S(1)} %get-tuple-element.72), channel_id=1, source_target_pairs={{0,6},{1,7},{2,4},{3,5},{4,2},{5,3},{6,0},{7,1},{8,14},{9,15},{10,... | collective-permute-start | bytes 24584 | tf_op jit(solution)/shard_map/ppermute | solution.py:666
  (21 other events, 113.8 us)

commit v6 on v5

--- a/solution.py
+++ b/solution.py
@@ -405,15 +405,15 @@
 
 
 def latent_kernel(
-    model_width, b0, b1, b2, b3, ku_ref, gain_ref, table_ref, unit_ref,
-    msg_ref, lat_ref, key_ref, own_ref,
+    model_width, own, b0, b1, b2, b3, ku_ref, gain_ref, table_ref, unit_ref,
+    msg_ref, own_ref,
 ):
     nk, pairs, _ = msg_ref.shape
     nt = b0.shape[0]
     heads = pairs // nt
     latent, _, nope = ku_ref.shape
     nope_dev = heads * nope
-    own, rope = key_ref.shape
+    rope = unit_ref.shape[1] // 2
     rope_dev = heads * rope
     total = four((b0, b1, b2, b3))
     base, half = nope_dev + rope_dev, latent // 2
@@ -426,8 +426,6 @@
     lat = (lat * gain_ref[...].astype(F32)).astype(BF)
     table = table_ref[...]
     key = turned(stat * own_scale, table, rope // 2).astype(BF)
-    lat_ref[...] = lat[:own]
-    key_ref[...] = key[:own, :rope]
     own_ref[:, :latent] = lat.astype(F32)
     own_ref[:, latent:] = key.astype(F32)
     qn = total[:, :nope_dev].astype(BF).astype(F32)
@@ -644,7 +642,9 @@
         ref[...] = (keep_ref[k] + got_ref[k].astype(F32)).astype(BF)
 
 
-def last_kernel(b0, b1, b2, b3, resid_ref, post_ref, s_ref, out_ref):
+def last_kernel(
+    b0, b1, b2, b3, resid_ref, post_ref, s_ref, own_ref, out_ref, lat_ref, key_ref
+):
     own, width = resid_ref.shape
     nt = post_ref.shape[0] // own
     total = four((b0, b1, b2, b3))
@@ -653,6 +653,9 @@
     mine = jnp.sum(jnp.where(here, added, 0.0), axis=1)
     mid = (resid_ref[...].astype(F32) + mine).astype(BF).astype(F32)
     out_ref[...] = (mid + total).astype(BF)
+    latent, rope = lat_ref.shape[1], key_ref.shape[1]
+    lat_ref[...] = own_ref[:own, :latent].astype(BF)
+    key_ref[...] = own_ref[:own, latent : latent + rope].astype(BF)
 
 
 def exchange(message, axis):
@@ -750,14 +753,9 @@
         scratch=[pltpu.VMEM((nk, rows, wide), BF)],
         flops=WAIT,
     )[::-1]
-    msg, new_latent, new_rope_key, own_block = call(
-        functools.partial(latent_kernel, model_width),
-        [
-            like((nk, pairs, latent + 128)),
-            like((own, latent)),
-            like((own, rope)),
-            like((nt, latent + 128), F32),
-        ],
+    msg, own_block = call(
+        functools.partial(latent_kernel, model_width, own),
+        [like((nk, pairs, latent + 128)), like((nt, latent + 128), F32)],
         *deal(msg[::-1], "kv"),
         key_up,
         latent_gain.reshape(1, latent),
@@ -844,8 +842,15 @@
         lax.ppermute(give, "tp", swap),
         flops=WAIT,
     )
-    next_resid = call(
-        last_kernel, like((own, width)), *deal(msg[::-1], "tp", 2), resid, post, s, flops=WAIT
+    next_resid, new_latent, new_rope_key = call(
+        last_kernel,
+        [like((own, width)), like((own, latent)), like((own, rope))],
+        *deal(msg[::-1], "tp", 2),
+        resid,
+        post,
+        s,
+        own_block,
+        flops=WAIT,
     )
     return (next_resid, new_latent, new_rope_key)
 

time: 96.4 us -> 95.9 us (level)
  no operation moved by 1% of the time
where the time goes in v6:
time: 95.9 us; the launch traced here: 95.6 us
  waiting for transfers between devices  35.1 us (37%)
  starting transfers between devices  31.8 us (33%)
  blocking collectives  14.2 us (15%)
  Pallas kernels  9.77 us (10%)
  local copies, waits for them, and re-layouts  3.81 us (4%)
    ppermute x21, starting transfers between devices, deal(): lax.ppermute(blocks[k], axis, [(i, i ^ k * step) for i in range(size)])  28.9 us
    ppermute x21, waiting for transfers between devices, deal(): lax.ppermute(blocks[k], axis, [(i, i ^ k * step) for i in range(size)])  23.1 us
    all_to_all x1, blocking collectives, exchange(): return lax.all_to_all(message, axis, 0, 0, tiled=True)  14.2 us
    pallas_call x18, Pallas kernels, call(): pl.pallas_call(kernel, out_shape=outs, in_specs=[VMEM] * len(args), out_s...  9.77 us
    all_to_all x1, waiting for transfers between devices, exchange(): return lax.all_to_all(message, axis, 0, 0, tiled=True)  8.46 us
    unnamed x38, local copies, waits for them, and re-layouts  3.81 us
    all_to_all x1, starting transfers between devices, exchange(): return lax.all_to_all(message, axis, 0, 0, tiled=True)  2.59 us
    ppermute x2, waiting for transfers between devices, kernel_body(): lax.ppermute(give, 'tp', swap)  2.39 us
  transfers between devices with their start and end apart: 26, of which 24 were waited for; matrix products, arithmetic and copies ran while one was open for 0% of the time, Pallas kernels for 3%

profile of v6, /device:TPU:0, one launch (start us, length us, event | category | flops | bytes accessed | tf_op | source)
XLA Modules:
  0.0 95.6 jit_solution(3069790810191751117)
XLA Ops:
  0.6 5.1 %collective-permute-start.2 = (bf16[4,1024]{1,0:T(4,128)(2,1)}, bf16[4,1024]{1,0:T(4,128)(2,1)S(1)}, u32[]{:S(2)}, u32[]{:S(2)}) collective-permute-start(bf16[4,1024]{1,0:T(4,128)(2,1)} %resid_ref.3), channel_id=1, source_target_pairs={{0,6},{1,7},{2,4},{3,5},{4,2},{5,3},{6,0},{7,1},{8,14},{9,15},{10,... | collective-permute-start | bytes 24584 | tf_op jit(solution)/shard_map/ppermute | solution.py:669
  7.6 2.9 %collective-permute-done.1.b2 = bf16[4,1024]{1,0:T(4,128)(2,1)S(1)} collective-permute-done((bf16[4,1024]{1,0:T(4,128)(2,1)}, bf16[4,1024]{1,0:T(4,128)(2,1)S(1)}, u32[]{:S(2)}, u32[]{:S(2)}) %collective-permute-start.1) | collective-permute-done | bytes 8224 | tf_op jit(solution)/shard_map/ppermute | solution.py:669
  13.3 1.6 %collective-permute-start.4 = (bf16[8,1920]{1,0:T(8,128)(2,1)S(1)}, bf16[8,1920]{1,0:T(8,128)(2,1)S(1)}, u32[]{:S(2)}, u32[]{:S(2)}) collective-permute-start(bf16[8,1920]{1,0:T(8,128)(2,1)S(1)} %get-tuple-element.41), channel_id=1, source_target_pairs={{0,8},{8,0},{16,24},{24,16},{1,9},{9,1},{17,25},{25,17},{2,10},{10... | collective-permute-start | bytes 92168 | tf_op jit(solution)/shard_map/ppermute | solution.py:669
  14.8 1.5 %collective-permute-start.5 = (bf16[8,1920]{1,0:T(8,128)(2,1)S(1)}, bf16[8,1920]{1,0:T(8,128)(2,1)S(1)}, u32[]{:S(2)}, u32[]{:S(2)}) collective-permute-start(bf16[8,1920]{1,0:T(8,128)(2,1)S(1)} %get-tuple-element.42), channel_id=1, source_target_pairs={{0,16},{8,24},{16,0},{24,8},{1,17},{9,25},{17,1},{25,9},{2,18},{10... | collective-permute-start | bytes 92168 | tf_op jit(solution)/shard_map/ppermute | solution.py:669
  17.2 1.5 %collective-permute-done.5.b2 = bf16[8,1920]{1,0:T(8,128)(2,1)S(1)} collective-permute-done((bf16[8,1920]{1,0:T(8,128)(2,1)S(1)}, bf16[8,1920]{1,0:T(8,128)(2,1)S(1)}, u32[]{:S(2)}, u32[]{:S(2)}) %collective-permute-start.5) | collective-permute-done | bytes 30752 | tf_op jit(solution)/shard_map/ppermute | solution.py:669
  18.7 2.4 %collective-permute-done.6.b3 = bf16[8,1920]{1,0:T(8,128)(2,1)S(1)} collective-permute-done((bf16[8,1920]{1,0:T(8,128)(2,1)S(1)}, bf16[8,1920]{1,0:T(8,128)(2,1)S(1)}, u32[]{:S(2)}, u32[]{:S(2)}) %collective-permute-start.6) | collective-permute-done | bytes 30752 | tf_op jit(solution)/shard_map/ppermute | solution.py:669
  21.6 14.2 %all_to_all.10 = bf16[32,8,640]{2,1,0:T(8,128)(2,1)S(1)} all-to-all(bf16[32,8,640]{2,1,0:T(8,128)(2,1)S(1)} %bitcast.12), channel_id=1, replica_groups=mesh['kv'=4,'tp'=8] {'kv','tp'}, dimensions={0} | all-to-all | bytes 655360 | tf_op jit(solution)/shard_map/all_to_all | solution.py:662
  35.8 2.0 %shard_map.198 = bf16[4,64,640]{2,1,0:T(8,128)(2,1)} custom-call(bf16[4,64,640]{2,1,0:T(8,128)(2,1)S(1)} %bitcast.13, bf16[4,512,512]{2,1,0:T(8,128)(2,1)S(1)} %copy-done.5, bf16[4,64,512]{2,1,0:T(8,128)(2,1)S(1)} %bitcast.21, f32[8,640]{1,0:T(8,128)S(1)} %get-tuple-element.45.own_ref), custom_call_target="tpu_custom_call" | custom-call | flops 4000000000 | bytes 3035136 | tf_op jit(solution)/shard_map/pallas_call | solution.py:273
  37.8 2.6 %all-to-all-start.1 = ((bf16[32,8,640]{2,1,0:T(8,128)(2,1)}), bf16[32,8,640]{2,1,0:T(8,128)(2,1)S(1)}, u32[]{:S(2)}, u32[]{:S(2)}) async-start(bf16[32,8,640]{2,1,0:T(8,128)(2,1)} %bitcast.7), calls=%async_computation.1 | async-start | bytes 655360 | tf_op jit(solution)/shard_map/all_to_all | solution.py:662
  40.4 1.8 %copy-done.1 = bf16[1024,1376]{0,1:T(8,128)(2,1)S(1)} copy-done((bf16[1024,1376]{0,1:T(8,128)(2,1)S(1)}, bf16[1024,1376]{0,1:T(8,128)(2,1)}, u32[]{:S(2)}) %copy-start.1) | copy-done | bytes 2818072
  42.2 1.7 %shard_map.199 = (bf16[32,768]{1,0:T(8,128)(2,1)S(1)}, bf16[32,768]{1,0:T(8,128)(2,1)S(1)}, bf16[32,768]{1,0:T(8,128)(2,1)S(1)}, bf16[32,768]{1,0:T(8,128)(2,1)S(1)}) custom-call(bf16[32,1024]{1,0:T(8,128)(2,1)S(1)} %get-tuple-element.46.rows_ref, f32[8,1024]{1,0:T(8,128)S(1)} %get-tuple-element.38.gains_ref, bf16[1376,1024]{1,0:T(8,128)(2,1)S(1)} %bitcast.14, ...), custom_call_target="tpu_custom_call" | custom-call | flops 4000000000 | bytes 5931008 | tf_op jit(solution)/shard_map/pallas_call | solution.py:273
  44.0 8.5 %all-to-all-done.1 = bf16[32,8,640]{2,1,0:T(8,128)(2,1)S(1)} async-done(((bf16[32,8,640]{2,1,0:T(8,128)(2,1)}), bf16[32,8,640]{2,1,0:T(8,128)(2,1)S(1)}, u32[]{:S(2)}, u32[]{:S(2)}) %all-to-all-start.1) | async-done | bytes 327712 | tf_op jit(solution)/shard_map/all_to_all | solution.py:662
  52.4 1.2 %copy-done.10 = bf16[512,8,128]{2,1,0:T(8,128)(2,1)S(1)} copy-done((bf16[512,8,128]{2,1,0:T(8,128)(2,1)S(1)}, bf16[512,8,128]{2,1,0:T(8,128)(2,1)}, u32[]{:S(2)}) %copy-start.10) | copy-done | bytes 1048600
  55.3 2.3 %collective-permute-start.9 = (bf16[8,4096]{1,0:T(8,128)(2,1)S(1)}, bf16[8,4096]{1,0:T(8,128)(2,1)S(1)}, u32[]{:S(2)}, u32[]{:S(2)}) collective-permute-start(bf16[8,4096]{1,0:T(8,128)(2,1)S(1)} %get-tuple-element.54), channel_id=1, source_target_pairs={{0,24},{8,16},{16,8},{24,0},{1,25},{9,17},{17,9},{25,1},{2,26},{10... | collective-permute-start | bytes 196616 | tf_op jit(solution)/shard_map/ppermute | solution.py:669
  62.3 1.8 %collective-permute-start.13 = (bf16[32,512]{1,0:T(8,128)(2,1)S(1)}, bf16[32,512]{1,0:T(8,128)(2,1)S(1)}, u32[]{:S(2)}, u32[]{:S(2)}) collective-permute-start(bf16[32,512]{1,0:T(8,128)(2,1)S(1)} %shard_map.202.b0), channel_id=1, source_target_pairs={{0,6},{1,7},{2,4},{3,5},{4,2},{5,3},{6,0},{7,1},{8,14},{9,15},{10,... | collective-permute-start | bytes 98312 | tf_op jit(solution)/shard_map/ppermute | solution.py:669
  64.1 2.6 %collective-permute-start.11 = (bf16[32,512]{1,0:T(8,128)(2,1)S(1)}, bf16[32,512]{1,0:T(8,128)(2,1)S(1)}, u32[]{:S(2)}, u32[]{:S(2)}) collective-permute-start(bf16[32,512]{1,0:T(8,128)(2,1)S(1)} %shard_map.202.b0), channel_id=1, source_target_pairs={{0,2},{1,3},{2,0},{3,1},{4,6},{5,7},{6,4},{7,5},{8,10},{9,11},{10,... | collective-permute-start | bytes 98312 | tf_op jit(solution)/shard_map/ppermute | solution.py:669
  66.7 1.3 %collective-permute-done.13.b3 = bf16[32,512]{1,0:T(8,128)(2,1)S(1)} collective-permute-done((bf16[32,512]{1,0:T(8,128)(2,1)S(1)}, bf16[32,512]{1,0:T(8,128)(2,1)S(1)}, u32[]{:S(2)}, u32[]{:S(2)}) %collective-permute-start.13) | collective-permute-done | bytes 32800 | tf_op jit(solution)/shard_map/ppermute | solution.py:669
  72.5 1.4 %collective-permute-start.16 = (bf16[32,768]{1,0:T(8,128)(2,1)S(1)}, bf16[32,768]{1,0:T(8,128)(2,1)S(1)}, u32[]{:S(2)}, u32[]{:S(2)}) collective-permute-start(bf16[32,768]{1,0:T(8,128)(2,1)S(1)} %get-tuple-element.61), channel_id=1, source_target_pairs={{0,16},{8,24},{16,0},{24,8},{1,17},{9,25},{17,1},{25,9},{2,18},{10... | collective-permute-start | bytes 147464 | tf_op jit(solution)/shard_map/ppermute | solution.py:669
  76.6 2.3 %collective-permute-done.17.b3 = bf16[32,768]{1,0:T(8,128)(2,1)S(1)} collective-permute-done((bf16[32,768]{1,0:T(8,128)(2,1)S(1)}, bf16[32,768]{1,0:T(8,128)(2,1)S(1)}, u32[]{:S(2)}, u32[]{:S(2)}) %collective-permute-start.17) | collective-permute-done | bytes 49184 | tf_op jit(solution)/shard_map/ppermute | solution.py:669
  81.3 1.4 %collective-permute-start.18 = (bf16[32,344]{1,0:T(8,128)(2,1)S(1)}, bf16[32,344]{1,0:T(8,128)(2,1)S(1)}, u32[]{:S(2)}, u32[]{:S(2)}) collective-permute-start(bf16[32,344]{1,0:T(8,128)(2,1)S(1)} %get-tuple-element.64.hidden_ref), channel_id=1, source_target_pairs={{0,8},{8,0},{16,24},{24,16},{1,9},{9,1},{17,25},{25,17},{2,10},{10... | collective-permute-start | bytes 66056 | tf_op jit(solution)/shard_map/ppermute | solution.py:669
  87.0 1.5 %collective-permute-start.22 = (bf16[4,1024]{1,0:T(4,128)(2,1)S(1)}, bf16[4,1024]{1,0:T(4,128)(2,1)S(1)}, u32[]{:S(2)}, u32[]{:S(2)}) collective-permute-start(bf16[4,1024]{1,0:T(4,128)(2,1)S(1)} %get-tuple-element.68), channel_id=1, source_target_pairs={{0,2},{1,3},{2,0},{3,1},{4,6},{5,7},{6,4},{7,5},{8,10},{9,11},{10,... | collective-permute-start | bytes 24584 | tf_op jit(solution)/shard_map/ppermute | solution.py:669
  89.4 2.0 %collective-permute-start.24 = (bf16[4,1024]{1,0:T(4,128)(2,1)S(1)}, bf16[4,1024]{1,0:T(4,128)(2,1)S(1)}, u32[]{:S(2)}, u32[]{:S(2)}) collective-permute-start(bf16[4,1024]{1,0:T(4,128)(2,1)S(1)} %get-tuple-element.70), channel_id=1, source_target_pairs={{0,6},{1,7},{2,4},{3,5},{4,2},{5,3},{6,0},{7,1},{8,14},{9,15},{10,... | collective-permute-start | bytes 24584 | tf_op jit(solution)/shard_map/ppermute | solution.py:669
  91.5 1.7 %collective-permute-done.23.b2 = bf16[4,1024]{1,0:T(4,128)(2,1)S(1)} collective-permute-done((bf16[4,1024]{1,0:T(4,128)(2,1)S(1)}, bf16[4,1024]{1,0:T(4,128)(2,1)S(1)}, u32[]{:S(2)}, u32[]{:S(2)}) %collective-permute-start.23) | collective-permute-done | bytes 8224 | tf_op jit(solution)/shard_map/ppermute | solution.py:669
  93.2 1.7 %collective-permute-done.24.b3 = bf16[4,1024]{1,0:T(4,128)(2,1)S(1)} collective-permute-done((bf16[4,1024]{1,0:T(4,128)(2,1)S(1)}, bf16[4,1024]{1,0:T(4,128)(2,1)S(1)}, u32[]{:S(2)}, u32[]{:S(2)}) %collective-permute-start.24) | collective-permute-done | bytes 8224 | tf_op jit(solution)/shard_map/ppermute | solution.py:669
  (86 shorter events, 27.5 us)
Async XLA Ops:
  0.6 7.0 %collective-permute-start.2 = (bf16[4,1024]{1,0:T(4,128)(2,1)}, bf16[4,1024]{1,0:T(4,128)(2,1)S(1)}, u32[]{:S(2)}, u32[]{:S(2)}) collective-permute-start(bf16[4,1024]{1,0:T(4,128)(2,1)} %resid_ref.3), channel_id=1, source_target_pairs={{0,6},{1,7},{2,4},{3,5},{4,2},{5,3},{6,0},{7,1},{8,14},{9,15},{10,... | collective-permute-start | bytes 24584 | tf_op jit(solution)/shard_map/ppermute | solution.py:669
  5.8 4.8 %collective-permute-start.1 = (bf16[4,1024]{1,0:T(4,128)(2,1)}, bf16[4,1024]{1,0:T(4,128)(2,1)S(1)}, u32[]{:S(2)}, u32[]{:S(2)}) collective-permute-start(bf16[4,1024]{1,0:T(4,128)(2,1)} %resid_ref.3), channel_id=1, source_target_pairs={{0,4},{1,5},{2,6},{3,7},{4,0},{5,1},{6,2},{7,3},{8,12},{9,13},{10,... | collective-permute-start | bytes 24584 | tf_op jit(solution)/shard_map/ppermute | solution.py:669
  5.8 4.8 %collective-permute-start = (bf16[4,1024]{1,0:T(4,128)(2,1)}, bf16[4,1024]{1,0:T(4,128)(2,1)S(1)}, u32[]{:S(2)}, u32[]{:S(2)}) collective-permute-start(bf16[4,1024]{1,0:T(4,128)(2,1)} %resid_ref.3), channel_id=1, source_target_pairs={{0,2},{1,3},{2,0},{3,1},{4,6},{5,7},{6,4},{7,5},{8,10},{9,11},{10,... | collective-permute-start | bytes 24584 | tf_op jit(solution)/shard_map/ppermute | solution.py:669
  10.6 1.3 %collective-permute-start.3 = (bf16[16,1024]{1,0:T(8,128)(2,1)S(1)}, bf16[16,1024]{1,0:T(8,128)(2,1)S(1)}, u32[]{:S(2)}, u32[]{:S(2)}) collective-permute-start(bf16[16,1024]{1,0:T(8,128)(2,1)S(1)} %shard_map.194.half_ref), channel_id=1, source_target_pairs={{0,1},{1,0},{2,3},{3,2},{4,5},{5,4},{6,7},{7,6},{8,9},{9,8},{10,11... | collective-permute-start | bytes 98312 | tf_op jit(solution)/shard_map/ppermute | solution.py:735
  13.3 4.0 %collective-permute-start.4 = (bf16[8,1920]{1,0:T(8,128)(2,1)S(1)}, bf16[8,1920]{1,0:T(8,128)(2,1)S(1)}, u32[]{:S(2)}, u32[]{:S(2)}) collective-permute-start(bf16[8,1920]{1,0:T(8,128)(2,1)S(1)} %get-tuple-element.41), channel_id=1, source_target_pairs={{0,8},{8,0},{16,24},{24,16},{1,9},{9,1},{17,25},{25,17},{2,10},{10... | collective-permute-start | bytes 92168 | tf_op jit(solution)/shard_map/ppermute | solution.py:669
  14.8 3.9 %collective-permute-start.5 = (bf16[8,1920]{1,0:T(8,128)(2,1)S(1)}, bf16[8,1920]{1,0:T(8,128)(2,1)S(1)}, u32[]{:S(2)}, u32[]{:S(2)}) collective-permute-start(bf16[8,1920]{1,0:T(8,128)(2,1)S(1)} %get-tuple-element.42), channel_id=1, source_target_pairs={{0,16},{8,24},{16,0},{24,8},{1,17},{9,25},{17,1},{25,9},{2,18},{10... | collective-permute-start | bytes 92168 | tf_op jit(solution)/shard_map/ppermute | solution.py:669
  16.3 4.8 %collective-permute-start.6 = (bf16[8,1920]{1,0:T(8,128)(2,1)S(1)}, bf16[8,1920]{1,0:T(8,128)(2,1)S(1)}, u32[]{:S(2)}, u32[]{:S(2)}) collective-permute-start(bf16[8,1920]{1,0:T(8,128)(2,1)S(1)} %get-tuple-element.43), channel_id=1, source_target_pairs={{0,24},{8,16},{16,8},{24,0},{1,25},{9,17},{17,9},{25,1},{2,26},{10... | collective-permute-start | bytes 92168 | tf_op jit(solution)/shard_map/ppermute | solution.py:669
  37.8 14.6 %all-to-all-start.1 = ((bf16[32,8,640]{2,1,0:T(8,128)(2,1)}), bf16[32,8,640]{2,1,0:T(8,128)(2,1)S(1)}, u32[]{:S(2)}, u32[]{:S(2)}) async-start(bf16[32,8,640]{2,1,0:T(8,128)(2,1)} %bitcast.7), calls=%async_computation.1 | async-start | bytes 655360 | tf_op jit(solution)/shard_map/all_to_all | solution.py:662
  54.1 4.3 %collective-permute-start.7 = (bf16[8,4096]{1,0:T(8,128)(2,1)S(1)}, bf16[8,4096]{1,0:T(8,128)(2,1)S(1)}, u32[]{:S(2)}, u32[]{:S(2)}) collective-permute-start(bf16[8,4096]{1,0:T(8,128)(2,1)S(1)} %get-tuple-element.52), channel_id=1, source_target_pairs={{0,8},{8,0},{16,24},{24,16},{1,9},{9,1},{17,25},{25,17},{2,10},{10... | collective-permute-start | bytes 196616 | tf_op jit(solution)/shard_map/ppermute | solution.py:669
  54.2 5.4 %collective-permute-start.8 = (bf16[8,4096]{1,0:T(8,128)(2,1)S(1)}, bf16[8,4096]{1,0:T(8,128)(2,1)S(1)}, u32[]{:S(2)}, u32[]{:S(2)}) collective-permute-start(bf16[8,4096]{1,0:T(8,128)(2,1)S(1)} %get-tuple-element.53), channel_id=1, source_target_pairs={{0,16},{8,24},{16,0},{24,8},{1,17},{9,25},{17,1},{25,9},{2,18},{10... | collective-permute-start | bytes 196616 | tf_op jit(solution)/shard_map/ppermute | solution.py:669
  55.3 5.2 %collective-permute-start.9 = (bf16[8,4096]{1,0:T(8,128)(2,1)S(1)}, bf16[8,4096]{1,0:T(8,128)(2,1)S(1)}, u32[]{:S(2)}, u32[]{:S(2)}) collective-permute-start(bf16[8,4096]{1,0:T(8,128)(2,1)S(1)} %get-tuple-element.54), channel_id=1, source_target_pairs={{0,24},{8,16},{16,8},{24,0},{1,25},{9,17},{17,9},{25,1},{2,26},{10... | collective-permute-start | bytes 196616 | tf_op jit(solution)/shard_map/ppermute | solution.py:669
  61.0 1.3 %collective-permute-start.10 = (bf16[32,512]{1,0:T(8,128)(2,1)S(1)}, bf16[32,512]{1,0:T(8,128)(2,1)S(1)}, u32[]{:S(2)}, u32[]{:S(2)}) collective-permute-start(bf16[32,512]{1,0:T(8,128)(2,1)S(1)} %get-tuple-element.56), channel_id=1, source_target_pairs={{0,1},{1,0},{2,3},{3,2},{4,5},{5,4},{6,7},{7,6},{8,9},{9,8},{10,11... | collective-permute-start | bytes 98312 | tf_op jit(solution)/shard_map/ppermute | solution.py:795
  62.3 5.8 %collective-permute-start.13 = (bf16[32,512]{1,0:T(8,128)(2,1)S(1)}, bf16[32,512]{1,0:T(8,128)(2,1)S(1)}, u32[]{:S(2)}, u32[]{:S(2)}) collective-permute-start(bf16[32,512]{1,0:T(8,128)(2,1)S(1)} %shard_map.202.b0), channel_id=1, source_target_pairs={{0,6},{1,7},{2,4},{3,5},{4,2},{5,3},{6,0},{7,1},{8,14},{9,15},{10,... | collective-permute-start | bytes 98312 | tf_op jit(solution)/shard_map/ppermute | solution.py:669
  64.1 4.9 %collective-permute-start.12 = (bf16[32,512]{1,0:T(8,128)(2,1)S(1)}, bf16[32,512]{1,0:T(8,128)(2,1)S(1)}, u32[]{:S(2)}, u32[]{:S(2)}) collective-permute-start(bf16[32,512]{1,0:T(8,128)(2,1)S(1)} %shard_map.202.b0), channel_id=1, source_target_pairs={{0,4},{1,5},{2,6},{3,7},{4,0},{5,1},{6,2},{7,3},{8,12},{9,13},{10,... | collective-permute-start | bytes 98312 | tf_op jit(solution)/shard_map/ppermute | solution.py:669
  64.1 5.1 %collective-permute-start.11 = (bf16[32,512]{1,0:T(8,128)(2,1)S(1)}, bf16[32,512]{1,0:T(8,128)(2,1)S(1)}, u32[]{:S(2)}, u32[]{:S(2)}) collective-permute-start(bf16[32,512]{1,0:T(8,128)(2,1)S(1)} %shard_map.202.b0), channel_id=1, source_target_pairs={{0,2},{1,3},{2,0},{3,1},{4,6},{5,7},{6,4},{7,5},{8,10},{9,11},{10,... | collective-permute-start | bytes 98312 | tf_op jit(solution)/shard_map/ppermute | solution.py:669
  71.5 4.2 %collective-permute-start.15 = (bf16[32,768]{1,0:T(8,128)(2,1)S(1)}, bf16[32,768]{1,0:T(8,128)(2,1)S(1)}, u32[]{:S(2)}, u32[]{:S(2)}) collective-permute-start(bf16[32,768]{1,0:T(8,128)(2,1)S(1)} %get-tuple-element.60), channel_id=1, source_target_pairs={{0,8},{8,0},{16,24},{24,16},{1,9},{9,1},{17,25},{25,17},{2,10},{10... | collective-permute-start | bytes 147464 | tf_op jit(solution)/shard_map/ppermute | solution.py:669
  72.5 4.1 %collective-permute-start.16 = (bf16[32,768]{1,0:T(8,128)(2,1)S(1)}, bf16[32,768]{1,0:T(8,128)(2,1)S(1)}, u32[]{:S(2)}, u32[]{:S(2)}) collective-permute-start(bf16[32,768]{1,0:T(8,128)(2,1)S(1)} %get-tuple-element.61), channel_id=1, source_target_pairs={{0,16},{8,24},{16,0},{24,8},{1,17},{9,25},{17,1},{25,9},{2,18},{10... | collective-permute-start | bytes 147464 | tf_op jit(solution)/shard_map/ppermute | solution.py:669
  73.9 5.0 %collective-permute-start.17 = (bf16[32,768]{1,0:T(8,128)(2,1)S(1)}, bf16[32,768]{1,0:T(8,128)(2,1)S(1)}, u32[]{:S(2)}, u32[]{:S(2)}) collective-permute-start(bf16[32,768]{1,0:T(8,128)(2,1)S(1)} %get-tuple-element.62), channel_id=1, source_target_pairs={{0,24},{8,16},{16,8},{24,0},{1,25},{9,17},{17,9},{25,1},{2,26},{10... | collective-permute-start | bytes 147464 | tf_op jit(solution)/shard_map/ppermute | solution.py:669
  79.1 4.8 %collective-permute-start.20 = (bf16[32,344]{1,0:T(8,128)(2,1)S(1)}, bf16[32,344]{1,0:T(8,128)(2,1)S(1)}, u32[]{:S(2)}, u32[]{:S(2)}) collective-permute-start(bf16[32,344]{1,0:T(8,128)(2,1)S(1)} %get-tuple-element.64.hidden_ref), channel_id=1, source_target_pairs={{0,24},{8,16},{16,8},{24,0},{1,25},{9,17},{17,9},{25,1},{2,26},{10... | collective-permute-start | bytes 66056 | tf_op jit(solution)/shard_map/ppermute | solution.py:669
  80.3 3.8 %collective-permute-start.19 = (bf16[32,344]{1,0:T(8,128)(2,1)S(1)}, bf16[32,344]{1,0:T(8,128)(2,1)S(1)}, u32[]{:S(2)}, u32[]{:S(2)}) collective-permute-start(bf16[32,344]{1,0:T(8,128)(2,1)S(1)} %get-tuple-element.64.hidden_ref), channel_id=1, source_target_pairs={{0,16},{8,24},{16,0},{24,8},{1,17},{9,25},{17,1},{25,9},{2,18},{10... | collective-permute-start | bytes 66056 | tf_op jit(solution)/shard_map/ppermute | solution.py:669
  81.3 3.8 %collective-permute-start.18 = (bf16[32,344]{1,0:T(8,128)(2,1)S(1)}, bf16[32,344]{1,0:T(8,128)(2,1)S(1)}, u32[]{:S(2)}, u32[]{:S(2)}) collective-permute-start(bf16[32,344]{1,0:T(8,128)(2,1)S(1)} %get-tuple-element.64.hidden_ref), channel_id=1, source_target_pairs={{0,8},{8,0},{16,24},{24,16},{1,9},{9,1},{17,25},{25,17},{2,10},{10... | collective-permute-start | bytes 66056 | tf_op jit(solution)/shard_map/ppermute | solution.py:669
  87.0 4.5 %collective-permute-start.22 = (bf16[4,1024]{1,0:T(4,128)(2,1)S(1)}, bf16[4,1024]{1,0:T(4,128)(2,1)S(1)}, u32[]{:S(2)}, u32[]{:S(2)}) collective-permute-start(bf16[4,1024]{1,0:T(4,128)(2,1)S(1)} %get-tuple-element.68), channel_id=1, source_target_pairs={{0,2},{1,3},{2,0},{3,1},{4,6},{5,7},{6,4},{7,5},{8,10},{9,11},{10,... | collective-permute-start | bytes 24584 | tf_op jit(solution)/shard_map/ppermute | solution.py:669
  88.5 4.6 %collective-permute-start.23 = (bf16[4,1024]{1,0:T(4,128)(2,1)S(1)}, bf16[4,1024]{1,0:T(4,128)(2,1)S(1)}, u32[]{:S(2)}, u32[]{:S(2)}) collective-permute-start(bf16[4,1024]{1,0:T(4,128)(2,1)S(1)} %get-tuple-element.69), channel_id=1, source_target_pairs={{0,4},{1,5},{2,6},{3,7},{4,0},{5,1},{6,2},{7,3},{8,12},{9,13},{10,... | collective-permute-start | bytes 24584 | tf_op jit(solution)/shard_map/ppermute | solution.py:669
  89.4 5.4 %collective-permute-start.24 = (bf16[4,1024]{1,0:T(4,128)(2,1)S(1)}, bf16[4,1024]{1,0:T(4,128)(2,1)S(1)}, u32[]{:S(2)}, u32[]{:S(2)}) collective-permute-start(bf16[4,1024]{1,0:T(4,128)(2,1)S(1)} %get-tuple-element.70), channel_id=1, source_target_pairs={{0,6},{1,7},{2,4},{3,5},{4,2},{5,3},{6,0},{7,1},{8,14},{9,15},{10,... | collective-permute-start | bytes 24584 | tf_op jit(solution)/shard_map/ppermute | solution.py:669
  (21 other events, 112.9 us)
